TPU v7x, 32 devices: a whole 2x2x4 slice. The times are simulated.
32 devices in a mesh: sp: 8 (over z, y), tp: 4 (over x, core).
Axes of the slice: x: 2, y: 2, z: 4, core: 2. Of those that a mesh axis runs over, the one named last changes fastest.
Arguments:
- query_rows: bfloat16 [4096, 2048], P('sp', 'tp'), may hold values from -40 to 40
- key_rows: bfloat16 [4096, 256], P('sp', 'tp'), may hold values from -6 to 6
- value_rows: bfloat16 [4096, 256], P('sp', 'tp'), may hold values from -12 to 12
- doc_ids: int32 [4096], P('sp'), may hold values from 0 to 3, never falling along the last dimension, each value on 1 to 2048 neighbouring positions
- sink_logit: float32 [32], P('tp'), may hold values from 1 to 6
- residual: bfloat16 [4096, 2048], P('sp'), may hold values from -10 to 10
- out_proj: bfloat16 [2048, 2048], P('tp'), may hold values from -0.25 to 0.25
- mix_gain: float32 [2048], replicated, may hold values from 0.1 to 1.9
- gate_proj: bfloat16 [2048, 5632], P('sp', 'tp'), may hold values from -0.125 to 0.125
- value_proj: bfloat16 [2048, 5632], P('sp', 'tp'), may hold values from -0.125 to 0.125
- gate_taps: float32 [3, 5632], P(None, 'tp'), may hold values from -3 to 3
- value_taps: float32 [3, 5632], P(None, 'tp'), may hold values from -3 to 3
- down_proj: bfloat16 [5632, 2048], P('tp', 'sp'), may hold values from -0.078125 to 0.078125
- final_gain: float32 [2048], P('tp'), may hold values from 0.1 to 1.9
Outputs:
- mixed: bfloat16 [4096, 2048], P('sp', 'tp')
All inputs are finite; a program needn't handle non-finite values.
Results may differ from a plain program's by a relative error of at most 0.012.
Values may be sent and summed in bfloat16 or wider, within the bound.
No kernel may reach another device: no remote copies, remote signals or barrier semaphores. Data moves between devices by JAX's collectives and lax.ppermute only.
A program may use at most 128 MiB of HBM per device.

v0:
```python
import math

import jax
import jax.numpy as jnp
from jax import lax
from jax.sharding import PartitionSpec as P

HD = 64
WIN = 128
TAPS = 3


mix_scale = math.sqrt(2.0)
norm_eps = 1e-05


def passed_along(block, axis, distance):
    devices = range(lax.axis_size(axis))
    route = [(i - distance, i) for i in devices if i - distance in devices]
    return lax.ppermute(block, axis, route)


def attend(query_block, key_block, value_block, query_pos, key_pos, query_doc, key_doc, sink):
    head_size = query_block.shape[-1]
    scores = jnp.einsum(
        "qkgd,skd->kgqs", query_block, key_block, preferred_element_type=jnp.float32
    ) * head_size ** (-0.5)
    diff = query_pos[:, None] - key_pos[None, :]
    valid = (
        (diff >= 0)
        & (diff < WIN)
        & (query_doc[:, None] == key_doc[None, :])
        & (key_pos[None, :] >= 0)
    )
    scores = jnp.where(valid[None, None], scores, -1e30)
    top = jnp.maximum(jnp.max(scores, axis=-1, keepdims=True), sink)
    weights = jnp.exp(scores - top)
    total = jnp.sum(weights, axis=-1, keepdims=True) + jnp.exp(sink - top)
    probs = (weights / total).astype(jnp.bfloat16)
    out = jnp.einsum("kgqs,skd->qkgd", probs, value_block, preferred_element_type=jnp.float32)
    return out.astype(jnp.bfloat16)


def depthwise(tail, current, taps, tail_docs, docs):
    extended = jnp.concatenate([tail, current])
    ext_docs = jnp.concatenate([tail_docs, docs])
    lag_rows = tail.shape[0]
    count = current.shape[0]
    total = jnp.zeros(current.shape, jnp.float32)
    for lag in range(lag_rows + 1):
        start = lag_rows - lag
        same = (ext_docs[start : start + count] == docs)[:, None]
        rows = extended[start : start + count].astype(jnp.float32)
        total = total + taps[lag][None, :] * jnp.where(same, rows, 0.0)
    return total


def on_device(
    query_rows,
    key_rows,
    value_rows,
    doc_ids,
    sink_logit,
    residual,
    out_proj,
    mix_gain,
    gate_proj,
    value_proj,
    gate_taps,
    value_taps,
    down_proj,
    final_gain,
):
    rows = query_rows.shape[0]
    kv_local = key_rows.shape[1] // HD
    heads_local = query_rows.shape[1] // HD
    groups = heads_local // kv_local
    offset = lax.axis_index("sp") * rows
    prev_keys, prev_values, prev_docs = passed_along(
        (key_rows[rows - WIN :], value_rows[rows - WIN :], doc_ids[rows - WIN :]), "sp", 1
    )
    all_keys = jnp.concatenate([prev_keys, key_rows]).reshape(rows + WIN, kv_local, HD)
    all_values = jnp.concatenate([prev_values, value_rows]).reshape(rows + WIN, kv_local, HD)
    all_docs = jnp.concatenate([prev_docs, doc_ids])
    key_pos = offset - WIN + jnp.arange(rows + WIN, dtype=jnp.int32)
    query_pos = offset + jnp.arange(rows, dtype=jnp.int32)
    queries = query_rows.reshape(rows, kv_local, groups, HD)
    sink = sink_logit.reshape(kv_local, groups, 1, 1)
    pieces = attend(queries, all_keys, all_values, query_pos, key_pos, doc_ids, all_docs, sink)
    heads = pieces.reshape(rows, heads_local * HD)
    partial_value = jnp.dot(heads, out_proj, preferred_element_type=jnp.float32)
    width = residual.shape[1]
    share = width // lax.axis_size("tp")
    col_start = lax.axis_index("tp") * share
    attn_total = lax.psum(partial_value.astype(jnp.bfloat16), "tp").astype(jnp.float32)
    first_sum = mix_scale * residual.astype(jnp.float32) + attn_total
    mean = jnp.mean(first_sum, axis=1, keepdims=True)
    var = jnp.mean(jnp.square(first_sum - mean), axis=1, keepdims=True)
    normed = ((first_sum - mean) * lax.rsqrt(var + norm_eps) * mix_gain[None, :]).astype(
        jnp.bfloat16
    )
    normed_own = lax.dynamic_slice_in_dim(normed, col_start, share, 1)
    up_gate = jnp.dot(
        normed,
        lax.all_gather(gate_proj, "sp", axis=0, tiled=True),
        preferred_element_type=jnp.float32,
    )
    up_value = jnp.dot(
        normed,
        lax.all_gather(value_proj, "sp", axis=0, tiled=True),
        preferred_element_type=jnp.float32,
    )
    up_gate = up_gate.astype(jnp.bfloat16)
    up_value = up_value.astype(jnp.bfloat16)
    lag_rows = TAPS - 1
    prev_gate, prev_value = passed_along(
        (up_gate[rows - lag_rows :], up_value[rows - lag_rows :]), "sp", 1
    )
    tail_docs = prev_docs[WIN - lag_rows :]
    conv_gate = depthwise(prev_gate, up_gate, gate_taps, tail_docs, doc_ids)
    conv_value = depthwise(prev_value, up_value, value_taps, tail_docs, doc_ids)
    hidden = (jax.nn.gelu(conv_gate) * conv_value).astype(jnp.bfloat16)
    terms = jnp.dot(
        hidden,
        lax.all_gather(down_proj, "sp", axis=1, tiled=True),
        preferred_element_type=jnp.float32,
    )
    ffn_own = lax.psum_scatter(
        terms.astype(jnp.bfloat16), "tp", scatter_dimension=1, tiled=True
    ).astype(jnp.float32)
    second_sum = mix_scale * normed_own.astype(jnp.float32) + ffn_own
    row_sum, row_squares = lax.psum(
        (jnp.sum(second_sum, axis=1), jnp.sum(second_sum * second_sum, axis=1)), "tp"
    )
    mean = row_sum / width
    var = row_squares / width - mean * mean
    return (
        (second_sum - mean[:, None]) * lax.rsqrt(var + norm_eps)[:, None] * final_gain[None, :]
    ).astype(jnp.bfloat16)


def solution(mesh):
    placed = (
        P("sp", "tp"),
        P("sp", "tp"),
        P("sp", "tp"),
        P("sp"),
        P("tp"),
        P("sp", None),
        P("tp", None),
        P(),
        P("sp", "tp"),
        P("sp", "tp"),
        P(None, "tp"),
        P(None, "tp"),
        P("tp", "sp"),
        P("tp"),
    )
    return jax.shard_map(
        on_device, mesh=mesh, in_specs=placed, out_specs=P("sp", "tp"), check_vma=False
    )
```

profile of v0, /device:TPU:0, one launch (start us, length us, event | category | flops | bytes accessed | tf_op | source)
XLA Modules:
  0.0 373.8 jit_solution(1086754709857433635)
XLA Ops:
  7.4 0.0 copy-start
  7.4 0.0 all-reduce.3.cloned.1.call-start
  7.4 0.8 slice.57
  8.2 4.9 %collective-permute-start.1 = (s32[128]{0:T(128)S(1)}, s32[128]{0:T(128)S(1)}, u32[]{:S(2)}, u32[]{:S(2)}) collective-permute-start(s32[128]{0:T(128)S(1)} %slice.57), channel_id=1, source_target_pairs={{0,4},{4,8},{8,12},{12,16},{16,20},{20,24},{24,28},{1,5},{5,9},{9,... | collective-permute-start | bytes 1544 | tf_op jit(solution)/shard_map/ppermute | solution.py:20
  13.1 0.7 slice.58
  13.8 3.4 collective-permute-start.2
  17.2 0.7 slice.56
  18.0 3.4 collective-permute-start
  21.4 1.3 copy.17
  22.7 0.0 collective-permute-done.1
  22.7 0.7 pad_add_fusion
  23.4 1.4 fusion.21
  24.8 0.0 collective-permute-done.2
  24.8 0.0 copy-start.9
  24.8 2.6 fusion.1
  27.4 0.0 copy-done.9
  27.4 0.1 broadcast_maximum_fusion
  27.5 2.1 fusion
  29.6 0.1 exponential_add_fusion
  29.7 0.0 collective-permute-done
  29.7 0.0 copy-done.7
  29.7 3.1 fusion.22
  32.9 0.0 copy-done
  32.9 2.6 convolution_convert_fusion.2
  35.5 0.0 all-reduce.3.cloned.1.call-update
  35.5 0.0 all-gather.4.cloned.1.call-start
  35.6 0.5 all-gather.4.cloned.1.call-update
  36.1 0.0 all-gather.6.cloned.1.call-start
  36.1 0.5 all-gather.6.cloned.1.call-update
  36.7 0.0 all-gather.8.cloned.1.call-start
  36.7 0.5 all-gather.8.cloned.1.call-update
  37.2 0.2 reduce-scatter.2.cloned.1.call-start
  37.5 0.0 copy-done.4
  37.5 0.0 copy-done.5
  37.5 0.1 slice_reduce_fusion.2
  37.6 0.1 slice.61
  37.7 0.0 copy-done.3
  37.7 0.1 pad_add_fusion.1
  37.7 48.6 %all-reduce.3.cloned.1.call-done = bf16[512,2048]{1,0:T(8,128)(2,1)} async-done(((bf16[512,2048]{1,0:T(8,128)(2,1)}), bf16[512,2048]{1,0:T(8,128)(2,1)}) %all-reduce.3.cloned.1.call-update) | async-done | bytes 2097168 | tf_op jit(solution)/shard_map/psum | solution.py:95
  86.3 3.1 fusion.4
  89.5 0.0 copy-done.1
  89.5 0.4 copy-done.2
  89.8 1.0 multiply_reduce_fusion
  90.8 0.0 copy-done.6
  90.9 2.4 multiply_convert_fusion
  93.2 36.4 %all-gather.4.cloned.1.call-done = bf16[2048,1408]{1,0:T(8,128)(2,1)} async-done(((bf16[256,1408]{1,0:T(8,128)(2,1)}), bf16[2048,1408]{1,0:T(8,128)(2,1)}) %all-gather.4.cloned.1.call-update) | async-done | bytes 5767184 | tf_op jit(solution)/shard_map/all_gather | solution.py:105
  129.6 6.7 %convolution_convert_fusion.1 = bf16[512,1408]{1,0:T(8,128)(2,1)S(1)} fusion(bf16[512,2048]{1,0:T(8,128)(2,1)} %multiply_convert_fusion, bf16[2048,1408]{1,0:T(8,128)(2,1)} %all-gather.4.cloned.1.call-done), kind=kOutput, calls=%fused_computation.13 | convolution fusion | flops 2953510912 | bytes 9306112 | tf_op jit(solution)/shard_map/dot_general | solution.py:103
  136.3 0.0 copy-start.10
  136.3 1.1 copy-done.10
  137.5 2.5 collective-permute-start.3
  139.9 82.1 %all-gather.6.cloned.1.call-done = bf16[2048,1408]{1,0:T(8,128)(2,1)} async-done(((bf16[256,1408]{1,0:T(8,128)(2,1)}), bf16[2048,1408]{1,0:T(8,128)(2,1)}) %all-gather.6.cloned.1.call-update) | async-done | bytes 5767184 | tf_op jit(solution)/shard_map/all_gather | solution.py:110
  222.0 6.7 %convolution_convert_fusion = bf16[512,1408]{1,0:T(8,128)(2,1)S(1)} fusion(bf16[512,2048]{1,0:T(8,128)(2,1)} %multiply_convert_fusion, bf16[2048,1408]{1,0:T(8,128)(2,1)} %all-gather.6.cloned.1.call-done), kind=kOutput, calls=%fused_computation.12 | convolution fusion | flops 2953510912 | bytes 9306112 | tf_op jit(solution)/shard_map/dot_general | solution.py:108
  228.7 2.5 collective-permute-start.4
  231.2 0.1 slice_compare_fusion.1
  231.3 83.8 %all-gather.8.cloned.1.call-done = bf16[1408,2048]{1,0:T(8,128)(2,1)} async-done(((bf16[1408,256]{1,0:T(8,128)(2,1)}), bf16[1408,2048]{1,0:T(8,128)(2,1)}) %all-gather.8.cloned.1.call-update) | async-done | bytes 5767184 | tf_op jit(solution)/shard_map/all_gather | solution.py:125
  315.1 0.0 collective-permute-done.3
  315.1 0.0 collective-permute-done.4
  315.1 12.0 %convolution_convert_fusion.3 = bf16[512,2048]{1,0:T(8,128)(2,1)} fusion(bf16[1408,2048]{1,0:T(8,128)(2,1)} %all-gather.8.cloned.1.call-done, bf16[512,1408]{1,0:T(8,128)(2,1)} %copy-done.11, bf16[512,1408]{1,0:T(8,128)(2,1)} %copy-done.10, bf16[2,1408]{1,0:T(2,128)(2,1)S(1)} %collective-permute-done.4, bf16[2,1408]{1,0:T(2,128)(2,1)S(1)} %collective-permute-done.3, ...), kind=kOutput, calls=%fused_computation.15 | convolution fusion | flops 2984116224 | bytes 10793984 | tf_op jit(solution)/shard_map/dot_general | solution.py:123
  327.1 0.0 reduce-scatter.2.cloned.1.call-update
  327.1 29.5 %reduce-scatter.2.cloned.1.call-done = bf16[512,512]{1,0:T(8,128)(2,1)} async-done(((bf16[512,2048]{1,0:T(8,128)(2,1)}), bf16[512,512]{1,0:T(8,128)(2,1)}) %reduce-scatter.2.cloned.1.call-update) | async-done | bytes 524304 | tf_op jit(solution)/shard_map/reduce_scatter | solution.py:128
  356.6 1.5 fusion.25
  358.2 5.8 %all-reduce = (f32[512]{0:T(512)S(1)}, f32[512]{0:T(512)S(1)}) all-reduce(f32[512]{0:T(512)S(1)} %get-tuple-element.6, f32[512]{0:T(512)S(1)} %get-tuple-element.5), channel_id=1, replica_groups=mesh['sp'=8,'tp'=4] {'tp'}, use_global_device_ids=true, to_apply=%region_9.10 | all-reduce | flops 1024 | bytes 8192 | tf_op jit(solution)/shard_map/psum | solution.py:132
  363.9 0.0 copy-done.8
  363.9 2.3 multiply_convert_fusion.1
  (18 shorter events, 0.1 us)
Async XLA Ops:
  7.4 25.5 %copy-start = (bf16[512,2048]{1,0:T(8,128)(2,1)S(1)}, bf16[512,2048]{1,0:T(8,128)(2,1)}, u32[]{:S(2)}) copy-start(bf16[512,2048]{1,0:T(8,128)(2,1)} %param.20) | copy-start | bytes 6291460
  7.4 78.9 %all-reduce.3.cloned.1.call-start = ((), (), s32[]{:S(2)}) async-start(), calls=%async_computation.1 | async-start | bytes 4194304 | tf_op jit(solution)/shard_map/psum | solution.py:95
  8.2 14.5 %collective-permute-start.1 = (s32[128]{0:T(128)S(1)}, s32[128]{0:T(128)S(1)}, u32[]{:S(2)}, u32[]{:S(2)}) collective-permute-start(s32[128]{0:T(128)S(1)} %slice.57), channel_id=1, source_target_pairs={{0,4},{4,8},{8,12},{12,16},{16,20},{20,24},{24,28},{1,5},{5,9},{9,... | collective-permute-start | bytes 1544 | tf_op jit(solution)/shard_map/ppermute | solution.py:20
  13.8 11.0 %collective-permute-start.2 = (bf16[128,64]{0,1:T(8,128)(2,1)S(1)}, bf16[128,64]{0,1:T(8,128)(2,1)S(1)}, u32[]{:S(2)}, u32[]{:S(2)}) collective-permute-start(bf16[128,64]{0,1:T(8,128)(2,1)S(1)} %slice.58), channel_id=1, source_target_pairs={{0,4},{4,8},{8,12},{12,16},{16,20},{20,24},{24,28},{1,5},{5,9},{9,... | collective-permute-start | bytes 49160 | tf_op jit(solution)/shard_map/ppermute | solution.py:20
  18.0 11.7 %collective-permute-start = (bf16[128,64]{0,1:T(8,128)(2,1)S(1)}, bf16[128,64]{0,1:T(8,128)(2,1)S(1)}, u32[]{:S(2)}, u32[]{:S(2)}) collective-permute-start(bf16[128,64]{0,1:T(8,128)(2,1)S(1)} %slice.56), channel_id=1, source_target_pairs={{0,4},{4,8},{8,12},{12,16},{16,20},{20,24},{24,28},{1,5},{5,9},{9,... | collective-permute-start | bytes 49160 | tf_op jit(solution)/shard_map/ppermute | solution.py:20
  24.8 2.6 copy-start.9
  27.5 2.2 copy-start.7
  35.5 2.0 copy-start.4
  35.5 2.0 copy-start.5
  35.5 2.2 copy-start.3
  35.5 94.1 %all-gather.4.cloned.1.call-start = ((), (), s32[]{:S(2)}) async-start(), calls=%async_computation.2 | async-start | bytes 6488064 | tf_op jit(solution)/shard_map/all_gather | solution.py:105
  36.1 185.9 %all-gather.6.cloned.1.call-start = ((), (), s32[]{:S(2)}) async-start(), calls=%async_computation.3 | async-start | bytes 6488064 | tf_op jit(solution)/shard_map/all_gather | solution.py:110
  36.7 278.4 %all-gather.8.cloned.1.call-start = ((), (), s32[]{:S(2)}) async-start(), calls=%async_computation.4 | async-start | bytes 6488064 | tf_op jit(solution)/shard_map/all_gather | solution.py:125
  37.2 319.4 %reduce-scatter.2.cloned.1.call-start = ((), (), s32[]{:S(2)}) async-start(), calls=%async_computation.5 | async-start | bytes 2621440 | tf_op jit(solution)/shard_map/reduce_scatter | solution.py:128
  86.3 3.1 copy-start.1
  86.3 3.5 copy-start.2
  89.4 1.4 copy-start.6
  136.3 1.1 copy-start.10
  137.5 177.6 %collective-permute-start.3 = (bf16[2,1408]{1,0:T(2,128)(2,1)S(1)}, bf16[2,1408]{1,0:T(2,128)(2,1)S(1)}, u32[]{:S(2)}, u32[]{:S(2)}) collective-permute-start(bf16[2,1408]{1,0:T(2,128)(2,1)S(1)} %slice.74), channel_id=1, source_target_pairs={{0,4},{4,8},{8,12},{12,16},{16,20},{20,24},{24,28},{1,5},{5,9},{9,... | collective-permute-start | bytes 16904 | tf_op jit(solution)/shard_map/ppermute | solution.py:20
  228.7 2.5 copy-start.11
  228.7 86.3 %collective-permute-start.4 = (bf16[2,1408]{1,0:T(2,128)(2,1)S(1)}, bf16[2,1408]{1,0:T(2,128)(2,1)S(1)}, u32[]{:S(2)}, u32[]{:S(2)}) collective-permute-start(bf16[2,1408]{1,0:T(2,128)(2,1)S(1)} %slice.77), channel_id=1, source_target_pairs={{0,4},{4,8},{8,12},{12,16},{16,20},{20,24},{24,28},{1,5},{5,9},{9,... | collective-permute-start | bytes 16904 | tf_op jit(solution)/shard_map/ppermute | solution.py:20
  327.1 36.8 %copy-start.8 = (f32[512]{0:T(512)S(1)}, f32[512]{0:T(512)}, u32[]{:S(2)}) copy-start(f32[512]{0:T(512)} %param.27) | copy-start | bytes 6148
Sparse Core Ops, SparseCore 0:
  35.6 50.6 all-reduce.2
  327.2 29.3 reduce-scatter.1
Sparse Core Ops, SparseCore 1:
  38.2 91.4 all-gather.3
  131.7 90.3 all-gather.5
  223.9 91.1 all-gather.7
where the time goes:
time: 374 us
  waiting for transfers between devices  282 us (75%)
  matrix products  33.7 us (9%)
  starting transfers between devices  17 us (5%)
  between operations  15.3 us (4%)
  other arithmetic  14.9 us (4%)
  blocking collectives  5.76 us (2%)
  local copies, waits for them, and re-layouts  5.23 us (1%)
    all_gather x1, waiting for transfers between devices, on_device(): lax.all_gather(down_proj, 'sp', axis=1, tiled=True)  83.8 us
    all_gather x1, waiting for transfers between devices, on_device(): lax.all_gather(value_proj, 'sp', axis=0, tiled=True)  82.1 us
    psum x1, waiting for transfers between devices, on_device(): lax.psum(partial_value.astype(jnp.bfloat16), 'tp').astype(jnp.float32)  48.6 us
    all_gather x1, waiting for transfers between devices, on_device(): lax.all_gather(gate_proj, 'sp', axis=0, tiled=True)  36.4 us
    reduce_scatter x1, waiting for transfers between devices, on_device(): lax.psum_scatter(terms.astype(jnp.bfloat16), 'tp', scatter_dimension=1, t...  29.5 us
    ppermute x5, starting transfers between devices, passed_along(): return lax.ppermute(block, axis, route)  16.6 us
    dot_general x1, matrix products, on_device(): jnp.dot(hidden, lax.all_gather(down_proj, 'sp', axis=1, tiled=True), pref...  12 us
  transfers between devices with their start and end apart: 10, of which 5 were waited for; matrix products, arithmetic and copies ran while one was open for 8% of the time, Pallas kernels for 0%

commit v1 on v0

--- a/solution.py
+++ b/solution.py
@@ -1,13 +1,19 @@
+import functools
 import math
 
 import jax
 import jax.numpy as jnp
 from jax import lax
+from jax.experimental import pallas as pl
+from jax.experimental.pallas import tpu as pltpu
 from jax.sharding import PartitionSpec as P
+
 
 HD = 64
 WIN = 128
 TAPS = 3
+LANES = 128
+TAIL = 8
 
 
 mix_scale = math.sqrt(2.0)
@@ -18,6 +24,20 @@
     devices = range(lax.axis_size(axis))
     route = [(i - distance, i) for i in devices if i - distance in devices]
     return lax.ppermute(block, axis, route)
+
+
+def swapped(block, sp_mask=0, tp_mask=0):
+    n_sp, n_tp = lax.axis_size("sp"), lax.axis_size("tp")
+    if not tp_mask:
+        return lax.ppermute(block, "sp", [(i, i ^ sp_mask) for i in range(n_sp)])
+    if not sp_mask:
+        return lax.ppermute(block, "tp", [(i, i ^ tp_mask) for i in range(n_tp)])
+    route = [
+        (i * n_tp + j, (i ^ sp_mask) * n_tp + (j ^ tp_mask))
+        for i in range(n_sp)
+        for j in range(n_tp)
+    ]
+    return lax.ppermute(block, ("sp", "tp"), route)
 
 
 def attend(query_block, key_block, value_block, query_pos, key_pos, query_doc, key_doc, sink):
@@ -53,6 +73,576 @@
         rows = extended[start : start + count].astype(jnp.float32)
         total = total + taps[lag][None, :] * jnp.where(same, rows, 0.0)
     return total
+
+
+def room(mib):
+    return pltpu.CompilerParams(vmem_limit_bytes=mib << 20)
+
+
+def hbm():
+    return pl.BlockSpec(memory_space=pltpu.HBM)
+
+
+def vmem():
+    return pl.BlockSpec(memory_space=pltpu.VMEM)
+
+
+def prepare_kernel(
+    which, gates, values_in, queries, keys, values, docs, residual, own, other, halo, *scratch
+):
+    q, k, v, r, gate, value, sems = scratch
+    cols = gate.shape[1]
+    rows = queries.shape[0]
+    whole = [
+        pltpu.make_async_copy(src, dst, sems.at[4 + i])
+        for i, (src, dst) in enumerate(((gates, gate), (values_in, value)))
+    ]
+    for copy in whole:
+        copy.start()
+    copies = [
+        pltpu.make_async_copy(src.at[pl.ds(rows - TAIL, TAIL)], dst, sems.at[i])
+        for i, (src, dst) in enumerate(((queries, q), (residual, r)))
+    ] + [
+        pltpu.make_async_copy(src.at[:, pl.ds(rows - 2 * WIN, 2 * WIN)], dst, sems.at[2 + i])
+        for i, (src, dst) in enumerate(((keys, k), (values, v)))
+    ]
+    for copy in copies:
+        copy.start()
+    for copy in copies:
+        copy.wait()
+    at = 0
+    for src in (k, v, docs, q, r):
+        for n in range(0, src.shape[1], LANES):
+            halo[at : at + src.shape[0], :] = src[:, n : n + LANES]
+            at += src.shape[0]
+    for copy in whole:
+        copy.wait()
+    half = cols // 2
+    main = half // LANES * LANES
+    rest = half - main
+
+    def emit(part, out):
+        start = part * (cols - main)
+        for n in range(0, main, LANES):
+            out[:, 2 * n : 2 * n + LANES] = gate[:, start + n : start + n + LANES]
+            out[:, 2 * n + LANES : 2 * n + 2 * LANES] = value[:, start + n : start + n + LANES]
+        left = gate[:, main : main + LANES].astype(jnp.float32)
+        right = value[:, main : main + LANES].astype(jnp.float32)
+        if part:
+            left = pltpu.roll(left, rest, 1)
+        else:
+            right = pltpu.roll(right, rest, 1)
+        lane = lax.broadcasted_iota(jnp.int32, left.shape, 1)
+        out[:, 2 * main :] = jnp.where(lane < rest, left, right).astype(out.dtype)
+
+    @pl.when(which[0] == 0)
+    def _():
+        emit(0, own)
+        emit(1, other)
+
+    @pl.when(which[0] != 0)
+    def _():
+        emit(1, own)
+        emit(0, other)
+
+
+def prepared(which, gate, value, queries, keys, values, docs, residual):
+    shape = jax.ShapeDtypeStruct(gate.shape, gate.dtype)
+    lines = 4 * HD * WIN // LANES + TAIL + TAIL * (queries.shape[1] + residual.shape[1]) // LANES
+    scratch = [(TAIL, queries.shape[1]), (HD, 2 * WIN), (HD, 2 * WIN)]
+    scratch += [(TAIL, residual.shape[1]), gate.shape, gate.shape]
+    return pl.pallas_call(
+        prepare_kernel,
+        in_specs=[pl.BlockSpec(memory_space=pltpu.SMEM)] + [hbm()] * 5 + [vmem(), hbm()],
+        out_specs=[vmem()] * 3,
+        out_shape=[shape, shape, jax.ShapeDtypeStruct((lines, LANES), jnp.bfloat16)],
+        scratch_shapes=[pltpu.VMEM(size, jnp.bfloat16) for size in scratch]
+        + [pltpu.SemaphoreType.DMA((6,))],
+        compiler_params=room(56),
+        name="prepare",
+    )(which, gate, value, queries, keys.T, values.T, docs, residual)
+
+
+def row_halves_kernel(which, down, own, other, sems):
+    rows = down.shape[0]
+    half = rows // 2
+    main = half // LANES * LANES
+    rest = half - main
+    for f, out in enumerate((own, other)):
+        part = which[0] ^ f
+        start = pl.multiple_of(part * (rows - main), 2 * TAIL)
+        left = pl.multiple_of(main + part * rest, 2 * TAIL)
+        copies = [
+            pltpu.make_async_copy(
+                down.at[pl.ds(start, main)], out.at[pl.ds(0, main)], sems.at[f, 0]
+            ),
+            pltpu.make_async_copy(
+                down.at[pl.ds(left, rest)], out.at[pl.ds(main, rest)], sems.at[f, 1]
+            ),
+        ]
+        for copy in copies:
+            copy.start()
+    for f, out in enumerate((own, other)):
+        pltpu.make_async_copy(
+            down.at[pl.ds(0, main)], out.at[pl.ds(0, main)], sems.at[f, 0]
+        ).wait()
+        pltpu.make_async_copy(
+            down.at[pl.ds(0, rest)], out.at[pl.ds(main, rest)], sems.at[f, 1]
+        ).wait()
+
+
+def row_halves(which, down):
+    shape = jax.ShapeDtypeStruct((down.shape[0] // 2, down.shape[1]), down.dtype)
+    return pl.pallas_call(
+        row_halves_kernel,
+        in_specs=[pl.BlockSpec(memory_space=pltpu.SMEM), hbm()],
+        out_specs=[vmem(), vmem()],
+        out_shape=[shape, shape],
+        scratch_shapes=[pltpu.SemaphoreType.DMA((2, 2))],
+        compiler_params=room(56),
+        name="row_halves",
+    )(which, down)
+
+
+def up_kernel(place, *refs, pieces, quarter):
+    chunks = refs[:4]
+    weights = refs[4 : 4 + pieces]
+    taps, hidden, own_normed, xs, ws, up, flags, same, sems = refs[4 + pieces :]
+    sp, tp = place[0], place[1]
+    x, core = tp // 2, tp % 2
+    piece_rows = weights[0].shape[0]
+    block = 4 * quarter
+    copies = []
+
+    def begin(src, dst):
+        copy = pltpu.make_async_copy(src, dst, sems.at[len(copies)])
+        copy.start()
+        copies.append(copy)
+
+    for i, chunk in enumerate(chunks):
+        number = (x ^ (i % 2)) * 2 + (core ^ (i // 2))
+        begin(
+            chunk.at[pl.ds(TAIL, quarter)],
+            xs.at[pl.ds(pl.multiple_of(TAIL + number * quarter, TAIL), quarter)],
+        )
+
+        begin(chunk.at[pl.ds(0, TAIL), pl.ds(0, LANES)], flags.at[number])
+
+        @pl.when(number == 0)
+        def _(chunk=chunk):
+            pltpu.make_async_copy(
+                chunk.at[pl.ds(0, TAIL)], xs.at[pl.ds(0, TAIL)], sems.at[8 + pieces]
+            ).start()
+
+    for j in range(pieces):
+        begin(weights[j], ws.at[pl.ds(pl.multiple_of((sp ^ j) * piece_rows, piece_rows), piece_rows)])
+    pltpu.make_async_copy(
+        chunks[0].at[pl.ds(0, TAIL)], xs.at[pl.ds(0, TAIL)], sems.at[8 + pieces]
+    ).wait()
+    for copy in copies:
+        copy.wait()
+
+    half = ws.shape[1] // 2
+    main = half // LANES * LANES
+    rest = half - main
+    pair = 2 * LANES
+    sub = 64
+    line = lax.broadcasted_iota(jnp.int32, (quarter, quarter), 0)
+    diagonal = line == lax.broadcasted_iota(jnp.int32, (quarter, quarter), 1)
+    ones = jnp.ones((quarter, LANES), jnp.bfloat16)
+    for i in range(4):
+        rows = flags[i].astype(jnp.float32)
+        for lag in range(2):
+            spread = jnp.where(diagonal, rows[lag : lag + 1], 0.0).astype(jnp.bfloat16)
+            same[lag, i * quarter : (i + 1) * quarter] = jnp.dot(
+                spread, ones, preferred_element_type=jnp.float32
+            )
+    up[...] = jnp.dot(xs[...], ws[...], preferred_element_type=jnp.float32)
+
+    def conv(rows, start, tap, one, two):
+        lag1 = rows[TAIL - 1 : TAIL - 1 + sub, start : start + LANES]
+        lag2 = rows[TAIL - 2 : TAIL - 2 + sub, start : start + LANES]
+        return (
+            tap[0:1] * rows[TAIL:, start : start + LANES]
+            + tap[1:2] * jnp.where(one > 0, lag1, 0.0)
+            + tap[2:3] * jnp.where(two > 0, lag2, 0.0)
+        )
+
+    def gelu(v):
+        inner = v * (math.sqrt(2.0 / math.pi) + (0.044715 * math.sqrt(2.0 / math.pi)) * (v * v))
+        return (0.5 * v) * (1.0 + jnp.tanh(inner))
+
+    def mix(i, _):
+        at = pl.ds(pl.multiple_of(i * sub, sub), sub)
+        reach = pl.ds(pl.multiple_of(i * sub, sub), sub + TAIL)
+        one, two = same[0, at, :], same[1, at, :]
+        for n in range(0, main, LANES):
+            rows = up[reach, 2 * n : 2 * n + pair]
+            tap = taps[:, 2 * n : 2 * n + pair]
+            h = gelu(conv(rows, 0, tap[:, :LANES], one, two))
+            h = h * conv(rows, LANES, tap[:, LANES:], one, two)
+            hidden[at, n : n + LANES] = h.astype(hidden.dtype)
+        mixed = conv(up[reach, 2 * main :], 0, taps[:, 2 * main :], one, two)
+        h = gelu(mixed) * pltpu.roll(mixed, rest, 1)
+        hidden[at, main:] = h[:, :rest].astype(hidden.dtype)
+        return 0
+
+    lax.fori_loop(0, block // sub, mix, 0)
+    share = own_normed.shape[1]
+    own_normed[...] = xs[TAIL:, pl.ds(pl.multiple_of(tp * share, share), share)]
+
+
+def up_hidden(place, chunks, weights, taps, share):
+    quarter = chunks[0].shape[0] - TAIL
+    width = chunks[0].shape[1]
+    block = 4 * quarter
+    cols = weights[0].shape[1]
+    anywhere = pl.BlockSpec(memory_space=pl.ANY)
+    return pl.pallas_call(
+        functools.partial(up_kernel, pieces=len(weights), quarter=quarter),
+        in_specs=[pl.BlockSpec(memory_space=pltpu.SMEM)]
+        + [anywhere] * (4 + len(weights))
+        + [vmem()],
+        out_specs=[vmem(), vmem()],
+        out_shape=[
+            jax.ShapeDtypeStruct((block, cols // 2), jnp.bfloat16),
+            jax.ShapeDtypeStruct((block, share), jnp.bfloat16),
+        ],
+        scratch_shapes=[
+            pltpu.VMEM((block + TAIL, width), jnp.bfloat16),
+            pltpu.VMEM((width, cols), jnp.bfloat16),
+            pltpu.VMEM((block + TAIL, cols), jnp.float32),
+            pltpu.VMEM((4, TAIL, LANES), jnp.bfloat16),
+            pltpu.VMEM((2, block, LANES), jnp.float32),
+            pltpu.SemaphoreType.DMA((9 + len(weights),)),
+        ],
+        compiler_params=room(24),
+        name="up_hidden",
+    )(place, *chunks, *weights, taps)
+
+
+def project_kernel(place, heads, weights, keep, send, left, right, made, came, went, *, quarter):
+    core = place[1] % 2
+    count = right.shape[0]
+    wide = right.shape[2]
+    loads = [pltpu.make_async_copy(heads, left, came.at[count])]
+    for n in range(count):
+        cols = pl.ds(n * wide, wide)
+        loads.append(pltpu.make_async_copy(weights.at[:, cols], right.at[n], came.at[n]))
+    for copy in loads:
+        copy.start()
+    loads[0].wait()
+    stores = []
+    for n in range(count):
+        loads[1 + n].wait()
+        term = jnp.dot(left[...], right[n], preferred_element_type=jnp.float32)
+        made[n] = term.astype(made.dtype)
+        for f, (out, owner) in enumerate(((send, 1 - core), (keep, core))):
+            for x in range(2):
+                start = pl.multiple_of((2 * x + owner) * quarter, quarter)
+                copy = pltpu.make_async_copy(
+                    made.at[n, pl.ds(start, quarter + TAIL)],
+                    out.at[x, :, pl.ds(n * wide, wide)],
+                    went.at[n, 2 * f + x],
+                )
+                copy.start()
+                stores.append(copy)
+    for copy in stores:
+        copy.wait()
+
+
+def project(place, heads, weights, quarter):
+    count, rows = 4, heads.shape[0]
+    depth, width = weights.shape
+    shape = jax.ShapeDtypeStruct((2, quarter + TAIL, width), jnp.bfloat16)
+    anywhere = pl.BlockSpec(memory_space=pl.ANY)
+    return pl.pallas_call(
+        functools.partial(project_kernel, quarter=quarter),
+        in_specs=[pl.BlockSpec(memory_space=pltpu.SMEM), anywhere, anywhere],
+        out_specs=[anywhere, anywhere],
+        out_shape=[shape, shape],
+        scratch_shapes=[
+            pltpu.VMEM((rows, depth), jnp.bfloat16),
+            pltpu.VMEM((count, depth, width // count), jnp.bfloat16),
+            pltpu.VMEM((count, rows, width // count), jnp.bfloat16),
+            pltpu.SemaphoreType.DMA((count + 1,)),
+            pltpu.SemaphoreType.DMA((count, 4)),
+        ],
+        compiler_params=room(56),
+        name="project",
+    )(place, heads, weights)
+
+
+def merge_kernel(which, first, second, keep, send, a, b, c, came, went, *, axis):
+    own = which[0]
+    pieces = []
+    for out, part in ((send, 1 - own), (keep, own)):
+        for j in range(first.shape[1 - axis]):
+            pieces.append((out.at[j], (part, j) if axis == 0 else (j, part)))
+    copies = []
+    for i, (_, at) in enumerate(pieces):
+        pair = [
+            pltpu.make_async_copy(src.at[at], dst.at[i], came.at[i, f])
+            for f, (src, dst) in enumerate(((first, a), (second, b)))
+        ]
+        for copy in pair:
+            copy.start()
+        copies.append(pair)
+    outs = []
+    for i, (out, _) in enumerate(pieces):
+        for copy in copies[i]:
+            copy.wait()
+        c[i] = a[i] + b[i]
+        outs.append(pltpu.make_async_copy(c.at[i], out, went.at[i]))
+        outs[-1].start()
+    for copy in outs:
+        copy.wait()
+
+
+def merge(which, first, second, axis, mib=8):
+    count = first.shape[1 - axis]
+    shape = jax.ShapeDtypeStruct((count, *first.shape[2:]), jnp.bfloat16)
+    anywhere = pl.BlockSpec(memory_space=pl.ANY)
+    scratch = pltpu.VMEM((2 * count, *first.shape[2:]), jnp.bfloat16)
+    return pl.pallas_call(
+        functools.partial(merge_kernel, axis=axis),
+        in_specs=[pl.BlockSpec(memory_space=pltpu.SMEM), anywhere, anywhere],
+        out_specs=[anywhere, anywhere],
+        out_shape=[shape, shape],
+        scratch_shapes=[scratch] * 3
+        + [pltpu.SemaphoreType.DMA((2 * count, 2)), pltpu.SemaphoreType.DMA((2 * count,))],
+        compiler_params=room(mib),
+        name="merge",
+    )(which, first, second)
+
+
+def norm_kernel(place, first, second, residual, before, gain, flags, out, base, sems):
+    tp = place[1]
+    rows = first.shape[0]
+    quarter = rows - TAIL
+    start = pl.multiple_of(tp * quarter, quarter)
+    body = pltpu.make_async_copy(
+        residual.at[pl.ds(start, quarter)], base.at[pl.ds(TAIL, quarter)], sems.at[0]
+    )
+    body.start()
+    top = base.at[pl.ds(0, TAIL)]
+
+    @pl.when(tp == 0)
+    def _():
+        pltpu.make_async_copy(before, top, sems.at[1]).start()
+
+    @pl.when(tp != 0)
+    def _():
+        at = pl.multiple_of(jnp.maximum(start - TAIL, 0), TAIL)
+        pltpu.make_async_copy(residual.at[pl.ds(at, TAIL)], top, sems.at[1]).start()
+
+    pltpu.make_async_copy(before, top, sems.at[1]).wait()
+    body.wait()
+    group = 64
+    for r in range(0, rows, group):
+        at = slice(r, min(r + group, rows))
+        total = first[at].astype(jnp.float32) + second[at].astype(jnp.float32)
+        total = mix_scale * base[at].astype(jnp.float32) + total
+        mean = jnp.mean(total, axis=1, keepdims=True)
+        var = jnp.mean(total * total, axis=1, keepdims=True) - mean * mean
+        out[at] = ((total - mean) * lax.rsqrt(var + norm_eps) * gain[...]).astype(out.dtype)
+    line = lax.broadcasted_iota(jnp.int32, (TAIL, LANES), 0)
+    rows_of = out[:TAIL, :LANES].astype(jnp.float32)
+    out[:TAIL, :LANES] = jnp.where(line < 2, flags[...], rows_of).astype(out.dtype)
+
+
+def normed_rows(place, first, second, residual, before, gain, flags):
+    return pl.pallas_call(
+        norm_kernel,
+        in_specs=[pl.BlockSpec(memory_space=pltpu.SMEM), vmem(), vmem(), hbm(), hbm(), vmem(), vmem()],
+        out_specs=vmem(),
+        out_shape=jax.ShapeDtypeStruct(first.shape, jnp.bfloat16),
+        scratch_shapes=[pltpu.VMEM(first.shape, jnp.bfloat16), pltpu.SemaphoreType.DMA((2,))],
+        compiler_params=room(56),
+        name="normed_rows",
+    )(place, first, second, residual, before, gain, flags)
+
+
+def down_kernel(place, near, far, *refs):
+    *pieces, keep, send, ws, sems = refs
+    sp, tp = place[0], place[1]
+    low, high, core = (sp // 2) % 2, sp // 4, tp % 2
+    width = pieces[0].shape[1]
+    copies = []
+    for k, piece in enumerate(pieces):
+        slot = 2 * (low ^ (k % 2) ^ core) + (high ^ (k // 2))
+        dst = ws.at[:, pl.ds(pl.multiple_of(slot * width, width), width)]
+        copies.append(pltpu.make_async_copy(piece, dst, sems.at[k]))
+        copies[-1].start()
+    for copy in copies:
+        copy.wait()
+    for out, base in ((send, 2 * width), (keep, 0)):
+        for m, hidden in enumerate((near, far)):
+            term = jnp.dot(
+                hidden[...], ws[:, base : base + 2 * width], preferred_element_type=jnp.float32
+            )
+            for owner_x in range(2):
+                out[owner_x, m] = term[:, owner_x * width : (owner_x + 1) * width].astype(out.dtype)
+
+
+def down_terms(place, near, far, pieces):
+    shape = (2, 2, near.shape[0], pieces[0].shape[1])
+    shape = jax.ShapeDtypeStruct(shape, jnp.bfloat16)
+    anywhere = pl.BlockSpec(memory_space=pl.ANY)
+    return pl.pallas_call(
+        down_kernel,
+        in_specs=[pl.BlockSpec(memory_space=pltpu.SMEM), vmem(), vmem()] + [anywhere] * len(pieces),
+        out_specs=[vmem(), vmem()],
+        out_shape=[shape, shape],
+        scratch_shapes=[
+            pltpu.VMEM((pieces[0].shape[0], len(pieces) * pieces[0].shape[1]), jnp.bfloat16),
+            pltpu.SemaphoreType.DMA((len(pieces),)),
+        ],
+        compiler_params=room(12),
+        name="down_terms",
+    )(place, near, far, *pieces)
+
+
+def reduced(keep, send, x, x_first):
+    rows, cols = keep.shape[2:]
+    own = jnp.zeros((1,), jnp.int32)
+    came = swapped(send, tp_mask=1)
+    keep, send = merge(x if x_first else own, keep, came, 0 if x_first else 1)
+    came = swapped(send, *((0, 2) if x_first else (2, 0)))
+    parts = lambda array: array.reshape(2, 2, rows // 2, cols)
+    keep, send = merge(own if x_first else x, parts(keep), parts(came), 0)
+    came = swapped(send, *((2, 0) if x_first else (0, 2)))
+    return keep.reshape(rows, cols), came.reshape(rows, cols)
+
+
+def local_heads(came, query_rows, key_rows, value_rows, doc_ids, sink_logit):
+    rows = query_rows.shape[0]
+    kv_local = key_rows.shape[1] // HD
+    heads_local = query_rows.shape[1] // HD
+    groups = heads_local // kv_local
+    reach = WIN + TAIL
+    offset = lax.axis_index("sp") * rows
+    at = 4 * HD * WIN // LANES
+    wide = lambda lines: jnp.concatenate(
+        [lines[i : i + TAIL] for i in range(0, lines.shape[0], TAIL)], axis=1
+    )
+    q_lines = TAIL * query_rows.shape[1] // LANES
+    prev_keys, prev_values = (
+        jnp.concatenate([came[i : i + HD], came[i + HD : i + 2 * HD]], axis=1)[:, 2 * WIN - reach :]
+        for i in (0, 2 * HD)
+    )
+    prev_docs = came[at : at + 2].reshape(2 * LANES)[2 * LANES - reach :].astype(jnp.int32)
+    at = at + TAIL
+    prev_queries = wide(came[at : at + q_lines])
+    prev_residual = wide(came[at + q_lines :])
+    all_keys = jnp.concatenate([prev_keys, key_rows.T], axis=1).T.reshape(rows + reach, kv_local, HD)
+    all_values = jnp.concatenate([prev_values, value_rows.T], axis=1).T
+    all_values = all_values.reshape(rows + reach, kv_local, HD)
+    all_docs = jnp.concatenate([prev_docs, doc_ids])
+    key_pos = offset - reach + jnp.arange(rows + reach, dtype=jnp.int32)
+    query_pos = offset - TAIL + jnp.arange(rows + TAIL, dtype=jnp.int32)
+    queries = jnp.concatenate([prev_queries, query_rows]).reshape(rows + TAIL, kv_local, groups, HD)
+    sink = sink_logit.reshape(kv_local, groups, 1, 1)
+    pieces = attend(
+        queries, all_keys, all_values, query_pos, key_pos, all_docs[WIN:], all_docs, sink
+    )
+    return pieces.reshape(rows + TAIL, heads_local * HD), prev_docs, prev_residual
+
+
+def paired(
+    query_rows,
+    key_rows,
+    value_rows,
+    doc_ids,
+    sink_logit,
+    residual,
+    out_proj,
+    mix_gain,
+    gate_proj,
+    value_proj,
+    gate_taps,
+    value_taps,
+    down_proj,
+    final_gain,
+):
+    rows, width = residual.shape
+    n_tp = lax.axis_size("tp")
+    quarter = rows // n_tp
+    share = width // n_tp
+    sp, tp = lax.axis_index("sp"), lax.axis_index("tp")
+    y, low = sp % 2, (sp // 2) % 2
+    x, core = tp // 2, tp % 2
+    place = jnp.stack([sp, tp]).astype(jnp.int32)
+    one = lambda index: index.astype(jnp.int32)[None]
+    low_at, x_at, core_at = one(low), one(x), one(core)
+
+    docs_rows = doc_ids[rows - 2 * LANES :].astype(jnp.bfloat16).reshape(2, LANES)
+    docs_rows = jnp.pad(docs_rows, ((0, TAIL - 2), (0, 0)))
+    own, other, halo = prepared(
+        low_at, gate_proj, value_proj, query_rows, key_rows, value_rows, docs_rows, residual
+    )
+    came_halo = passed_along(halo, "sp", 1)
+    from_z = [own, swapped(other, 2), swapped(own, 4), swapped(other, 6)]
+    up_weights = []
+    for piece in from_z:
+        up_weights += [piece, swapped(piece, 1)]
+    own, other = row_halves(low_at, down_proj)
+    down_same = [own, swapped(other, 2), swapped(own, 4), swapped(other, 6)]
+    down_far = [swapped(piece, 1) for piece in down_same]
+
+    heads, prev_docs, prev_residual = local_heads(
+        came_halo, query_rows, key_rows, value_rows, doc_ids, sink_logit
+    )
+    docs = jnp.concatenate([prev_docs[-2:], doc_ids])
+    flags = jnp.stack([docs[1:-1] == doc_ids, docs[:-2] == doc_ids]).astype(jnp.float32)
+    flags = lax.dynamic_slice_in_dim(flags, tp * quarter, quarter, 1)
+    flags = jnp.pad(flags, ((0, TAIL - 2), (0, 0)))
+    keep, send = project(place, heads, out_proj, quarter)
+    came = swapped(send, tp_mask=1)
+    keep, send = merge(x_at, keep[:, None], came[:, None], 0, 56)
+    came = swapped(send, tp_mask=2)
+    normed = normed_rows(
+        place, keep[0], came[0], residual, prev_residual, mix_gain[None, :], flags
+    )
+    near = [normed, swapped(normed, tp_mask=2)]
+    near += [swapped(near[0], tp_mask=1), swapped(near[1], tp_mask=1)]
+    normed = swapped(normed, sp_mask=2)
+    far = [normed, swapped(normed, tp_mask=2)]
+    far += [swapped(far[0], tp_mask=1), swapped(far[1], tp_mask=1)]
+
+    cols = gate_proj.shape[1]
+    half = cols // 2
+    main = half // LANES * LANES
+    rest = half - main
+    cut = lambda taps, start, size: lax.dynamic_slice_in_dim(taps, start, size, 1)
+    mains = [cut(t, low * (cols - main), main) for t in (gate_taps, value_taps)]
+    rests = [cut(t, main + low * rest, rest) for t in (gate_taps, value_taps)]
+    mains = jnp.stack([t.reshape(TAPS, main // LANES, LANES) for t in mains], axis=2)
+    taps = jnp.concatenate([mains.reshape(TAPS, 2 * main), *rests], axis=1)
+    taps = jnp.pad(taps, ((0, 8 - TAPS), (0, 0)))
+
+    near, own_normed = up_hidden(place, near, up_weights, taps, share)
+    far, _ = up_hidden(place, far, up_weights, taps, share)
+    terms = down_terms(place, near, far, down_same)
+    ffn_same = reduced(*terms, x_at, False)
+    terms = down_terms(place, near, far, down_far)
+    ffn_far = reduced(*terms, x_at, True)
+    add = lambda pair: pair[0].astype(jnp.float32) + pair[1].astype(jnp.float32)
+    ffn_same, ffn_far = add(ffn_same), add(ffn_far)
+    ffn_own = jnp.where(
+        y == 0,
+        jnp.concatenate([ffn_same, ffn_far], axis=1),
+        jnp.concatenate([ffn_far, ffn_same], axis=1),
+    )
+    second_sum = mix_scale * own_normed.astype(jnp.float32) + ffn_own
+    row_sum, row_squares = lax.psum(
+        (jnp.sum(second_sum, axis=1), jnp.sum(second_sum * second_sum, axis=1)), "tp"
+    )
+    mean = row_sum / width
+    var = row_squares / width - mean * mean
+    return (
+        (second_sum - mean[:, None]) * lax.rsqrt(var + norm_eps)[:, None] * final_gain[None, :]
+    ).astype(jnp.bfloat16)
 
 
 def on_device(
@@ -156,6 +746,11 @@
         P("tp", "sp"),
         P("tp"),
     )
+    fits = mesh.shape["sp"] == 2 * mesh.shape["tp"] and mesh.shape["tp"] == 4
     return jax.shard_map(
-        on_device, mesh=mesh, in_specs=placed, out_specs=P("sp", "tp"), check_vma=False
-    )
+        paired if fits else on_device,
+        mesh=mesh,
+        in_specs=placed,
+        out_specs=P("sp", "tp"),
+        check_vma=False,
+    )

time: 374 us -> 267 us (0.71)
  waiting for transfers between devices: 282 us -> 123 us
  Pallas kernels: 0 us -> 47.3 us
  starting transfers between devices: 17 us -> 53 us
  matrix products: 33.7 us -> 6.9 us
  local copies, waits for them, and re-layouts: 5.23 us -> 20.3 us
  between operations: 15.3 us -> 0.53 us
  other arithmetic: 14.9 us -> 9 us
    all_gather x3 -> x0, waiting for transfers between devices: 202 us -> none  [the longest x1 83.8 us: on_device(): lax.all_gather(down_proj, 'sp', axis=1, tiled=True)]
    ppermute x0 -> x29, waiting for transfers between devices: none -> 121 us  [the longest x17 103 us: swapped(): return lax.ppermute(block, 'sp', [(i, i ^ sp_mask) for i in range(n_sp)])]
    psum x1 -> x0, waiting for transfers between devices: 48.6 us -> none  [on_device(): lax.psum(partial_value.astype(jnp.bfloat16), 'tp').astype(jnp.float32)]
    ppermute x0 -> x29, starting transfers between devices: none -> 48.1 us  [the longest x17 43.2 us: swapped(): return lax.ppermute(block, 'sp', [(i, i ^ sp_mask) for i in range(n_sp)])]
    pallas_call x0 -> x13, Pallas kernels: none -> 47.3 us  [the longest x2 18.5 us: up_hidden(): pl.pallas_call(functools.partial(up_kernel, pieces=len(weights), quarter=...]
    reduce_scatter x1 -> x0, waiting for transfers between devices: 29.5 us -> none  [on_device(): lax.psum_scatter(terms.astype(jnp.bfloat16), 'tp', scatter_dimension=1, t...]
    dot_general x4 -> x0, matrix products: 28 us -> none  [the longest x1 12 us: on_device(): jnp.dot(hidden, lax.all_gather(down_proj, 'sp', axis=1, tiled=True), pref...]
    unnamed x25 -> x79, local copies, waits for them, and re-layouts: 2.77 us -> 17.4 us
  transfers between devices with their start and end apart: 10 -> 30, of which waited for: 5 -> 14; matrix products, arithmetic and copies ran while one was open for 8% -> 1% of each run, Pallas kernels for 0% -> 12%
where the time goes in v1:
time: 267 us; the launch traced here: 266 us
  waiting for transfers between devices  123 us (46%)
  starting transfers between devices  53 us (20%)
  Pallas kernels  47.3 us (18%)
  local copies, waits for them, and re-layouts  20.3 us (8%)
  other arithmetic  9 us (3%)
  matrix products  6.9 us (3%)
  blocking collectives  5.87 us (2%)
    ppermute x17, waiting for transfers between devices, swapped(): return lax.ppermute(block, 'sp', [(i, i ^ sp_mask) for i in range(n_sp)])  103 us
    ppermute x17, starting transfers between devices, swapped(): return lax.ppermute(block, 'sp', [(i, i ^ sp_mask) for i in range(n_sp)])  43.2 us
    pallas_call x2, Pallas kernels, up_hidden(): pl.pallas_call(functools.partial(up_kernel, pieces=len(weights), quarter=...  18.5 us
    ppermute x12, waiting for transfers between devices, swapped(): return lax.ppermute(block, 'tp', [(i, i ^ tp_mask) for i in range(n_tp)])  18.4 us
    unnamed x79, local copies, waits for them, and re-layouts  17.4 us
    pallas_call x5, Pallas kernels, merge(): pl.pallas_call(functools.partial(merge_kernel, axis=axis), in_specs=[pl.B...  7.74 us
    pallas_call x2, Pallas kernels, down_terms(): pl.pallas_call(down_kernel, in_specs=[pl.BlockSpec(memory_space=pltpu.SME...  7.35 us
    psum x1, blocking collectives, paired(): lax.psum((jnp.sum(second_sum, axis=1), jnp.sum(second_sum * second_sum, a...  5.87 us
  transfers between devices with their start and end apart: 30, of which 14 were waited for; matrix products, arithmetic and copies ran while one was open for 1% of the time, Pallas kernels for 12%

profile of v1, /device:TPU:0, one launch (start us, length us, event | category | flops | bytes accessed | tf_op | source)
XLA Modules:
  0.0 266.3 jit_solution(13318971501291573271)
XLA Ops:
  0.0 0.8 convert.3
  1.4 3.4 %prepare.1 = (bf16[256,1408]{1,0:T(8,128)(2,1)}, bf16[256,1408]{1,0:T(8,128)(2,1)}, bf16[424,128]{1,0:T(8,128)(2,1)}) custom-call(s32[1]{0:T(128)} %bitcast.3.which, bf16[256,1408]{1,0:T(8,128)(2,1)} %gates.1, bf16[256,1408]{1,0:T(8,128)(2,1)} %values_in.1, bf16[512,512]{1,0:T(8,128)(2,1)} %queries.1, bf16[64,512]{1,0:T(8,128)(2,1)} %bitcast.69, ...), custom_call_target="tpu_custom_call" | custom-call | tf_op jit(solution)/shard_map/prepare/pallas_call | solution.py:154
  4.8 4.9 %collective-permute-start = (bf16[424,128]{1,0:T(8,128)(2,1)}, bf16[424,128]{1,0:T(8,128)(2,1)S(1)}, u32[]{:S(2)}, u32[]{:S(2)}) collective-permute-start(bf16[424,128]{1,0:T(8,128)(2,1)} %get-tuple-element.29), channel_id=1, source_target_pairs={{0,4},{4,8},{8,12},{12,16},{16,20},{20,24},{24,28},{1,5},{5,9},{9,... | collective-permute-start | bytes 325640 | tf_op jit(solution)/shard_map/ppermute | solution.py:26
  9.8 0.6 pad_add_fusion.2.place
  10.4 1.9 collective-permute-done
  12.5 1.1 pad_maximum_fusion
  14.7 2.7 %fusion.1 = (f32[8,520]{1,0:T(8,128)S(1)}, f32[648,520,8]{0,1,2:T(8,128)S(1)}) fusion(pred[520,648]{1,0:T(8,128)(4,1)S(1)} %fusion.6, bf16[520,8,64]{0,2,1:T(8,128)(2,1)S(1)} %bitcast.64, bf16[64,128]{1,0:T(8,128)(2,1)S(1)} %get-tuple-element.63, bf16[64,128]{1,0:T(8,128)(2,1)S(1)} %get-tuple-element.64, bf16[64,512]{1,0:T(8,128)(2,1)S(1)} %bitcast.70), kind=kOutput, calls=%fused_computation.4 | convolution fusion | flops 353378752 | bytes 11767104 | tf_op jit(solution)/shard_map/qkgd,skd->kgqs/dot_general | solution.py:45
  17.6 3.8 %fusion = f32[8,520]{1,0:T(8,128)S(1)} fusion(f32[648,520,8]{0,1,2:T(8,128)S(1)} %get-tuple-element.71, f32[8,520]{1,0:T(8,128)S(1)} %broadcast_maximum_fusion, pred[520,648]{1,0:T(8,128)(4,1)S(1)} %fusion.6), kind=kLoop, calls=%fused_computation.3 | loop fusion | flops 10778560 | bytes 11152960 | tf_op jit(solution)/shard_map/reduce_sum | solution.py:58
  21.5 4.2 %fusion.7 = bf16[64,8,520]{2,0,1:T(8,128)(2,1)S(1)} fusion(f32[8,520]{1,0:T(8,128)S(1)} %exponential_add_fusion, f32[8,520]{1,0:T(8,128)S(1)} %broadcast_maximum_fusion, f32[648,520,8]{0,1,2:T(8,128)S(1)} %get-tuple-element.71, pred[520,648]{1,0:T(8,128)(4,1)S(1)} %fusion.6, bf16[64,128]{1,0:T(8,128)(2,1)S(1)} %get-tuple-element.65, ...), kind=kOutput, calls=%fused_computation.12 | convolution fusion | flops 359040512 | bytes 11783744 | tf_op jit(solution)/shard_map/kgqs,skd->qkgd/dot_general | solution.py:60
  25.7 1.0 copy.18.heads
  26.7 4.7 %project.1 = (bf16[2,136,2048]{2,1,0:T(8,128)(2,1)}, bf16[2,136,2048]{2,1,0:T(8,128)(2,1)}) custom-call(s32[2]{0:T(128)} %pad_add_fusion.2.place, bf16[520,512]{1,0:T(8,128)(2,1)} %copy.18.heads, bf16[512,2048]{1,0:T(8,128)(2,1)} %weights.1), custom_call_target="tpu_custom_call" | custom-call | tf_op jit(solution)/shard_map/project/pallas_call | solution.py:359
  31.5 2.9 %collective-permute-done.1 = bf16[2,136,2048]{2,1,0:T(8,128)(2,1)S(1)} collective-permute-done((bf16[2,136,2048]{2,1,0:T(8,128)(2,1)}, bf16[2,136,2048]{2,1,0:T(8,128)(2,1)S(1)}, u32[]{:S(2)}, u32[]{:S(2)}) %collective-permute-start.1) | collective-permute-done | bytes 1114144 | tf_op jit(solution)/shard_map/ppermute | solution.py:34
  34.5 1.0 copy-done.23
  35.5 2.5 merge.5
  38.0 1.6 collective-permute-start.2
  39.5 2.0 row_halves.1
  41.5 3.4 %collective-permute-start.17 = (bf16[704,256]{1,0:T(8,128)(2,1)}, bf16[704,256]{1,0:T(8,128)(2,1)}, u32[]{:S(2)}, u32[]{:S(2)}) collective-permute-start(bf16[704,256]{1,0:T(8,128)(2,1)} %get-tuple-element.40), channel_id=1, source_target_pairs={{0,8},{4,12},{8,0},{12,4},{16,24},{20,28},{24,16},{28,20},{1,9},{5... | collective-permute-start | bytes 1081352 | tf_op jit(solution)/shard_map/ppermute | solution.py:32
  44.9 2.6 collective-permute-start.18
  47.8 2.5 collective-permute-start.11
  50.3 11.0 %collective-permute-done.17.refs_1_ = bf16[704,256]{1,0:T(8,128)(2,1)} collective-permute-done((bf16[704,256]{1,0:T(8,128)(2,1)}, bf16[704,256]{1,0:T(8,128)(2,1)}, u32[]{:S(2)}, u32[]{:S(2)}) %collective-permute-start.17) | collective-permute-done | bytes 360480 | tf_op jit(solution)/shard_map/ppermute | solution.py:32
  61.3 34.7 %collective-permute-done.18.refs_2_ = bf16[704,256]{1,0:T(8,128)(2,1)} collective-permute-done((bf16[704,256]{1,0:T(8,128)(2,1)}, bf16[704,256]{1,0:T(8,128)(2,1)}, u32[]{:S(2)}, u32[]{:S(2)}) %collective-permute-start.18) | collective-permute-done | bytes 360480 | tf_op jit(solution)/shard_map/ppermute | solution.py:32
  96.0 2.6 collective-permute-start.19
  100.0 3.6 %normed_rows.1.refs_0_ = bf16[136,2048]{1,0:T(8,128)(2,1)} custom-call(s32[2]{0:T(128)} %pad_add_fusion.2.place, bf16[136,2048]{1,0:T(8,128)(2,1)} %bitcast.68, bf16[136,2048]{1,0:T(8,128)(2,1)} %bitcast.20.second, bf16[512,2048]{1,0:T(8,128)(2,1)} %residual.3, bf16[8,2048]{1,0:T(8,128)(2,1)} %copy-done.26, f32[1,2048]{1,0:T(1,128)} %bitcast.73, ...), custom_call_target="tpu_custom_call" | custom-call | tf_op jit(solution)/shard_map/normed_rows/pallas_call | solution.py:455
  103.7 14.1 %collective-permute-done.19.refs_3_ = bf16[704,256]{1,0:T(8,128)(2,1)} collective-permute-done((bf16[704,256]{1,0:T(8,128)(2,1)}, bf16[704,256]{1,0:T(8,128)(2,1)}, u32[]{:S(2)}, u32[]{:S(2)}) %collective-permute-start.19) | collective-permute-done | bytes 360480 | tf_op jit(solution)/shard_map/ppermute | solution.py:32
  117.7 23.8 %collective-permute-start.13 = (bf16[136,2048]{1,0:T(8,128)(2,1)}, bf16[136,2048]{1,0:T(8,128)(2,1)S(1)}, u32[]{:S(2)}, u32[]{:S(2)}) collective-permute-start(bf16[136,2048]{1,0:T(8,128)(2,1)} %normed_rows.1.refs_0_), channel_id=1, source_target_pairs={{0,8},{4,12},{8,0},{12,4},{16,24},{20,28},{24,16},{28,20},{1,9},{5... | collective-permute-start | bytes 1671176 | tf_op jit(solution)/shard_map/ppermute | solution.py:32
  141.5 0.6 collective-permute-start.10
  142.2 1.4 collective-permute-start.12
  144.1 9.2 %collective-permute-done.13.refs_0_ = bf16[136,2048]{1,0:T(8,128)(2,1)S(1)} collective-permute-done((bf16[136,2048]{1,0:T(8,128)(2,1)}, bf16[136,2048]{1,0:T(8,128)(2,1)S(1)}, u32[]{:S(2)}, u32[]{:S(2)}) %collective-permute-start.13) | collective-permute-done | bytes 557088 | tf_op jit(solution)/shard_map/ppermute | solution.py:32
  153.9 0.9 copy-done.1
  155.3 5.2 %collective-permute-done.10.refs_9_ = bf16[256,1408]{1,0:T(8,128)(2,1)S(1)} collective-permute-done((bf16[256,1408]{1,0:T(8,128)(2,1)S(1)}, bf16[256,1408]{1,0:T(8,128)(2,1)S(1)}, u32[]{:S(2)}, u32[]{:S(2)}) %collective-permute-start.10) | collective-permute-done | bytes 720928 | tf_op jit(solution)/shard_map/ppermute | solution.py:32
  160.6 0.9 copy-done.3
  161.5 14.5 %collective-permute-done.12.refs_11_ = bf16[256,1408]{1,0:T(8,128)(2,1)S(1)} collective-permute-done((bf16[256,1408]{1,0:T(8,128)(2,1)S(1)}, bf16[256,1408]{1,0:T(8,128)(2,1)S(1)}, u32[]{:S(2)}, u32[]{:S(2)}) %collective-permute-start.12) | collective-permute-done | bytes 720928 | tf_op jit(solution)/shard_map/ppermute | solution.py:32
  176.0 0.9 copy-done.6
  176.9 0.8 copy-done.11
  178.2 0.8 copy-done.13
  179.0 9.9 %collective-permute-done.8.refs_7_ = bf16[256,1408]{1,0:T(8,128)(2,1)S(1)} collective-permute-done((bf16[256,1408]{1,0:T(8,128)(2,1)S(1)}, bf16[256,1408]{1,0:T(8,128)(2,1)S(1)}, u32[]{:S(2)}, u32[]{:S(2)}) %collective-permute-start.8) | collective-permute-done | bytes 720928 | tf_op jit(solution)/shard_map/ppermute | solution.py:32
  189.0 0.9 copy-done.8
  189.8 0.6 collective-permute-start.23
  190.5 0.8 copy-done.17
  191.3 1.4 collective-permute-start.24
  192.7 0.8 copy-done.15
  193.5 0.6 collective-permute-start.25
  194.1 0.9 copy-done.19
  195.0 1.4 collective-permute-start.26
  196.7 1.1 copy-done.2
  197.8 1.1 copy-done.4
  198.9 1.1 copy-done.7
  200.0 1.1 copy-done.9
  201.1 1.1 copy-done.10
  202.2 1.1 copy-done.14
  203.2 1.1 copy-done.18
  204.3 1.1 copy-done.20
  205.3 8.8 %up_hidden.2 = (bf16[512,704]{1,0:T(8,128)(2,1)S(1)}, bf16[512,512]{1,0:T(8,128)(2,1)S(1)}) custom-call(s32[2]{0:T(128)S(1)} %copy-done.22, bf16[136,2048]{1,0:T(8,128)(2,1)S(1)} %copy-done.10, bf16[136,2048]{1,0:T(8,128)(2,1)S(1)} %copy-done.14, bf16[136,2048]{1,0:T(8,128)(2,1)S(1)} %copy-done.18, bf16[136,2048]{1,0:T(8,128)(2,1)S(1)} %copy-done.20, ...), custom_call_target="tpu_custom_call" | custom-call | tf_op jit(solution)/shard_map/up_hidden/pallas_call | solution.py:301
  214.2 9.7 %up_hidden.3 = (bf16[512,704]{1,0:T(8,128)(2,1)S(1)}, bf16[512,512]{1,0:T(8,128)(2,1)}) custom-call(s32[2]{0:T(128)S(1)} %copy-done.22, bf16[136,2048]{1,0:T(8,128)(2,1)S(1)} %copy-done.12, bf16[136,2048]{1,0:T(8,128)(2,1)} %collective-permute-done.14.refs_1_, bf16[136,2048]{1,0:T(8,128)(2,1)S(1)} %copy-done.16, ...), custom_call_target="tpu_custom_call" | custom-call | tf_op jit(solution)/shard_map/up_hidden/pallas_call | solution.py:301
  223.9 3.7 %down_terms.3 = (bf16[2,2,512,256]{3,2,1,0:T(8,128)(2,1)S(1)}, bf16[2,2,512,256]{3,2,1,0:T(8,128)(2,1)S(1)}) custom-call(s32[2]{0:T(128)S(1)} %copy-done.22, bf16[512,704]{1,0:T(8,128)(2,1)S(1)} %get-tuple-element.37.near, bf16[512,704]{1,0:T(8,128)(2,1)S(1)} %get-tuple-element.38.far, bf16[704,256]{1,0:T(8,128)(2,1)} %collective-permute-done.23.refs_0_, ...), custom_call_target="tpu_custom_call" | custom-call | tf_op jit(solution)/shard_map/down_terms/pallas_call | solution.py:492
  227.7 3.6 %down_terms.2 = (bf16[2,2,512,256]{3,2,1,0:T(8,128)(2,1)S(1)}, bf16[2,2,512,256]{3,2,1,0:T(8,128)(2,1)S(1)}) custom-call(s32[2]{0:T(128)S(1)} %copy-done.22, bf16[512,704]{1,0:T(8,128)(2,1)S(1)} %get-tuple-element.37.near, bf16[512,704]{1,0:T(8,128)(2,1)S(1)} %get-tuple-element.38.far, bf16[704,256]{1,0:T(8,128)(2,1)S(1)} %copy-done.21, ...), custom_call_target="tpu_custom_call" | custom-call | tf_op jit(solution)/shard_map/down_terms/pallas_call | solution.py:492
  233.0 1.3 collective-permute-done.20.second
  235.0 11.3 %collective-permute-done.28 = bf16[2,512,256]{2,1,0:T(8,128)(2,1)S(1)} collective-permute-done((bf16[2,512,256]{2,1,0:T(8,128)(2,1)S(1)}, bf16[2,512,256]{2,1,0:T(8,128)(2,1)S(1)}, u32[]{:S(2)}, u32[]{:S(2)}) %collective-permute-start.28) | collective-permute-done | bytes 524320 | tf_op jit(solution)/shard_map/ppermute | solution.py:34
  246.3 2.2 merge.9
  248.9 2.2 merge.7
  251.7 4.3 %collective-permute-done.29 = bf16[2,256,256]{2,1,0:T(8,128)(2,1)S(1)} collective-permute-done((bf16[2,256,256]{2,1,0:T(8,128)(2,1)S(1)}, bf16[2,256,256]{2,1,0:T(8,128)(2,1)S(1)}, u32[]{:S(2)}, u32[]{:S(2)}) %collective-permute-start.29) | collective-permute-done | bytes 262176 | tf_op jit(solution)/shard_map/ppermute | solution.py:32
  256.0 2.9 %collective-permute-done.22 = bf16[2,256,256]{2,1,0:T(8,128)(2,1)S(1)} collective-permute-done((bf16[2,256,256]{2,1,0:T(8,128)(2,1)S(1)}, bf16[2,256,256]{2,1,0:T(8,128)(2,1)S(1)}, u32[]{:S(2)}, u32[]{:S(2)}) %collective-permute-start.22) | collective-permute-done | bytes 262176 | tf_op jit(solution)/shard_map/ppermute | solution.py:34
  259.3 5.9 %all-reduce.3 = (f32[512]{0:T(512)S(1)}, f32[512]{0:T(512)S(1)}) all-reduce(f32[512]{0:T(512)S(1)} %get-tuple-element.54, f32[512]{0:T(512)S(1)} %get-tuple-element.53), channel_id=1, replica_groups=mesh['sp'=8,'tp'=4] {'tp'}, use_global_device_ids=true, to_apply=%region_5.6 | all-reduce | flops 1024 | bytes 8192 | tf_op jit(solution)/shard_map/psum | solution.py:638
  265.2 1.1 multiply_convert_fusion
  (131 shorter events, 10.4 us)
Async XLA Ops:
  0.0 14.0 %copy-start.27 = (s32[512]{0:T(512)S(1)}, s32[512]{0:T(512)}, u32[]{:S(2)}) copy-start(s32[512]{0:T(512)} %param.17) | copy-start | bytes 6148
  0.0 14.7 %copy-start.24 = (bf16[512,64]{0,1:T(8,128)(2,1)S(1)}, bf16[512,64]{0,1:T(8,128)(2,1)}, u32[]{:S(2)}) copy-start(bf16[512,64]{0,1:T(8,128)(2,1)} %param.15) | copy-start | bytes 196612
  4.8 7.5 %collective-permute-start = (bf16[424,128]{1,0:T(8,128)(2,1)}, bf16[424,128]{1,0:T(8,128)(2,1)S(1)}, u32[]{:S(2)}, u32[]{:S(2)}) collective-permute-start(bf16[424,128]{1,0:T(8,128)(2,1)} %get-tuple-element.29), channel_id=1, source_target_pairs={{0,4},{4,8},{8,12},{12,16},{16,20},{20,24},{24,28},{1,5},{5,9},{9,... | collective-permute-start | bytes 325640 | tf_op jit(solution)/shard_map/ppermute | solution.py:26
  12.5 5.0 %copy-start.26 = (bf16[8,2048]{1,0:T(8,128)(2,1)}, bf16[8,2048]{1,0:T(8,128)(2,1)S(1)}, u32[]{:S(2)}) copy-start(bf16[8,2048]{1,0:T(8,128)(2,1)S(1)} %get-tuple-element.57.before) | copy-start | bytes 98308
  14.7 2.7 %copy-start.30 = (f32[8]{0:T(128)S(1)}, f32[8]{0:T(128)}, u32[]{:S(2)}) copy-start(f32[8]{0:T(128)} %param.18) | copy-start | bytes 100
  17.6 3.9 %copy-start.25 = (bf16[512,64]{0,1:T(8,128)(2,1)S(1)}, bf16[512,64]{0,1:T(8,128)(2,1)}, u32[]{:S(2)}) copy-start(bf16[512,64]{0,1:T(8,128)(2,1)} %param.16) | copy-start | bytes 196612
  25.6 21.8 %copy-start = (bf16[256,1408]{1,0:T(8,128)(2,1)S(1)}, bf16[256,1408]{1,0:T(8,128)(2,1)}, u32[]{:S(2)}) copy-start(bf16[256,1408]{1,0:T(8,128)(2,1)} %get-tuple-element.34.refs_4_) | copy-start | bytes 2162692
  25.6 170.7 %copy-start.28 = (f32[3,1408]{1,0:T(4,128)S(1)}, f32[3,1408]{1,0:T(4,128)}, u32[]{:S(2)}) copy-start(f32[3,1408]{1,0:T(4,128)} %param.25) | copy-start | bytes 50692
  25.7 170.7 %copy-start.29 = (f32[3,1408]{1,0:T(4,128)S(1)}, f32[3,1408]{1,0:T(4,128)}, u32[]{:S(2)}) copy-start(f32[3,1408]{1,0:T(4,128)} %param.24) | copy-start | bytes 50692
  25.7 171.0 %copy-start.22 = (s32[2]{0:T(128)S(1)}, s32[2]{0:T(128)}, u32[]{:S(2)}) copy-start(s32[2]{0:T(128)} %pad_add_fusion.2.place) | copy-start | bytes 28
  31.4 3.0 %collective-permute-start.1 = (bf16[2,136,2048]{2,1,0:T(8,128)(2,1)}, bf16[2,136,2048]{2,1,0:T(8,128)(2,1)S(1)}, u32[]{:S(2)}, u32[]{:S(2)}) collective-permute-start(bf16[2,136,2048]{2,1,0:T(8,128)(2,1)} %get-tuple-element.31), channel_id=1, source_target_pairs={{0,1},{1,0},{2,3},{3,2},{4,5},{5,4},{6,7},{7,6},{8,9},{9,8},{10,11... | collective-permute-start | bytes 3342344 | tf_op jit(solution)/shard_map/ppermute | solution.py:34
  34.5 1.0 copy-start.23
  38.0 60.7 %collective-permute-start.2 = (bf16[1,136,2048]{2,1,0:T(8,128)(2,1)}, bf16[1,136,2048]{2,1,0:T(8,128)(2,1)}, u32[]{:S(2)}, u32[]{:S(2)}) collective-permute-start(bf16[1,136,2048]{2,1,0:T(8,128)(2,1)} %get-tuple-element.33), channel_id=1, source_target_pairs={{0,2},{1,3},{2,0},{3,1},{4,6},{5,7},{6,4},{7,5},{8,10},{9,11},{10,... | collective-permute-start | bytes 1671176 | tf_op jit(solution)/shard_map/ppermute | solution.py:34
  41.5 19.7 %collective-permute-start.17 = (bf16[704,256]{1,0:T(8,128)(2,1)}, bf16[704,256]{1,0:T(8,128)(2,1)}, u32[]{:S(2)}, u32[]{:S(2)}) collective-permute-start(bf16[704,256]{1,0:T(8,128)(2,1)} %get-tuple-element.40), channel_id=1, source_target_pairs={{0,8},{4,12},{8,0},{12,4},{16,24},{20,28},{24,16},{28,20},{1,9},{5... | collective-permute-start | bytes 1081352 | tf_op jit(solution)/shard_map/ppermute | solution.py:32
  44.9 51.1 %collective-permute-start.18 = (bf16[704,256]{1,0:T(8,128)(2,1)}, bf16[704,256]{1,0:T(8,128)(2,1)}, u32[]{:S(2)}, u32[]{:S(2)}) collective-permute-start(bf16[704,256]{1,0:T(8,128)(2,1)} %get-tuple-element.39.refs_0_), channel_id=1, source_target_pairs={{0,16},{4,20},{8,24},{12,28},{16,0},{20,4},{24,8},{28,12},{1,17},{... | collective-permute-start | bytes 1081352 | tf_op jit(solution)/shard_map/ppermute | solution.py:32
  47.5 94.1 %collective-permute-start.9 = (bf16[256,1408]{1,0:T(8,128)(2,1)S(1)}, bf16[256,1408]{1,0:T(8,128)(2,1)S(1)}, u32[]{:S(2)}, u32[]{:S(2)}) collective-permute-start(bf16[256,1408]{1,0:T(8,128)(2,1)S(1)} %copy-done), channel_id=1, source_target_pairs={{0,16},{4,20},{8,24},{12,28},{16,0},{20,4},{24,8},{28,12},{1,17},{... | collective-permute-start | bytes 2162696 | tf_op jit(solution)/shard_map/ppermute | solution.py:32
  47.8 94.4 %collective-permute-start.11 = (bf16[256,1408]{1,0:T(8,128)(2,1)}, bf16[256,1408]{1,0:T(8,128)(2,1)S(1)}, u32[]{:S(2)}, u32[]{:S(2)}) collective-permute-start(bf16[256,1408]{1,0:T(8,128)(2,1)} %get-tuple-element.35), channel_id=1, source_target_pairs={{0,24},{4,28},{8,16},{12,20},{16,8},{20,12},{24,0},{28,4},{1,25},{... | collective-permute-start | bytes 2162696 | tf_op jit(solution)/shard_map/ppermute | solution.py:32
  61.2 82.4 %collective-permute-start.7 = (bf16[256,1408]{1,0:T(8,128)(2,1)}, bf16[256,1408]{1,0:T(8,128)(2,1)S(1)}, u32[]{:S(2)}, u32[]{:S(2)}) collective-permute-start(bf16[256,1408]{1,0:T(8,128)(2,1)} %get-tuple-element.35), channel_id=1, source_target_pairs={{0,8},{4,12},{8,0},{12,4},{16,24},{20,28},{24,16},{28,20},{1,9},{5... | collective-permute-start | bytes 2162696 | tf_op jit(solution)/shard_map/ppermute | solution.py:32
  96.0 21.8 %collective-permute-start.19 = (bf16[704,256]{1,0:T(8,128)(2,1)}, bf16[704,256]{1,0:T(8,128)(2,1)}, u32[]{:S(2)}, u32[]{:S(2)}) collective-permute-start(bf16[704,256]{1,0:T(8,128)(2,1)} %get-tuple-element.40), channel_id=1, source_target_pairs={{0,24},{4,28},{8,16},{12,20},{16,8},{20,12},{24,0},{28,4},{1,25},{... | collective-permute-start | bytes 1081352 | tf_op jit(solution)/shard_map/ppermute | solution.py:32
  98.6 55.2 %collective-permute-start.6 = (bf16[256,1408]{1,0:T(8,128)(2,1)S(1)}, bf16[256,1408]{1,0:T(8,128)(2,1)S(1)}, u32[]{:S(2)}, u32[]{:S(2)}) collective-permute-start(bf16[256,1408]{1,0:T(8,128)(2,1)S(1)} %copy-done), channel_id=1, source_target_pairs={{0,4},{4,0},{8,12},{12,8},{16,20},{20,16},{24,28},{28,24},{1,5},{5... | collective-permute-start | bytes 2162696 | tf_op jit(solution)/shard_map/ppermute | solution.py:32
  117.7 35.6 %collective-permute-start.13 = (bf16[136,2048]{1,0:T(8,128)(2,1)}, bf16[136,2048]{1,0:T(8,128)(2,1)S(1)}, u32[]{:S(2)}, u32[]{:S(2)}) collective-permute-start(bf16[136,2048]{1,0:T(8,128)(2,1)} %normed_rows.1.refs_0_), channel_id=1, source_target_pairs={{0,8},{4,12},{8,0},{12,4},{16,24},{20,28},{24,16},{28,20},{1,9},{5... | collective-permute-start | bytes 1671176 | tf_op jit(solution)/shard_map/ppermute | solution.py:32
  141.5 19.0 %collective-permute-start.10 = (bf16[256,1408]{1,0:T(8,128)(2,1)S(1)}, bf16[256,1408]{1,0:T(8,128)(2,1)S(1)}, u32[]{:S(2)}, u32[]{:S(2)}) collective-permute-start(bf16[256,1408]{1,0:T(8,128)(2,1)S(1)} %collective-permute-done.9.refs_8_), channel_id=1, source_target_pairs={{0,4},{4,0},{8,12},{12,8},{16,20},{20,16},{24,28},{28,24},{1,5},{5... | collective-permute-start | bytes 2162696 | tf_op jit(solution)/shard_map/ppermute | solution.py:32
  142.2 33.8 %collective-permute-start.12 = (bf16[256,1408]{1,0:T(8,128)(2,1)S(1)}, bf16[256,1408]{1,0:T(8,128)(2,1)S(1)}, u32[]{:S(2)}, u32[]{:S(2)}) collective-permute-start(bf16[256,1408]{1,0:T(8,128)(2,1)S(1)} %collective-permute-done.11.refs_10_), channel_id=1, source_target_pairs={{0,4},{4,0},{8,12},{12,8},{16,20},{20,16},{24,28},{28,24},{1,5},{5... | collective-permute-start | bytes 2162696 | tf_op jit(solution)/shard_map/ppermute | solution.py:32
  143.6 34.1 %collective-permute-start.3 = (bf16[136,2048]{1,0:T(8,128)(2,1)}, bf16[136,2048]{1,0:T(8,128)(2,1)S(1)}, u32[]{:S(2)}, u32[]{:S(2)}) collective-permute-start(bf16[136,2048]{1,0:T(8,128)(2,1)} %normed_rows.1.refs_0_), channel_id=1, source_target_pairs={{0,2},{1,3},{2,0},{3,1},{4,6},{5,7},{6,4},{7,5},{8,10},{9,11},{10,... | collective-permute-start | bytes 1671176 | tf_op jit(solution)/shard_map/ppermute | solution.py:34
  153.3 25.7 %collective-permute-start.14 = (bf16[136,2048]{1,0:T(8,128)(2,1)S(1)}, bf16[136,2048]{1,0:T(8,128)(2,1)}, u32[]{:S(2)}, u32[]{:S(2)}) collective-permute-start(bf16[136,2048]{1,0:T(8,128)(2,1)S(1)} %collective-permute-done.13.refs_0_), channel_id=1, source_target_pairs={{0,2},{1,3},{2,0},{3,1},{4,6},{5,7},{6,4},{7,5},{8,10},{9,11},{10,... | collective-permute-start | bytes 1671176 | tf_op jit(solution)/shard_map/ppermute | solution.py:34
  153.8 0.9 copy-start.1
  154.7 34.3 %collective-permute-start.8 = (bf16[256,1408]{1,0:T(8,128)(2,1)S(1)}, bf16[256,1408]{1,0:T(8,128)(2,1)S(1)}, u32[]{:S(2)}, u32[]{:S(2)}) collective-permute-start(bf16[256,1408]{1,0:T(8,128)(2,1)S(1)} %collective-permute-done.7.refs_6_), channel_id=1, source_target_pairs={{0,4},{4,0},{8,12},{12,8},{16,20},{20,16},{24,28},{28,24},{1,5},{5... | collective-permute-start | bytes 2162696 | tf_op jit(solution)/shard_map/ppermute | solution.py:32
  160.6 0.9 copy-start.3
  161.5 29.0 %collective-permute-start.4 = (bf16[136,2048]{1,0:T(8,128)(2,1)}, bf16[136,2048]{1,0:T(8,128)(2,1)S(1)}, u32[]{:S(2)}, u32[]{:S(2)}) collective-permute-start(bf16[136,2048]{1,0:T(8,128)(2,1)} %normed_rows.1.refs_0_), channel_id=1, source_target_pairs={{0,1},{1,0},{2,3},{3,2},{4,5},{5,4},{6,7},{7,6},{8,9},{9,8},{10,11... | collective-permute-start | bytes 1671176 | tf_op jit(solution)/shard_map/ppermute | solution.py:34
  176.0 0.9 copy-start.6
  176.9 15.8 %collective-permute-start.15 = (bf16[136,2048]{1,0:T(8,128)(2,1)S(1)}, bf16[136,2048]{1,0:T(8,128)(2,1)S(1)}, u32[]{:S(2)}, u32[]{:S(2)}) collective-permute-start(bf16[136,2048]{1,0:T(8,128)(2,1)S(1)} %collective-permute-done.13.refs_0_), channel_id=1, source_target_pairs={{0,1},{1,0},{2,3},{3,2},{4,5},{5,4},{6,7},{7,6},{8,9},{9,8},{10,11... | collective-permute-start | bytes 1671176 | tf_op jit(solution)/shard_map/ppermute | solution.py:34
  176.9 0.8 copy-start.11
  177.7 16.4 %collective-permute-start.5 = (bf16[136,2048]{1,0:T(8,128)(2,1)S(1)}, bf16[136,2048]{1,0:T(8,128)(2,1)S(1)}, u32[]{:S(2)}, u32[]{:S(2)}) collective-permute-start(bf16[136,2048]{1,0:T(8,128)(2,1)S(1)} %collective-permute-done.3.refs_1_), channel_id=1, source_target_pairs={{0,1},{1,0},{2,3},{3,2},{4,5},{5,4},{6,7},{7,6},{8,9},{9,8},{10,11... | collective-permute-start | bytes 1671176 | tf_op jit(solution)/shard_map/ppermute | solution.py:34
  178.2 0.8 copy-start.13
  179.0 35.1 %collective-permute-start.16 = (bf16[136,2048]{1,0:T(8,128)(2,1)}, bf16[136,2048]{1,0:T(8,128)(2,1)}, u32[]{:S(2)}, u32[]{:S(2)}) collective-permute-start(bf16[136,2048]{1,0:T(8,128)(2,1)} %collective-permute-done.14.refs_1_), channel_id=1, source_target_pairs={{0,1},{1,0},{2,3},{3,2},{4,5},{5,4},{6,7},{7,6},{8,9},{9,8},{10,11... | collective-permute-start | bytes 1671176 | tf_op jit(solution)/shard_map/ppermute | solution.py:34
  189.0 0.9 copy-start.8
  189.8 34.0 %collective-permute-start.23 = (bf16[704,256]{1,0:T(8,128)(2,1)}, bf16[704,256]{1,0:T(8,128)(2,1)}, u32[]{:S(2)}, u32[]{:S(2)}) collective-permute-start(bf16[704,256]{1,0:T(8,128)(2,1)} %get-tuple-element.39.refs_0_), channel_id=1, source_target_pairs={{0,4},{4,0},{8,12},{12,8},{16,20},{20,16},{24,28},{28,24},{1,5},{5... | collective-permute-start | bytes 1081352 | tf_op jit(solution)/shard_map/ppermute | solution.py:32
  190.5 0.8 copy-start.17
  191.3 32.6 %collective-permute-start.24 = (bf16[704,256]{1,0:T(8,128)(2,1)}, bf16[704,256]{1,0:T(8,128)(2,1)}, u32[]{:S(2)}, u32[]{:S(2)}) collective-permute-start(bf16[704,256]{1,0:T(8,128)(2,1)} %collective-permute-done.17.refs_1_), channel_id=1, source_target_pairs={{0,4},{4,0},{8,12},{12,8},{16,20},{20,16},{24,28},{28,24},{1,5},{5... | collective-permute-start | bytes 1081352 | tf_op jit(solution)/shard_map/ppermute | solution.py:32
  192.7 0.8 copy-start.15
  193.5 30.4 %collective-permute-start.25 = (bf16[704,256]{1,0:T(8,128)(2,1)}, bf16[704,256]{1,0:T(8,128)(2,1)}, u32[]{:S(2)}, u32[]{:S(2)}) collective-permute-start(bf16[704,256]{1,0:T(8,128)(2,1)} %collective-permute-done.18.refs_2_), channel_id=1, source_target_pairs={{0,4},{4,0},{8,12},{12,8},{16,20},{20,16},{24,28},{28,24},{1,5},{5... | collective-permute-start | bytes 1081352 | tf_op jit(solution)/shard_map/ppermute | solution.py:32
  194.1 0.9 copy-start.19
  195.0 28.9 %collective-permute-start.26 = (bf16[704,256]{1,0:T(8,128)(2,1)}, bf16[704,256]{1,0:T(8,128)(2,1)}, u32[]{:S(2)}, u32[]{:S(2)}) collective-permute-start(bf16[704,256]{1,0:T(8,128)(2,1)} %collective-permute-done.19.refs_3_), channel_id=1, source_target_pairs={{0,4},{4,0},{8,12},{12,8},{16,20},{20,16},{24,28},{28,24},{1,5},{5... | collective-permute-start | bytes 1081352 | tf_op jit(solution)/shard_map/ppermute | solution.py:32
  196.7 1.1 copy-start.2
  197.8 1.1 copy-start.4
  198.9 1.1 copy-start.7
  200.0 1.1 copy-start.9
  201.1 1.1 copy-start.10
  202.2 1.1 copy-start.14
  203.2 1.1 copy-start.18
  204.3 1.1 copy-start.20
  205.3 8.8 %copy-start.5 = (bf16[256,1408]{1,0:T(8,128)(2,1)S(1)}, bf16[256,1408]{1,0:T(8,128)(2,1)}, u32[]{:S(2)}) copy-start(bf16[256,1408]{1,0:T(8,128)(2,1)} %copy-done.3) | copy-start | bytes 2162692
  205.3 8.8 %copy-start.12 = (bf16[136,2048]{1,0:T(8,128)(2,1)S(1)}, bf16[136,2048]{1,0:T(8,128)(2,1)}, u32[]{:S(2)}) copy-start(bf16[136,2048]{1,0:T(8,128)(2,1)} %copy-done.11) | copy-start | bytes 1671172
  205.3 8.8 %copy-start.16 = (bf16[136,2048]{1,0:T(8,128)(2,1)S(1)}, bf16[136,2048]{1,0:T(8,128)(2,1)}, u32[]{:S(2)}) copy-start(bf16[136,2048]{1,0:T(8,128)(2,1)} %copy-done.15) | copy-start | bytes 1671172
  214.1 13.6 %copy-start.21 = (bf16[704,256]{1,0:T(8,128)(2,1)S(1)}, bf16[704,256]{1,0:T(8,128)(2,1)}, u32[]{:S(2)}) copy-start(bf16[704,256]{1,0:T(8,128)(2,1)} %get-tuple-element.39.refs_0_) | copy-start | bytes 1081348
  227.6 37.6 %copy-start.31 = (f32[512]{0:T(512)S(1)}, f32[512]{0:T(512)}, u32[]{:S(2)}) copy-start(f32[512]{0:T(512)} %param.27) | copy-start | bytes 6148
  227.6 4.3 %collective-permute-start.27 = (bf16[2,2,512,256]{3,2,1,0:T(8,128)(2,1)S(1)}, bf16[2,2,512,256]{3,2,1,0:T(8,128)(2,1)S(1)}, u32[]{:S(2)}, u32[]{:S(2)}) collective-permute-start(bf16[2,2,512,256]{3,2,1,0:T(8,128)(2,1)S(1)} %get-tuple-element.48), channel_id=1, source_target_pairs={{0,1},{1,0},{2,3},{3,2},{4,5},{5,4},{6,7},{7,6},{8,9},{9,8},{10,11... | collective-permute-start | bytes 3145736 | tf_op jit(solution)/shard_map/ppermute | solution.py:34
  231.4 2.8 %collective-permute-start.20 = (bf16[2,2,512,256]{3,2,1,0:T(8,128)(2,1)S(1)}, bf16[2,2,512,256]{3,2,1,0:T(8,128)(2,1)S(1)}, u32[]{:S(2)}, u32[]{:S(2)}) collective-permute-start(bf16[2,2,512,256]{3,2,1,0:T(8,128)(2,1)S(1)} %get-tuple-element.42), channel_id=1, source_target_pairs={{0,1},{1,0},{2,3},{3,2},{4,5},{5,4},{6,7},{7,6},{8,9},{9,8},{10,11... | collective-permute-start | bytes 3145736 | tf_op jit(solution)/shard_map/ppermute | solution.py:34
  232.4 13.9 %collective-permute-start.28 = (bf16[2,512,256]{2,1,0:T(8,128)(2,1)S(1)}, bf16[2,512,256]{2,1,0:T(8,128)(2,1)S(1)}, u32[]{:S(2)}, u32[]{:S(2)}) collective-permute-start(bf16[2,512,256]{2,1,0:T(8,128)(2,1)S(1)} %get-tuple-element.50), channel_id=1, source_target_pairs={{0,2},{1,3},{2,0},{3,1},{4,6},{5,7},{6,4},{7,5},{8,10},{9,11},{10,... | collective-permute-start | bytes 1572872 | tf_op jit(solution)/shard_map/ppermute | solution.py:34
  234.7 14.3 %collective-permute-start.21 = (bf16[2,512,256]{2,1,0:T(8,128)(2,1)S(1)}, bf16[2,512,256]{2,1,0:T(8,128)(2,1)S(1)}, u32[]{:S(2)}, u32[]{:S(2)}) collective-permute-start(bf16[2,512,256]{2,1,0:T(8,128)(2,1)S(1)} %get-tuple-element.44), channel_id=1, source_target_pairs={{0,8},{4,12},{8,0},{12,4},{16,24},{20,28},{24,16},{28,20},{1,9},{5... | collective-permute-start | bytes 1572872 | tf_op jit(solution)/shard_map/ppermute | solution.py:32
  248.5 7.4 %collective-permute-start.29 = (bf16[2,256,256]{2,1,0:T(8,128)(2,1)S(1)}, bf16[2,256,256]{2,1,0:T(8,128)(2,1)S(1)}, u32[]{:S(2)}, u32[]{:S(2)}) collective-permute-start(bf16[2,256,256]{2,1,0:T(8,128)(2,1)S(1)} %get-tuple-element.52), channel_id=1, source_target_pairs={{0,8},{4,12},{8,0},{12,4},{16,24},{20,28},{24,16},{28,20},{1,9},{5... | collective-permute-start | bytes 786440 | tf_op jit(solution)/shard_map/ppermute | solution.py:32
  251.1 7.8 %collective-permute-start.22 = (bf16[2,256,256]{2,1,0:T(8,128)(2,1)S(1)}, bf16[2,256,256]{2,1,0:T(8,128)(2,1)S(1)}, u32[]{:S(2)}, u32[]{:S(2)}) collective-permute-start(bf16[2,256,256]{2,1,0:T(8,128)(2,1)S(1)} %get-tuple-element.46), channel_id=1, source_target_pairs={{0,2},{1,3},{2,0},{3,1},{4,6},{5,7},{6,4},{7,5},{8,10},{9,11},{10,... | collective-permute-start | bytes 786440 | tf_op jit(solution)/shard_map/ppermute | solution.py:34

commit v2 on v1

--- a/solution.py
+++ b/solution.py
@@ -14,6 +14,7 @@
 TAPS = 3
 LANES = 128
 TAIL = 8
+RS_ROOM = 56
 
 
 mix_scale = math.sqrt(2.0)
@@ -111,7 +112,9 @@
     for copy in copies:
         copy.wait()
     at = 0
-    for src in (k, v, docs, q, r):
+    last = docs[docs.shape[0] - 2 :, :].astype(jnp.float32)
+    last = jnp.concatenate([last, jnp.zeros((TAIL - 2, LANES), jnp.float32)])
+    for src in (k, v, last.astype(halo.dtype), q, r):
         for n in range(0, src.shape[1], LANES):
             halo[at : at + src.shape[0], :] = src[:, n : n + LANES]
             at += src.shape[0]
@@ -205,43 +208,49 @@
 
 
 def up_kernel(place, *refs, pieces, quarter):
-    chunks = refs[:4]
-    weights = refs[4 : 4 + pieces]
-    taps, hidden, own_normed, xs, ws, up, flags, same, sems = refs[4 + pieces :]
+    chunks = (refs[:4], refs[4:8])
+    weights = refs[8 : 8 + pieces]
+    taps, *hiddens, own_normed, xs, ws, up, flags, same, sems = refs[8 + pieces :]
     sp, tp = place[0], place[1]
     x, core = tp // 2, tp % 2
     piece_rows = weights[0].shape[0]
     block = 4 * quarter
-    copies = []
-
-    def begin(src, dst):
-        copy = pltpu.make_async_copy(src, dst, sems.at[len(copies)])
-        copy.start()
-        copies.append(copy)
-
-    for i, chunk in enumerate(chunks):
-        number = (x ^ (i % 2)) * 2 + (core ^ (i // 2))
-        begin(
-            chunk.at[pl.ds(TAIL, quarter)],
-            xs.at[pl.ds(pl.multiple_of(TAIL + number * quarter, TAIL), quarter)],
+
+    def rows_in(m):
+        copies = []
+        for i, chunk in enumerate(chunks[m]):
+            number = (x ^ (i % 2)) * 2 + (core ^ (i // 2))
+            parts = (
+                (
+                    chunk.at[pl.ds(TAIL, quarter)],
+                    xs.at[m, pl.ds(pl.multiple_of(TAIL + number * quarter, TAIL), quarter)],
+                ),
+                (chunk.at[pl.ds(0, TAIL), pl.ds(0, LANES)], flags.at[m, number]),
+            )
+            for f, (src, dst) in enumerate(parts):
+                copies.append(pltpu.make_async_copy(src, dst, sems.at[m, 2 * i + f]))
+                copies[-1].start()
+
+            @pl.when(number == 0)
+            def _(chunk=chunk):
+                pltpu.make_async_copy(
+                    chunk.at[pl.ds(0, TAIL)], xs.at[m, pl.ds(0, TAIL)], sems.at[m, 8]
+                ).start()
+
+        copies.append(
+            pltpu.make_async_copy(
+                chunks[m][0].at[pl.ds(0, TAIL)], xs.at[m, pl.ds(0, TAIL)], sems.at[m, 8]
+            )
         )
-
-        begin(chunk.at[pl.ds(0, TAIL), pl.ds(0, LANES)], flags.at[number])
-
-        @pl.when(number == 0)
-        def _(chunk=chunk):
-            pltpu.make_async_copy(
-                chunk.at[pl.ds(0, TAIL)], xs.at[pl.ds(0, TAIL)], sems.at[8 + pieces]
-            ).start()
-
+        return copies
+
+    near = rows_in(0)
+    loads = []
     for j in range(pieces):
-        begin(weights[j], ws.at[pl.ds(pl.multiple_of((sp ^ j) * piece_rows, piece_rows), piece_rows)])
-    pltpu.make_async_copy(
-        chunks[0].at[pl.ds(0, TAIL)], xs.at[pl.ds(0, TAIL)], sems.at[8 + pieces]
-    ).wait()
-    for copy in copies:
-        copy.wait()
-
+        dst = ws.at[pl.ds(pl.multiple_of((sp ^ j) * piece_rows, piece_rows), piece_rows)]
+        loads.append(pltpu.make_async_copy(weights[j], dst, sems.at[2, j]))
+        loads[-1].start()
+    far = rows_in(1)
     half = ws.shape[1] // 2
     main = half // LANES * LANES
     rest = half - main
@@ -250,14 +259,15 @@
     line = lax.broadcasted_iota(jnp.int32, (quarter, quarter), 0)
     diagonal = line == lax.broadcasted_iota(jnp.int32, (quarter, quarter), 1)
     ones = jnp.ones((quarter, LANES), jnp.bfloat16)
-    for i in range(4):
-        rows = flags[i].astype(jnp.float32)
-        for lag in range(2):
-            spread = jnp.where(diagonal, rows[lag : lag + 1], 0.0).astype(jnp.bfloat16)
-            same[lag, i * quarter : (i + 1) * quarter] = jnp.dot(
-                spread, ones, preferred_element_type=jnp.float32
-            )
-    up[...] = jnp.dot(xs[...], ws[...], preferred_element_type=jnp.float32)
+
+    def spread_flags(m):
+        for i in range(4):
+            rows = flags[m, i].astype(jnp.float32)
+            for lag in range(2):
+                spread = jnp.where(diagonal, rows[lag : lag + 1], 0.0).astype(jnp.bfloat16)
+                same[lag, i * quarter : (i + 1) * quarter] = jnp.dot(
+                    spread, ones, preferred_element_type=jnp.float32
+                )
 
     def conv(rows, start, tap, one, two):
         lag1 = rows[TAIL - 1 : TAIL - 1 + sub, start : start + LANES]
@@ -272,53 +282,73 @@
         inner = v * (math.sqrt(2.0 / math.pi) + (0.044715 * math.sqrt(2.0 / math.pi)) * (v * v))
         return (0.5 * v) * (1.0 + jnp.tanh(inner))
 
-    def mix(i, _):
-        at = pl.ds(pl.multiple_of(i * sub, sub), sub)
-        reach = pl.ds(pl.multiple_of(i * sub, sub), sub + TAIL)
-        one, two = same[0, at, :], same[1, at, :]
-        for n in range(0, main, LANES):
-            rows = up[reach, 2 * n : 2 * n + pair]
-            tap = taps[:, 2 * n : 2 * n + pair]
-            h = gelu(conv(rows, 0, tap[:, :LANES], one, two))
-            h = h * conv(rows, LANES, tap[:, LANES:], one, two)
-            hidden[at, n : n + LANES] = h.astype(hidden.dtype)
-        mixed = conv(up[reach, 2 * main :], 0, taps[:, 2 * main :], one, two)
-        h = gelu(mixed) * pltpu.roll(mixed, rest, 1)
-        hidden[at, main:] = h[:, :rest].astype(hidden.dtype)
-        return 0
-
-    lax.fori_loop(0, block // sub, mix, 0)
+    def mix(hidden):
+        def step(i, _):
+            at = pl.ds(pl.multiple_of(i * sub, sub), sub)
+            reach = pl.ds(pl.multiple_of(i * sub, sub), sub + TAIL)
+            one, two = same[0, at, :], same[1, at, :]
+            for n in range(0, main, LANES):
+                rows = up[reach, 2 * n : 2 * n + pair]
+                tap = taps[:, 2 * n : 2 * n + pair]
+                h = gelu(conv(rows, 0, tap[:, :LANES], one, two))
+                h = h * conv(rows, LANES, tap[:, LANES:], one, two)
+                hidden[at, n : n + LANES] = h.astype(hidden.dtype)
+            mixed = conv(up[reach, 2 * main :], 0, taps[:, 2 * main :], one, two)
+            h = gelu(mixed) * pltpu.roll(mixed, rest, 1)
+            hidden[at, main:] = h[:, :rest].astype(hidden.dtype)
+            return 0
+
+        lax.fori_loop(0, block // sub, step, 0)
+
+    depth = ws.shape[0] // 2
+    for copy in (*near, *loads[: pieces // 2]):
+        copy.wait()
+    first = sp // (pieces // 2)
+    at = pl.ds(pl.multiple_of(first * depth, depth), depth)
+    up[...] = jnp.dot(xs[0, :, at], ws[at, :], preferred_element_type=jnp.float32)
+    spread_flags(0)
+    for copy in loads[pieces // 2 :]:
+        copy.wait()
+    at = pl.ds(pl.multiple_of((1 - first) * depth, depth), depth)
+    up[...] += jnp.dot(xs[0, :, at], ws[at, :], preferred_element_type=jnp.float32)
+    mix(hiddens[0])
+    for copy in far:
+        copy.wait()
+    spread_flags(1)
+    up[...] = jnp.dot(xs[1], ws[...], preferred_element_type=jnp.float32)
+    mix(hiddens[1])
     share = own_normed.shape[1]
-    own_normed[...] = xs[TAIL:, pl.ds(pl.multiple_of(tp * share, share), share)]
-
-
-def up_hidden(place, chunks, weights, taps, share):
-    quarter = chunks[0].shape[0] - TAIL
-    width = chunks[0].shape[1]
+    own_normed[...] = xs[0, TAIL:, pl.ds(pl.multiple_of(tp * share, share), share)]
+
+
+def up_hidden(place, near, far, weights, taps, share):
+    quarter = near[0].shape[0] - TAIL
+    width = near[0].shape[1]
     block = 4 * quarter
     cols = weights[0].shape[1]
     anywhere = pl.BlockSpec(memory_space=pl.ANY)
     return pl.pallas_call(
         functools.partial(up_kernel, pieces=len(weights), quarter=quarter),
         in_specs=[pl.BlockSpec(memory_space=pltpu.SMEM)]
-        + [anywhere] * (4 + len(weights))
+        + [anywhere] * (8 + len(weights))
         + [vmem()],
-        out_specs=[vmem(), vmem()],
+        out_specs=[vmem()] * 3,
         out_shape=[
+            jax.ShapeDtypeStruct((block, cols // 2), jnp.bfloat16),
             jax.ShapeDtypeStruct((block, cols // 2), jnp.bfloat16),
             jax.ShapeDtypeStruct((block, share), jnp.bfloat16),
         ],
         scratch_shapes=[
-            pltpu.VMEM((block + TAIL, width), jnp.bfloat16),
+            pltpu.VMEM((2, block + TAIL, width), jnp.bfloat16),
             pltpu.VMEM((width, cols), jnp.bfloat16),
             pltpu.VMEM((block + TAIL, cols), jnp.float32),
-            pltpu.VMEM((4, TAIL, LANES), jnp.bfloat16),
+            pltpu.VMEM((2, 4, TAIL, LANES), jnp.bfloat16),
             pltpu.VMEM((2, block, LANES), jnp.float32),
-            pltpu.SemaphoreType.DMA((9 + len(weights),)),
+            pltpu.SemaphoreType.DMA((3, max(9, len(weights)))),
         ],
         compiler_params=room(24),
         name="up_hidden",
-    )(place, *chunks, *weights, taps)
+    )(place, *near, *far, *weights, taps)
 
 
 def project_kernel(place, heads, weights, keep, send, left, right, made, came, went, *, quarter):
@@ -368,52 +398,71 @@
             pltpu.SemaphoreType.DMA((count + 1,)),
             pltpu.SemaphoreType.DMA((count, 4)),
         ],
-        compiler_params=room(56),
+        compiler_params=room(RS_ROOM),
         name="project",
     )(place, heads, weights)
 
 
-def merge_kernel(which, first, second, keep, send, a, b, c, came, went, *, axis):
+def merge_kernel(which, first, second, keep, send):
     own = which[0]
-    pieces = []
     for out, part in ((send, 1 - own), (keep, own)):
-        for j in range(first.shape[1 - axis]):
-            pieces.append((out.at[j], (part, j) if axis == 0 else (j, part)))
-    copies = []
-    for i, (_, at) in enumerate(pieces):
-        pair = [
-            pltpu.make_async_copy(src.at[at], dst.at[i], came.at[i, f])
-            for f, (src, dst) in enumerate(((first, a), (second, b)))
-        ]
-        for copy in pair:
-            copy.start()
-        copies.append(pair)
-    outs = []
-    for i, (out, _) in enumerate(pieces):
-        for copy in copies[i]:
-            copy.wait()
-        c[i] = a[i] + b[i]
-        outs.append(pltpu.make_async_copy(c.at[i], out, went.at[i]))
-        outs[-1].start()
-    for copy in outs:
-        copy.wait()
-
-
-def merge(which, first, second, axis, mib=8):
-    count = first.shape[1 - axis]
-    shape = jax.ShapeDtypeStruct((count, *first.shape[2:]), jnp.bfloat16)
-    anywhere = pl.BlockSpec(memory_space=pl.ANY)
-    scratch = pltpu.VMEM((2 * count, *first.shape[2:]), jnp.bfloat16)
+        out[...] = first[part] + second[part]
+
+
+def merge(which, first, second):
+    shape = jax.ShapeDtypeStruct(first.shape[1:], jnp.bfloat16)
     return pl.pallas_call(
-        functools.partial(merge_kernel, axis=axis),
-        in_specs=[pl.BlockSpec(memory_space=pltpu.SMEM), anywhere, anywhere],
-        out_specs=[anywhere, anywhere],
+        merge_kernel,
+        in_specs=[pl.BlockSpec(memory_space=pltpu.SMEM), vmem(), vmem()],
+        out_specs=[vmem(), vmem()],
         out_shape=[shape, shape],
-        scratch_shapes=[scratch] * 3
-        + [pltpu.SemaphoreType.DMA((2 * count, 2)), pltpu.SemaphoreType.DMA((2 * count,))],
-        compiler_params=room(mib),
+        compiler_params=room(RS_ROOM),
         name="merge",
     )(which, first, second)
+
+
+def fold_kernel(which, first, second, keep_a, send_a, keep_b, send_b):
+    own = which[0]
+    half = first.shape[3] // 2
+    for l in range(2):
+        for out, part in ((send_a, 1 - own), (keep_a, own)):
+            out[l] = first[part, l, :, :half] + second[part, l, :, :half]
+    for x in range(2):
+        for out, part in ((send_b, 1), (keep_b, 0)):
+            out[x] = first[x, part, :, half:] + second[x, part, :, half:]
+
+
+def fold(which, first, second):
+    _, _, rows, cols = first.shape
+    shape = jax.ShapeDtypeStruct((2, rows, cols // 2), jnp.bfloat16)
+    return pl.pallas_call(
+        fold_kernel,
+        in_specs=[pl.BlockSpec(memory_space=pltpu.SMEM), vmem(), vmem()],
+        out_specs=[vmem()] * 4,
+        out_shape=[shape] * 4,
+        compiler_params=room(4),
+        name="fold",
+    )(which, first, second)
+
+
+def refold_kernel(which, keep_a, came_a, keep_b, came_b, stay_a, send_a, stay_b, send_b):
+    own = which[0]
+    stay_a[...] = keep_a[0] + came_a[0]
+    send_a[...] = keep_a[1] + came_a[1]
+    stay_b[...] = keep_b[own] + came_b[own]
+    send_b[...] = keep_b[1 - own] + came_b[1 - own]
+
+
+def refold(which, *arrays):
+    shape = jax.ShapeDtypeStruct(arrays[0].shape[1:], jnp.bfloat16)
+    return pl.pallas_call(
+        refold_kernel,
+        in_specs=[pl.BlockSpec(memory_space=pltpu.SMEM)] + [vmem()] * 4,
+        out_specs=[vmem()] * 4,
+        out_shape=[shape] * 4,
+        compiler_params=room(4),
+        name="refold",
+    )(which, *arrays)
 
 
 def norm_kernel(place, first, second, residual, before, gain, flags, out, base, sems):
@@ -458,7 +507,7 @@
         out_specs=vmem(),
         out_shape=jax.ShapeDtypeStruct(first.shape, jnp.bfloat16),
         scratch_shapes=[pltpu.VMEM(first.shape, jnp.bfloat16), pltpu.SemaphoreType.DMA((2,))],
-        compiler_params=room(56),
+        compiler_params=room(RS_ROOM),
         name="normed_rows",
     )(place, first, second, residual, before, gain, flags)
 
@@ -503,16 +552,16 @@
     )(place, near, far, *pieces)
 
 
-def reduced(keep, send, x, x_first):
-    rows, cols = keep.shape[2:]
-    own = jnp.zeros((1,), jnp.int32)
+def reduced(keep, send, x):
     came = swapped(send, tp_mask=1)
-    keep, send = merge(x if x_first else own, keep, came, 0 if x_first else 1)
-    came = swapped(send, *((0, 2) if x_first else (2, 0)))
-    parts = lambda array: array.reshape(2, 2, rows // 2, cols)
-    keep, send = merge(own if x_first else x, parts(keep), parts(came), 0)
-    came = swapped(send, *((2, 0) if x_first else (0, 2)))
-    return keep.reshape(rows, cols), came.reshape(rows, cols)
+    keep_a, send_a, keep_b, send_b = fold(x, keep, came)
+    came_b = swapped(send_b, sp_mask=2)
+    came_a = swapped(send_a, tp_mask=2)
+    keep_a, send_a, keep_b, send_b = refold(x, keep_a, came_a, keep_b, came_b)
+    came_a = swapped(send_a, sp_mask=2)
+    came_b = swapped(send_b, tp_mask=2)
+    add = lambda one, two: one.astype(jnp.float32) + two.astype(jnp.float32)
+    return jnp.concatenate([add(keep_a, came_a), add(keep_b, came_b)], axis=1)
 
 
 def local_heads(came, query_rows, key_rows, value_rows, doc_ids, sink_logit):
@@ -576,8 +625,7 @@
     one = lambda index: index.astype(jnp.int32)[None]
     low_at, x_at, core_at = one(low), one(x), one(core)
 
-    docs_rows = doc_ids[rows - 2 * LANES :].astype(jnp.bfloat16).reshape(2, LANES)
-    docs_rows = jnp.pad(docs_rows, ((0, TAIL - 2), (0, 0)))
+    docs_rows = doc_ids.reshape(rows // LANES, LANES)
     own, other, halo = prepared(
         low_at, gate_proj, value_proj, query_rows, key_rows, value_rows, docs_rows, residual
     )
@@ -599,10 +647,10 @@
     flags = jnp.pad(flags, ((0, TAIL - 2), (0, 0)))
     keep, send = project(place, heads, out_proj, quarter)
     came = swapped(send, tp_mask=1)
-    keep, send = merge(x_at, keep[:, None], came[:, None], 0, 56)
+    keep, send = merge(x_at, keep, came)
     came = swapped(send, tp_mask=2)
     normed = normed_rows(
-        place, keep[0], came[0], residual, prev_residual, mix_gain[None, :], flags
+        place, keep, came, residual, prev_residual, mix_gain[None, :], flags
     )
     near = [normed, swapped(normed, tp_mask=2)]
     near += [swapped(near[0], tp_mask=1), swapped(near[1], tp_mask=1)]
@@ -621,14 +669,11 @@
     taps = jnp.concatenate([mains.reshape(TAPS, 2 * main), *rests], axis=1)
     taps = jnp.pad(taps, ((0, 8 - TAPS), (0, 0)))
 
-    near, own_normed = up_hidden(place, near, up_weights, taps, share)
-    far, _ = up_hidden(place, far, up_weights, taps, share)
+    near, far, own_normed = up_hidden(place, near, far, up_weights, taps, share)
     terms = down_terms(place, near, far, down_same)
-    ffn_same = reduced(*terms, x_at, False)
+    ffn_same = reduced(*terms, x_at)
     terms = down_terms(place, near, far, down_far)
-    ffn_far = reduced(*terms, x_at, True)
-    add = lambda pair: pair[0].astype(jnp.float32) + pair[1].astype(jnp.float32)
-    ffn_same, ffn_far = add(ffn_same), add(ffn_far)
+    ffn_far = reduced(*terms, x_at)
     ffn_own = jnp.where(
         y == 0,
         jnp.concatenate([ffn_same, ffn_far], axis=1),

time: 267 us -> 258 us (0.966)
  Pallas kernels: 47.3 us -> 39.3 us
  waiting for transfers between devices: 123 us -> 116 us
  starting transfers between devices: 53 us -> 59.7 us
    ppermute x12 -> x14, waiting for transfers between devices: 18.4 us -> 12 us  [swapped(): return lax.ppermute(block, 'tp', [(i, i ^ tp_mask) for i in range(n_tp)])]
    pallas_call x5, Pallas kernels: 7.74 us -> 3.39 us  [the longest x1 2.71 us: merge(): pl.pallas_call(merge_kernel, in_specs=[pl.BlockSpec(memory_space=pltpu.SM...]
    pallas_call x2 -> x1, Pallas kernels: 18.5 us -> 14.8 us  [up_hidden(): pl.pallas_call(functools.partial(up_kernel, pieces=len(weights), quarter=...]
    ppermute x12 -> x14, starting transfers between devices: 4.95 us -> 8.52 us  [swapped(): return lax.ppermute(block, 'tp', [(i, i ^ tp_mask) for i in range(n_tp)])]
    ppermute x17 -> x19, starting transfers between devices: 43.2 us -> 46.3 us  [swapped(): return lax.ppermute(block, 'sp', [(i, i ^ sp_mask) for i in range(n_sp)])]
    ppermute x17 -> x19, waiting for transfers between devices: 103 us -> 102 us  [swapped(): return lax.ppermute(block, 'sp', [(i, i ^ sp_mask) for i in range(n_sp)])]
  transfers between devices with their start and end apart: 30 -> 34, of which waited for: 14 -> 17; matrix products, arithmetic and copies ran while one was open for 1% -> 1% of each run, Pallas kernels for 12% -> 10%
where the time goes in v2:
time: 258 us
  waiting for transfers between devices  116 us (45%)
  starting transfers between devices  59.7 us (23%)
  Pallas kernels  39.3 us (15%)
  local copies, waits for them, and re-layouts  19.9 us (8%)
  other arithmetic  9.25 us (4%)
  matrix products  6.9 us (3%)
  blocking collectives  5.66 us (2%)
    ppermute x19, waiting for transfers between devices, swapped(): return lax.ppermute(block, 'sp', [(i, i ^ sp_mask) for i in range(n_sp)])  102 us
    ppermute x19, starting transfers between devices, swapped(): return lax.ppermute(block, 'sp', [(i, i ^ sp_mask) for i in range(n_sp)])  46.3 us
    unnamed x79, local copies, waits for them, and re-layouts  17.6 us
    pallas_call x1, Pallas kernels, up_hidden(): pl.pallas_call(functools.partial(up_kernel, pieces=len(weights), quarter=...  14.8 us
    ppermute x14, waiting for transfers between devices, swapped(): return lax.ppermute(block, 'tp', [(i, i ^ tp_mask) for i in range(n_tp)])  12 us
    ppermute x14, starting transfers between devices, swapped(): return lax.ppermute(block, 'tp', [(i, i ^ tp_mask) for i in range(n_tp)])  8.52 us
    pallas_call x2, Pallas kernels, down_terms(): pl.pallas_call(down_kernel, in_specs=[pl.BlockSpec(memory_space=pltpu.SME...  7.25 us
    psum x1, blocking collectives, paired(): lax.psum((jnp.sum(second_sum, axis=1), jnp.sum(second_sum * second_sum, a...  5.66 us
  transfers between devices with their start and end apart: 34, of which 17 were waited for; matrix products, arithmetic and copies ran while one was open for 1% of the time, Pallas kernels for 10%

profile of v2, /device:TPU:0, one launch (start us, length us, event | category | flops | bytes accessed | tf_op | source)
XLA Modules:
  0.0 257.6 jit_solution(369126277469799901)
XLA Ops:
  0.0 3.5 %prepare.1 = (bf16[256,1408]{1,0:T(8,128)(2,1)}, bf16[256,1408]{1,0:T(8,128)(2,1)}, bf16[424,128]{1,0:T(8,128)(2,1)}) custom-call(s32[1]{0:T(128)} %bitcast.3.which, bf16[256,1408]{1,0:T(8,128)(2,1)} %gates.1, bf16[256,1408]{1,0:T(8,128)(2,1)} %values_in.1, bf16[512,512]{1,0:T(8,128)(2,1)} %queries.1, bf16[64,512]{1,0:T(8,128)(2,1)} %bitcast.47, ...), custom_call_target="tpu_custom_call" | custom-call | tf_op jit(solution)/shard_map/prepare/pallas_call | solution.py:157
  3.5 4.9 %collective-permute-start = (bf16[424,128]{1,0:T(8,128)(2,1)}, bf16[424,128]{1,0:T(8,128)(2,1)S(1)}, u32[]{:S(2)}, u32[]{:S(2)}) collective-permute-start(bf16[424,128]{1,0:T(8,128)(2,1)} %get-tuple-element.37), channel_id=1, source_target_pairs={{0,4},{4,8},{8,12},{12,16},{16,20},{20,24},{24,28},{1,5},{5,9},{9,... | collective-permute-start | bytes 325640 | tf_op jit(solution)/shard_map/ppermute | solution.py:27
  9.1 2.0 collective-permute-done
  11.2 1.1 pad_maximum_fusion
  12.8 0.6 fusion.6
  13.4 2.7 %fusion.1 = (f32[8,520]{1,0:T(8,128)S(1)}, f32[648,520,8]{0,1,2:T(8,128)S(1)}) fusion(pred[520,648]{1,0:T(8,128)(4,1)S(1)} %fusion.6, bf16[520,8,64]{0,2,1:T(8,128)(2,1)S(1)} %bitcast.45, bf16[64,128]{1,0:T(8,128)(2,1)S(1)} %get-tuple-element.80, bf16[64,128]{1,0:T(8,128)(2,1)S(1)} %get-tuple-element.81, bf16[64,512]{1,0:T(8,128)(2,1)S(1)} %bitcast.48), kind=kOutput, calls=%fused_computation.4 | convolution fusion | flops 353378752 | bytes 11767104 | tf_op jit(solution)/shard_map/qkgd,skd->kgqs/dot_general | solution.py:46
  16.3 3.9 %fusion = f32[8,520]{1,0:T(8,128)S(1)} fusion(f32[648,520,8]{0,1,2:T(8,128)S(1)} %get-tuple-element.88, f32[8,520]{1,0:T(8,128)S(1)} %broadcast_maximum_fusion, pred[520,648]{1,0:T(8,128)(4,1)S(1)} %fusion.6), kind=kLoop, calls=%fused_computation.3 | loop fusion | flops 10778560 | bytes 11152960 | tf_op jit(solution)/shard_map/reduce_sum | solution.py:59
  20.2 4.2 %fusion.7 = bf16[64,8,520]{2,0,1:T(8,128)(2,1)S(1)} fusion(f32[8,520]{1,0:T(8,128)S(1)} %exponential_add_fusion, f32[8,520]{1,0:T(8,128)S(1)} %broadcast_maximum_fusion, f32[648,520,8]{0,1,2:T(8,128)S(1)} %get-tuple-element.88, pred[520,648]{1,0:T(8,128)(4,1)S(1)} %fusion.6, bf16[64,128]{1,0:T(8,128)(2,1)S(1)} %get-tuple-element.82, ...), kind=kOutput, calls=%fused_computation.12 | convolution fusion | flops 359040512 | bytes 11783744 | tf_op jit(solution)/shard_map/kgqs,skd->qkgd/dot_general | solution.py:61
  24.4 1.0 copy.18.heads
  25.5 4.7 %project.1 = (bf16[2,136,2048]{2,1,0:T(8,128)(2,1)}, bf16[2,136,2048]{2,1,0:T(8,128)(2,1)}) custom-call(s32[2]{0:T(128)} %pad_add_fusion.2.place, bf16[520,512]{1,0:T(8,128)(2,1)} %copy.18.heads, bf16[512,2048]{1,0:T(8,128)(2,1)} %weights.1), custom_call_target="tpu_custom_call" | custom-call | tf_op jit(solution)/shard_map/project/pallas_call | solution.py:389
  30.3 2.9 %collective-permute-done.1.second = bf16[2,136,2048]{2,1,0:T(8,128)(2,1)S(1)} collective-permute-done((bf16[2,136,2048]{2,1,0:T(8,128)(2,1)}, bf16[2,136,2048]{2,1,0:T(8,128)(2,1)S(1)}, u32[]{:S(2)}, u32[]{:S(2)}) %collective-permute-start.1) | collective-permute-done | bytes 1114144 | tf_op jit(solution)/shard_map/ppermute | solution.py:35
  33.2 1.0 copy-done.23
  34.2 2.7 %merge.1 = (bf16[136,2048]{1,0:T(8,128)(2,1)}, bf16[136,2048]{1,0:T(8,128)(2,1)}) custom-call(s32[1]{0:T(128)} %bitcast.2.which, bf16[2,136,2048]{2,1,0:T(8,128)(2,1)} %get-tuple-element.38.first, bf16[2,136,2048]{2,1,0:T(8,128)(2,1)} %copy-done.23), custom_call_target="tpu_custom_call" | custom-call | tf_op jit(solution)/shard_map/merge/pallas_call | solution.py:414
  36.9 1.5 collective-permute-start.2
  38.4 2.0 row_halves.1
  40.4 3.4 %collective-permute-start.17 = (bf16[704,256]{1,0:T(8,128)(2,1)}, bf16[704,256]{1,0:T(8,128)(2,1)}, u32[]{:S(2)}, u32[]{:S(2)}) collective-permute-start(bf16[704,256]{1,0:T(8,128)(2,1)} %get-tuple-element.48), channel_id=1, source_target_pairs={{0,8},{4,12},{8,0},{12,4},{16,24},{20,28},{24,16},{28,20},{1,9},{5... | collective-permute-start | bytes 1081352 | tf_op jit(solution)/shard_map/ppermute | solution.py:33
  43.8 2.6 %collective-permute-start.18 = (bf16[704,256]{1,0:T(8,128)(2,1)}, bf16[704,256]{1,0:T(8,128)(2,1)S(1)}, u32[]{:S(2)}, u32[]{:S(2)}) collective-permute-start(bf16[704,256]{1,0:T(8,128)(2,1)} %get-tuple-element.47.refs_0_), channel_id=1, source_target_pairs={{0,16},{4,20},{8,24},{12,28},{16,0},{20,4},{24,8},{28,12},{1,17},{... | collective-permute-start | bytes 1081352 | tf_op jit(solution)/shard_map/ppermute | solution.py:33
  46.8 14.1 %collective-permute-done.17.refs_1_ = bf16[704,256]{1,0:T(8,128)(2,1)} collective-permute-done((bf16[704,256]{1,0:T(8,128)(2,1)}, bf16[704,256]{1,0:T(8,128)(2,1)}, u32[]{:S(2)}, u32[]{:S(2)}) %collective-permute-start.17) | collective-permute-done | bytes 360480 | tf_op jit(solution)/shard_map/ppermute | solution.py:33
  61.0 3.9 %collective-permute-start.15 = (bf16[256,1408]{1,0:T(8,128)(2,1)}, bf16[256,1408]{1,0:T(8,128)(2,1)S(1)}, u32[]{:S(2)}, u32[]{:S(2)}) collective-permute-start(bf16[256,1408]{1,0:T(8,128)(2,1)} %get-tuple-element.43), channel_id=1, source_target_pairs={{0,24},{4,28},{8,16},{12,20},{16,8},{20,12},{24,0},{28,4},{1,25},{... | collective-permute-start | bytes 2162696 | tf_op jit(solution)/shard_map/ppermute | solution.py:33
  65.0 1.5 collective-permute-start.19
  67.9 3.6 %normed_rows.1.refs_0_ = bf16[136,2048]{1,0:T(8,128)(2,1)} custom-call(s32[2]{0:T(128)} %pad_add_fusion.2.place, bf16[136,2048]{1,0:T(8,128)(2,1)} %get-tuple-element.40.first, bf16[136,2048]{1,0:T(8,128)(2,1)} %collective-permute-done.2.second, bf16[512,2048]{1,0:T(8,128)(2,1)} %residual.3, bf16[8,2048]{1,0:T(8,128)(2,1)} %copy-done.26, ...), custom_call_target="tpu_custom_call" | custom-call | tf_op jit(solution)/shard_map/normed_rows/pallas_call | solution.py:504
  71.6 45.1 %collective-permute-done.19.refs_3_ = bf16[704,256]{1,0:T(8,128)(2,1)} collective-permute-done((bf16[704,256]{1,0:T(8,128)(2,1)}, bf16[704,256]{1,0:T(8,128)(2,1)}, u32[]{:S(2)}, u32[]{:S(2)}) %collective-permute-start.19) | collective-permute-done | bytes 360480 | tf_op jit(solution)/shard_map/ppermute | solution.py:33
  116.7 23.8 %collective-permute-start.6 = (bf16[136,2048]{1,0:T(8,128)(2,1)}, bf16[136,2048]{1,0:T(8,128)(2,1)S(1)}, u32[]{:S(2)}, u32[]{:S(2)}) collective-permute-start(bf16[136,2048]{1,0:T(8,128)(2,1)} %normed_rows.1.refs_0_), channel_id=1, source_target_pairs={{0,8},{4,12},{8,0},{12,4},{16,24},{20,28},{24,16},{28,20},{1,9},{5... | collective-permute-start | bytes 1671176 | tf_op jit(solution)/shard_map/ppermute | solution.py:33
  140.5 0.6 collective-permute-start.12
  141.1 1.4 collective-permute-start.14
  143.1 9.2 %collective-permute-done.6.refs_4_ = bf16[136,2048]{1,0:T(8,128)(2,1)S(1)} collective-permute-done((bf16[136,2048]{1,0:T(8,128)(2,1)}, bf16[136,2048]{1,0:T(8,128)(2,1)S(1)}, u32[]{:S(2)}, u32[]{:S(2)}) %collective-permute-start.6) | collective-permute-done | bytes 557088 | tf_op jit(solution)/shard_map/ppermute | solution.py:33
  152.8 0.9 copy-done.2
  154.3 5.2 %collective-permute-done.12.refs_11_ = bf16[256,1408]{1,0:T(8,128)(2,1)S(1)} collective-permute-done((bf16[256,1408]{1,0:T(8,128)(2,1)S(1)}, bf16[256,1408]{1,0:T(8,128)(2,1)S(1)}, u32[]{:S(2)}, u32[]{:S(2)}) %collective-permute-start.12) | collective-permute-done | bytes 720928 | tf_op jit(solution)/shard_map/ppermute | solution.py:33
  159.5 0.9 copy-done.4
  160.9 0.8 copy-done.10
  161.7 13.2 %collective-permute-done.14.refs_13_ = bf16[256,1408]{1,0:T(8,128)(2,1)S(1)} collective-permute-done((bf16[256,1408]{1,0:T(8,128)(2,1)S(1)}, bf16[256,1408]{1,0:T(8,128)(2,1)S(1)}, u32[]{:S(2)}, u32[]{:S(2)}) %collective-permute-start.14) | collective-permute-done | bytes 720928 | tf_op jit(solution)/shard_map/ppermute | solution.py:33
  175.0 0.9 copy-done.6
  176.4 11.6 %collective-permute-done.16.refs_15_ = bf16[256,1408]{1,0:T(8,128)(2,1)S(1)} collective-permute-done((bf16[256,1408]{1,0:T(8,128)(2,1)S(1)}, bf16[256,1408]{1,0:T(8,128)(2,1)S(1)}, u32[]{:S(2)}, u32[]{:S(2)}) %collective-permute-start.16) | collective-permute-done | bytes 720928 | tf_op jit(solution)/shard_map/ppermute | solution.py:33
  187.9 0.9 copy-done.8
  189.4 0.8 copy-done.12
  190.2 1.4 collective-permute-start.26
  191.6 0.8 copy-done.14
  193.1 0.8 copy-done.16
  193.9 1.4 collective-permute-start.28
  195.6 1.0 copy-done
  196.7 1.1 copy-done.3
  197.8 1.1 copy-done.5
  198.9 1.1 copy-done.7
  200.0 1.1 copy-done.9
  201.1 1.1 copy-done.11
  202.1 1.1 copy-done.13
  203.2 1.1 copy-done.15
  204.3 1.1 copy-done.17
  205.3 14.8 %up_hidden.1 = (bf16[512,704]{1,0:T(8,128)(2,1)S(1)}, bf16[512,704]{1,0:T(8,128)(2,1)S(1)}, bf16[512,512]{1,0:T(8,128)(2,1)S(1)}) custom-call(s32[2]{0:T(128)S(1)} %copy-done.22, bf16[136,2048]{1,0:T(8,128)(2,1)S(1)} %copy-done, bf16[136,2048]{1,0:T(8,128)(2,1)S(1)} %copy-done.11, bf16[136,2048]{1,0:T(8,128)(2,1)S(1)} %copy-done.13, ...), custom_call_target="tpu_custom_call" | custom-call | tf_op jit(solution)/shard_map/up_hidden/pallas_call | solution.py:330
  220.2 3.7 %down_terms.3 = (bf16[2,2,512,256]{3,2,1,0:T(8,128)(2,1)S(1)}, bf16[2,2,512,256]{3,2,1,0:T(8,128)(2,1)S(1)}) custom-call(s32[2]{0:T(128)S(1)} %copy-done.22, bf16[512,704]{1,0:T(8,128)(2,1)S(1)} %get-tuple-element.45.near, bf16[512,704]{1,0:T(8,128)(2,1)S(1)} %get-tuple-element.46.far, bf16[704,256]{1,0:T(8,128)(2,1)} %collective-permute-done.25.refs_0_, ...), custom_call_target="tpu_custom_call" | custom-call | tf_op jit(solution)/shard_map/down_terms/pallas_call | solution.py:541
  224.1 3.5 %down_terms.2 = (bf16[2,2,512,256]{3,2,1,0:T(8,128)(2,1)S(1)}, bf16[2,2,512,256]{3,2,1,0:T(8,128)(2,1)S(1)}) custom-call(s32[2]{0:T(128)S(1)} %copy-done.22, bf16[512,704]{1,0:T(8,128)(2,1)S(1)} %get-tuple-element.45.near, bf16[512,704]{1,0:T(8,128)(2,1)S(1)} %get-tuple-element.46.far, bf16[704,256]{1,0:T(8,128)(2,1)S(1)} %copy-done.19, ...), custom_call_target="tpu_custom_call" | custom-call | tf_op jit(solution)/shard_map/down_terms/pallas_call | solution.py:541
  229.6 0.9 collective-permute-done.20.second
  230.7 0.7 collective-permute-start.21
  231.4 1.5 collective-permute-start.22
  232.8 4.8 %collective-permute-done.30.came_a = bf16[2,512,128]{2,1,0:T(8,128)(2,1)S(1)} collective-permute-done((bf16[2,512,128]{2,1,0:T(8,128)(2,1)S(1)}, bf16[2,512,128]{2,1,0:T(8,128)(2,1)S(1)}, u32[]{:S(2)}, u32[]{:S(2)}) %collective-permute-start.30) | collective-permute-done | bytes 262176 | tf_op jit(solution)/shard_map/ppermute | solution.py:35
  238.3 0.6 collective-permute-start.32
  238.9 1.5 collective-permute-start.33
  240.4 2.8 %collective-permute-done.21.came_a = bf16[2,512,128]{2,1,0:T(8,128)(2,1)S(1)} collective-permute-done((bf16[2,512,128]{2,1,0:T(8,128)(2,1)S(1)}, bf16[2,512,128]{2,1,0:T(8,128)(2,1)S(1)}, u32[]{:S(2)}, u32[]{:S(2)}) %collective-permute-start.21) | collective-permute-done | bytes 262176 | tf_op jit(solution)/shard_map/ppermute | solution.py:35
  243.9 0.6 collective-permute-start.23
  244.5 1.5 collective-permute-start.24
  246.6 2.4 collective-permute-done.23
  249.5 1.4 fusion.28
  250.9 5.7 %all-reduce.2 = (f32[512]{0:T(512)S(1)}, f32[512]{0:T(512)S(1)}) all-reduce(f32[512]{0:T(512)S(1)} %get-tuple-element.70, f32[512]{0:T(512)S(1)} %get-tuple-element.69), channel_id=1, replica_groups=mesh['sp'=8,'tp'=4] {'tp'}, use_global_device_ids=true, to_apply=%region_5.6 | all-reduce | flops 1024 | bytes 8192 | tf_op jit(solution)/shard_map/psum | solution.py:683
  256.6 1.0 multiply_convert_fusion
  (137 shorter events, 12.5 us)
Async XLA Ops:
  0.0 13.4 %copy-start.24 = (bf16[512,64]{0,1:T(8,128)(2,1)S(1)}, bf16[512,64]{0,1:T(8,128)(2,1)}, u32[]{:S(2)}) copy-start(bf16[512,64]{0,1:T(8,128)(2,1)} %param.15) | copy-start | bytes 196612
  0.0 12.7 %copy-start.27 = (s32[512]{0:T(512)S(1)}, s32[512]{0:T(512)}, u32[]{:S(2)}) copy-start(s32[512]{0:T(512)} %param.17) | copy-start | bytes 6148
  3.5 7.5 %collective-permute-start = (bf16[424,128]{1,0:T(8,128)(2,1)}, bf16[424,128]{1,0:T(8,128)(2,1)S(1)}, u32[]{:S(2)}, u32[]{:S(2)}) collective-permute-start(bf16[424,128]{1,0:T(8,128)(2,1)} %get-tuple-element.37), channel_id=1, source_target_pairs={{0,4},{4,8},{8,12},{12,16},{16,20},{20,24},{24,28},{1,5},{5,9},{9,... | collective-permute-start | bytes 325640 | tf_op jit(solution)/shard_map/ppermute | solution.py:27
  11.2 5.0 %copy-start.26 = (bf16[8,2048]{1,0:T(8,128)(2,1)}, bf16[8,2048]{1,0:T(8,128)(2,1)S(1)}, u32[]{:S(2)}) copy-start(bf16[8,2048]{1,0:T(8,128)(2,1)S(1)} %get-tuple-element.74.before) | copy-start | bytes 98308
  13.4 2.7 %copy-start.31 = (f32[8]{0:T(128)S(1)}, f32[8]{0:T(128)}, u32[]{:S(2)}) copy-start(f32[8]{0:T(128)} %param.18) | copy-start | bytes 100
  16.3 4.0 %copy-start.25 = (bf16[512,64]{0,1:T(8,128)(2,1)S(1)}, bf16[512,64]{0,1:T(8,128)(2,1)}, u32[]{:S(2)}) copy-start(bf16[512,64]{0,1:T(8,128)(2,1)} %param.16) | copy-start | bytes 196612
  24.4 22.4 %copy-start.1 = (bf16[256,1408]{1,0:T(8,128)(2,1)S(1)}, bf16[256,1408]{1,0:T(8,128)(2,1)}, u32[]{:S(2)}) copy-start(bf16[256,1408]{1,0:T(8,128)(2,1)} %get-tuple-element.42.refs_8_) | copy-start | bytes 2162692
  24.4 170.9 %copy-start.28 = (f32[3,1408]{1,0:T(4,128)S(1)}, f32[3,1408]{1,0:T(4,128)}, u32[]{:S(2)}) copy-start(f32[3,1408]{1,0:T(4,128)} %param.25) | copy-start | bytes 50692
  24.4 170.9 %copy-start.29 = (f32[3,1408]{1,0:T(4,128)S(1)}, f32[3,1408]{1,0:T(4,128)}, u32[]{:S(2)}) copy-start(f32[3,1408]{1,0:T(4,128)} %param.24) | copy-start | bytes 50692
  24.4 171.2 %copy-start.22 = (s32[2]{0:T(128)S(1)}, s32[2]{0:T(128)}, u32[]{:S(2)}) copy-start(s32[2]{0:T(128)} %pad_add_fusion.2.place) | copy-start | bytes 28
  30.2 3.0 %collective-permute-start.1 = (bf16[2,136,2048]{2,1,0:T(8,128)(2,1)}, bf16[2,136,2048]{2,1,0:T(8,128)(2,1)S(1)}, u32[]{:S(2)}, u32[]{:S(2)}) collective-permute-start(bf16[2,136,2048]{2,1,0:T(8,128)(2,1)} %get-tuple-element.39), channel_id=1, source_target_pairs={{0,1},{1,0},{2,3},{3,2},{4,5},{5,4},{6,7},{7,6},{8,9},{9,8},{10,11... | collective-permute-start | bytes 3342344 | tf_op jit(solution)/shard_map/ppermute | solution.py:35
  33.2 1.0 copy-start.23
  36.9 29.6 %collective-permute-start.2 = (bf16[136,2048]{1,0:T(8,128)(2,1)}, bf16[136,2048]{1,0:T(8,128)(2,1)}, u32[]{:S(2)}, u32[]{:S(2)}) collective-permute-start(bf16[136,2048]{1,0:T(8,128)(2,1)} %get-tuple-element.41), channel_id=1, source_target_pairs={{0,2},{1,3},{2,0},{3,1},{4,6},{5,7},{6,4},{7,5},{8,10},{9,11},{10,... | collective-permute-start | bytes 1671176 | tf_op jit(solution)/shard_map/ppermute | solution.py:35
  40.4 20.6 %collective-permute-start.17 = (bf16[704,256]{1,0:T(8,128)(2,1)}, bf16[704,256]{1,0:T(8,128)(2,1)}, u32[]{:S(2)}, u32[]{:S(2)}) collective-permute-start(bf16[704,256]{1,0:T(8,128)(2,1)} %get-tuple-element.48), channel_id=1, source_target_pairs={{0,8},{4,12},{8,0},{12,4},{16,24},{20,28},{24,16},{28,20},{1,9},{5... | collective-permute-start | bytes 1081352 | tf_op jit(solution)/shard_map/ppermute | solution.py:33
  43.8 21.2 %collective-permute-start.18 = (bf16[704,256]{1,0:T(8,128)(2,1)}, bf16[704,256]{1,0:T(8,128)(2,1)S(1)}, u32[]{:S(2)}, u32[]{:S(2)}) collective-permute-start(bf16[704,256]{1,0:T(8,128)(2,1)} %get-tuple-element.47.refs_0_), channel_id=1, source_target_pairs={{0,16},{4,20},{8,24},{12,28},{16,0},{20,4},{24,8},{28,12},{1,17},{... | collective-permute-start | bytes 1081352 | tf_op jit(solution)/shard_map/ppermute | solution.py:33
  46.4 94.1 %collective-permute-start.11 = (bf16[256,1408]{1,0:T(8,128)(2,1)}, bf16[256,1408]{1,0:T(8,128)(2,1)S(1)}, u32[]{:S(2)}, u32[]{:S(2)}) collective-permute-start(bf16[256,1408]{1,0:T(8,128)(2,1)} %get-tuple-element.43), channel_id=1, source_target_pairs={{0,8},{4,12},{8,0},{12,4},{16,24},{20,28},{24,16},{28,20},{1,9},{5... | collective-permute-start | bytes 2162696 | tf_op jit(solution)/shard_map/ppermute | solution.py:33
  46.8 94.3 %collective-permute-start.13 = (bf16[256,1408]{1,0:T(8,128)(2,1)S(1)}, bf16[256,1408]{1,0:T(8,128)(2,1)S(1)}, u32[]{:S(2)}, u32[]{:S(2)}) collective-permute-start(bf16[256,1408]{1,0:T(8,128)(2,1)S(1)} %copy-done.1), channel_id=1, source_target_pairs={{0,16},{4,20},{8,24},{12,28},{16,0},{20,4},{24,8},{28,12},{1,17},{... | collective-permute-start | bytes 2162696 | tf_op jit(solution)/shard_map/ppermute | solution.py:33
  61.0 81.6 %collective-permute-start.15 = (bf16[256,1408]{1,0:T(8,128)(2,1)}, bf16[256,1408]{1,0:T(8,128)(2,1)S(1)}, u32[]{:S(2)}, u32[]{:S(2)}) collective-permute-start(bf16[256,1408]{1,0:T(8,128)(2,1)} %get-tuple-element.43), channel_id=1, source_target_pairs={{0,24},{4,28},{8,16},{12,20},{16,8},{20,12},{24,0},{28,4},{1,25},{... | collective-permute-start | bytes 2162696 | tf_op jit(solution)/shard_map/ppermute | solution.py:33
  65.0 6.6 %copy-start.20 = (bf16[704,256]{1,0:T(8,128)(2,1)}, bf16[704,256]{1,0:T(8,128)(2,1)S(1)}, u32[]{:S(2)}) copy-start(bf16[704,256]{1,0:T(8,128)(2,1)S(1)} %collective-permute-done.18.refs_2_) | copy-start | bytes 1081348
  65.0 51.7 %collective-permute-start.19 = (bf16[704,256]{1,0:T(8,128)(2,1)}, bf16[704,256]{1,0:T(8,128)(2,1)}, u32[]{:S(2)}, u32[]{:S(2)}) collective-permute-start(bf16[704,256]{1,0:T(8,128)(2,1)} %get-tuple-element.48), channel_id=1, source_target_pairs={{0,24},{4,28},{8,16},{12,20},{16,8},{20,12},{24,0},{28,4},{1,25},{... | collective-permute-start | bytes 1081352 | tf_op jit(solution)/shard_map/ppermute | solution.py:33
  66.6 86.3 %collective-permute-start.10 = (bf16[256,1408]{1,0:T(8,128)(2,1)S(1)}, bf16[256,1408]{1,0:T(8,128)(2,1)S(1)}, u32[]{:S(2)}, u32[]{:S(2)}) collective-permute-start(bf16[256,1408]{1,0:T(8,128)(2,1)S(1)} %copy-done.1), channel_id=1, source_target_pairs={{0,4},{4,0},{8,12},{12,8},{16,20},{20,16},{24,28},{28,24},{1,5},{5... | collective-permute-start | bytes 2162696 | tf_op jit(solution)/shard_map/ppermute | solution.py:33
  116.7 35.6 %collective-permute-start.6 = (bf16[136,2048]{1,0:T(8,128)(2,1)}, bf16[136,2048]{1,0:T(8,128)(2,1)S(1)}, u32[]{:S(2)}, u32[]{:S(2)}) collective-permute-start(bf16[136,2048]{1,0:T(8,128)(2,1)} %normed_rows.1.refs_0_), channel_id=1, source_target_pairs={{0,8},{4,12},{8,0},{12,4},{16,24},{20,28},{24,16},{28,20},{1,9},{5... | collective-permute-start | bytes 1671176 | tf_op jit(solution)/shard_map/ppermute | solution.py:33
  140.5 19.0 %collective-permute-start.12 = (bf16[256,1408]{1,0:T(8,128)(2,1)S(1)}, bf16[256,1408]{1,0:T(8,128)(2,1)S(1)}, u32[]{:S(2)}, u32[]{:S(2)}) collective-permute-start(bf16[256,1408]{1,0:T(8,128)(2,1)S(1)} %collective-permute-done.11.refs_10_), channel_id=1, source_target_pairs={{0,4},{4,0},{8,12},{12,8},{16,20},{20,16},{24,28},{28,24},{1,5},{5... | collective-permute-start | bytes 2162696 | tf_op jit(solution)/shard_map/ppermute | solution.py:33
  141.1 33.8 %collective-permute-start.14 = (bf16[256,1408]{1,0:T(8,128)(2,1)S(1)}, bf16[256,1408]{1,0:T(8,128)(2,1)S(1)}, u32[]{:S(2)}, u32[]{:S(2)}) collective-permute-start(bf16[256,1408]{1,0:T(8,128)(2,1)S(1)} %collective-permute-done.13.refs_12_), channel_id=1, source_target_pairs={{0,4},{4,0},{8,12},{12,8},{16,20},{20,16},{24,28},{28,24},{1,5},{5... | collective-permute-start | bytes 2162696 | tf_op jit(solution)/shard_map/ppermute | solution.py:33
  142.6 17.8 %collective-permute-start.3 = (bf16[136,2048]{1,0:T(8,128)(2,1)}, bf16[136,2048]{1,0:T(8,128)(2,1)S(1)}, u32[]{:S(2)}, u32[]{:S(2)}) collective-permute-start(bf16[136,2048]{1,0:T(8,128)(2,1)} %normed_rows.1.refs_0_), channel_id=1, source_target_pairs={{0,2},{1,3},{2,0},{3,1},{4,6},{5,7},{6,4},{7,5},{8,10},{9,11},{10,... | collective-permute-start | bytes 1671176 | tf_op jit(solution)/shard_map/ppermute | solution.py:35
  152.3 23.6 %collective-permute-start.7 = (bf16[136,2048]{1,0:T(8,128)(2,1)S(1)}, bf16[136,2048]{1,0:T(8,128)(2,1)}, u32[]{:S(2)}, u32[]{:S(2)}) collective-permute-start(bf16[136,2048]{1,0:T(8,128)(2,1)S(1)} %collective-permute-done.6.refs_4_), channel_id=1, source_target_pairs={{0,2},{1,3},{2,0},{3,1},{4,6},{5,7},{6,4},{7,5},{8,10},{9,11},{10,... | collective-permute-start | bytes 1671176 | tf_op jit(solution)/shard_map/ppermute | solution.py:35
  152.8 0.9 copy-start.2
  153.7 34.2 %collective-permute-start.16 = (bf16[256,1408]{1,0:T(8,128)(2,1)S(1)}, bf16[256,1408]{1,0:T(8,128)(2,1)S(1)}, u32[]{:S(2)}, u32[]{:S(2)}) collective-permute-start(bf16[256,1408]{1,0:T(8,128)(2,1)S(1)} %collective-permute-done.15.refs_14_), channel_id=1, source_target_pairs={{0,4},{4,0},{8,12},{12,8},{16,20},{20,16},{24,28},{28,24},{1,5},{5... | collective-permute-start | bytes 2162696 | tf_op jit(solution)/shard_map/ppermute | solution.py:33
  159.5 0.9 copy-start.4
  160.4 29.0 %collective-permute-start.4 = (bf16[136,2048]{1,0:T(8,128)(2,1)}, bf16[136,2048]{1,0:T(8,128)(2,1)S(1)}, u32[]{:S(2)}, u32[]{:S(2)}) collective-permute-start(bf16[136,2048]{1,0:T(8,128)(2,1)} %normed_rows.1.refs_0_), channel_id=1, source_target_pairs={{0,1},{1,0},{2,3},{3,2},{4,5},{5,4},{6,7},{7,6},{8,9},{9,8},{10,11... | collective-permute-start | bytes 1671176 | tf_op jit(solution)/shard_map/ppermute | solution.py:35
  160.4 31.2 %collective-permute-start.5 = (bf16[136,2048]{1,0:T(8,128)(2,1)S(1)}, bf16[136,2048]{1,0:T(8,128)(2,1)S(1)}, u32[]{:S(2)}, u32[]{:S(2)}) collective-permute-start(bf16[136,2048]{1,0:T(8,128)(2,1)S(1)} %collective-permute-done.3.refs_1_), channel_id=1, source_target_pairs={{0,1},{1,0},{2,3},{3,2},{4,5},{5,4},{6,7},{7,6},{8,9},{9,8},{10,11... | collective-permute-start | bytes 1671176 | tf_op jit(solution)/shard_map/ppermute | solution.py:35
  160.9 0.8 copy-start.10
  175.0 0.9 copy-start.6
  175.8 17.3 %collective-permute-start.8 = (bf16[136,2048]{1,0:T(8,128)(2,1)S(1)}, bf16[136,2048]{1,0:T(8,128)(2,1)S(1)}, u32[]{:S(2)}, u32[]{:S(2)}) collective-permute-start(bf16[136,2048]{1,0:T(8,128)(2,1)S(1)} %collective-permute-done.6.refs_4_), channel_id=1, source_target_pairs={{0,1},{1,0},{2,3},{3,2},{4,5},{5,4},{6,7},{7,6},{8,9},{9,8},{10,11... | collective-permute-start | bytes 1671176 | tf_op jit(solution)/shard_map/ppermute | solution.py:35
  175.8 19.7 %collective-permute-start.9 = (bf16[136,2048]{1,0:T(8,128)(2,1)}, bf16[136,2048]{1,0:T(8,128)(2,1)}, u32[]{:S(2)}, u32[]{:S(2)}) collective-permute-start(bf16[136,2048]{1,0:T(8,128)(2,1)} %collective-permute-done.7.refs_5_), channel_id=1, source_target_pairs={{0,1},{1,0},{2,3},{3,2},{4,5},{5,4},{6,7},{7,6},{8,9},{9,8},{10,11... | collective-permute-start | bytes 1671176 | tf_op jit(solution)/shard_map/ppermute | solution.py:35
  187.9 0.9 copy-start.8
  188.8 31.3 %collective-permute-start.25 = (bf16[704,256]{1,0:T(8,128)(2,1)}, bf16[704,256]{1,0:T(8,128)(2,1)}, u32[]{:S(2)}, u32[]{:S(2)}) collective-permute-start(bf16[704,256]{1,0:T(8,128)(2,1)} %get-tuple-element.47.refs_0_), channel_id=1, source_target_pairs={{0,4},{4,0},{8,12},{12,8},{16,20},{20,16},{24,28},{28,24},{1,5},{5... | collective-permute-start | bytes 1081352 | tf_op jit(solution)/shard_map/ppermute | solution.py:33
  190.2 29.9 %collective-permute-start.26 = (bf16[704,256]{1,0:T(8,128)(2,1)}, bf16[704,256]{1,0:T(8,128)(2,1)}, u32[]{:S(2)}, u32[]{:S(2)}) collective-permute-start(bf16[704,256]{1,0:T(8,128)(2,1)} %collective-permute-done.17.refs_1_), channel_id=1, source_target_pairs={{0,4},{4,0},{8,12},{12,8},{16,20},{20,16},{24,28},{28,24},{1,5},{5... | collective-permute-start | bytes 1081352 | tf_op jit(solution)/shard_map/ppermute | solution.py:33
  191.6 0.8 copy-start.14
  192.5 27.7 %collective-permute-start.27 = (bf16[704,256]{1,0:T(8,128)(2,1)}, bf16[704,256]{1,0:T(8,128)(2,1)}, u32[]{:S(2)}, u32[]{:S(2)}) collective-permute-start(bf16[704,256]{1,0:T(8,128)(2,1)} %copy-done.20), channel_id=1, source_target_pairs={{0,4},{4,0},{8,12},{12,8},{16,20},{20,16},{24,28},{28,24},{1,5},{5... | collective-permute-start | bytes 1081352 | tf_op jit(solution)/shard_map/ppermute | solution.py:33
  193.9 26.4 %collective-permute-start.28 = (bf16[704,256]{1,0:T(8,128)(2,1)}, bf16[704,256]{1,0:T(8,128)(2,1)}, u32[]{:S(2)}, u32[]{:S(2)}) collective-permute-start(bf16[704,256]{1,0:T(8,128)(2,1)} %collective-permute-done.19.refs_3_), channel_id=1, source_target_pairs={{0,4},{4,0},{8,12},{12,8},{16,20},{20,16},{24,28},{28,24},{1,5},{5... | collective-permute-start | bytes 1081352 | tf_op jit(solution)/shard_map/ppermute | solution.py:33
  195.6 1.1 copy-start
  196.6 1.1 copy-start.3
  197.8 1.1 copy-start.5
  198.9 1.1 copy-start.7
  200.0 1.1 copy-start.9
  201.1 1.1 copy-start.11
  202.1 1.1 copy-start.13
  203.2 1.1 copy-start.15
  204.3 1.1 copy-start.17
  205.3 18.7 %copy-start.19 = (bf16[704,256]{1,0:T(8,128)(2,1)S(1)}, bf16[704,256]{1,0:T(8,128)(2,1)}, u32[]{:S(2)}) copy-start(bf16[704,256]{1,0:T(8,128)(2,1)} %get-tuple-element.47.refs_0_) | copy-start | bytes 1081348
  205.3 18.7 %copy-start.21 = (bf16[704,256]{1,0:T(8,128)(2,1)S(1)}, bf16[704,256]{1,0:T(8,128)(2,1)}, u32[]{:S(2)}) copy-start(bf16[704,256]{1,0:T(8,128)(2,1)} %copy-done.20) | copy-start | bytes 1081348
  220.1 10.5 %copy-start.18 = (bf16[512,512]{1,0:T(8,128)(2,1)}, bf16[512,512]{1,0:T(8,128)(2,1)S(1)}, u32[]{:S(2)}) copy-start(bf16[512,512]{1,0:T(8,128)(2,1)S(1)} %get-tuple-element.44) | copy-start | bytes 1572868
  223.9 32.6 %copy-start.30 = (f32[512]{0:T(512)S(1)}, f32[512]{0:T(512)}, u32[]{:S(2)}) copy-start(f32[512]{0:T(512)} %param.27) | copy-start | bytes 6148
  224.0 4.2 %collective-permute-start.29 = (bf16[2,2,512,256]{3,2,1,0:T(8,128)(2,1)S(1)}, bf16[2,2,512,256]{3,2,1,0:T(8,128)(2,1)S(1)}, u32[]{:S(2)}, u32[]{:S(2)}) collective-permute-start(bf16[2,2,512,256]{3,2,1,0:T(8,128)(2,1)S(1)} %get-tuple-element.60), channel_id=1, source_target_pairs={{0,1},{1,0},{2,3},{3,2},{4,5},{5,4},{6,7},{7,6},{8,9},{9,8},{10,11... | collective-permute-start | bytes 3145736 | tf_op jit(solution)/shard_map/ppermute | solution.py:35
  227.6 2.8 %collective-permute-start.20 = (bf16[2,2,512,256]{3,2,1,0:T(8,128)(2,1)S(1)}, bf16[2,2,512,256]{3,2,1,0:T(8,128)(2,1)S(1)}, u32[]{:S(2)}, u32[]{:S(2)}) collective-permute-start(bf16[2,2,512,256]{3,2,1,0:T(8,128)(2,1)S(1)} %get-tuple-element.50), channel_id=1, source_target_pairs={{0,1},{1,0},{2,3},{3,2},{4,5},{5,4},{6,7},{7,6},{8,9},{9,8},{10,11... | collective-permute-start | bytes 3145736 | tf_op jit(solution)/shard_map/ppermute | solution.py:35
  228.4 9.2 %collective-permute-start.30 = (bf16[2,512,128]{2,1,0:T(8,128)(2,1)S(1)}, bf16[2,512,128]{2,1,0:T(8,128)(2,1)S(1)}, u32[]{:S(2)}, u32[]{:S(2)}) collective-permute-start(bf16[2,512,128]{2,1,0:T(8,128)(2,1)S(1)} %get-tuple-element.62), channel_id=1, source_target_pairs={{0,2},{1,3},{2,0},{3,1},{4,6},{5,7},{6,4},{7,5},{8,10},{9,11},{10,... | collective-permute-start | bytes 786440 | tf_op jit(solution)/shard_map/ppermute | solution.py:35
  229.0 9.2 %collective-permute-start.31 = (bf16[2,512,128]{2,1,0:T(8,128)(2,1)S(1)}, bf16[2,512,128]{2,1,0:T(8,128)(2,1)S(1)}, u32[]{:S(2)}, u32[]{:S(2)}) collective-permute-start(bf16[2,512,128]{2,1,0:T(8,128)(2,1)S(1)} %get-tuple-element.64), channel_id=1, source_target_pairs={{0,8},{4,12},{8,0},{12,4},{16,24},{20,28},{24,16},{28,20},{1,9},{5... | collective-permute-start | bytes 786440 | tf_op jit(solution)/shard_map/ppermute | solution.py:33
  230.7 12.6 %collective-permute-start.21 = (bf16[2,512,128]{2,1,0:T(8,128)(2,1)S(1)}, bf16[2,512,128]{2,1,0:T(8,128)(2,1)S(1)}, u32[]{:S(2)}, u32[]{:S(2)}) collective-permute-start(bf16[2,512,128]{2,1,0:T(8,128)(2,1)S(1)} %get-tuple-element.52), channel_id=1, source_target_pairs={{0,2},{1,3},{2,0},{3,1},{4,6},{5,7},{6,4},{7,5},{8,10},{9,11},{10,... | collective-permute-start | bytes 786440 | tf_op jit(solution)/shard_map/ppermute | solution.py:35
  231.4 12.4 %collective-permute-start.22 = (bf16[2,512,128]{2,1,0:T(8,128)(2,1)S(1)}, bf16[2,512,128]{2,1,0:T(8,128)(2,1)S(1)}, u32[]{:S(2)}, u32[]{:S(2)}) collective-permute-start(bf16[2,512,128]{2,1,0:T(8,128)(2,1)S(1)} %get-tuple-element.54), channel_id=1, source_target_pairs={{0,8},{4,12},{8,0},{12,4},{16,24},{20,28},{24,16},{28,20},{1,9},{5... | collective-permute-start | bytes 786440 | tf_op jit(solution)/shard_map/ppermute | solution.py:33
  238.3 8.2 %collective-permute-start.32 = (bf16[512,128]{1,0:T(8,128)(2,1)S(1)}, bf16[512,128]{1,0:T(8,128)(2,1)S(1)}, u32[]{:S(2)}, u32[]{:S(2)}) collective-permute-start(bf16[512,128]{1,0:T(8,128)(2,1)S(1)} %get-tuple-element.66), channel_id=1, source_target_pairs={{0,8},{4,12},{8,0},{12,4},{16,24},{20,28},{24,16},{28,20},{1,9},{5... | collective-permute-start | bytes 393224 | tf_op jit(solution)/shard_map/ppermute | solution.py:33
  238.9 7.6 %collective-permute-start.33 = (bf16[512,128]{1,0:T(8,128)(2,1)S(1)}, bf16[512,128]{1,0:T(8,128)(2,1)S(1)}, u32[]{:S(2)}, u32[]{:S(2)}) collective-permute-start(bf16[512,128]{1,0:T(8,128)(2,1)S(1)} %get-tuple-element.68), channel_id=1, source_target_pairs={{0,2},{1,3},{2,0},{3,1},{4,6},{5,7},{6,4},{7,5},{8,10},{9,11},{10,... | collective-permute-start | bytes 393224 | tf_op jit(solution)/shard_map/ppermute | solution.py:35
  243.9 5.0 %collective-permute-start.23 = (bf16[512,128]{1,0:T(8,128)(2,1)S(1)}, bf16[512,128]{1,0:T(8,128)(2,1)S(1)}, u32[]{:S(2)}, u32[]{:S(2)}) collective-permute-start(bf16[512,128]{1,0:T(8,128)(2,1)S(1)} %get-tuple-element.56), channel_id=1, source_target_pairs={{0,8},{4,12},{8,0},{12,4},{16,24},{20,28},{24,16},{28,20},{1,9},{5... | collective-permute-start | bytes 393224 | tf_op jit(solution)/shard_map/ppermute | solution.py:33
  244.5 5.0 %collective-permute-start.24 = (bf16[512,128]{1,0:T(8,128)(2,1)S(1)}, bf16[512,128]{1,0:T(8,128)(2,1)S(1)}, u32[]{:S(2)}, u32[]{:S(2)}) collective-permute-start(bf16[512,128]{1,0:T(8,128)(2,1)S(1)} %get-tuple-element.58), channel_id=1, source_target_pairs={{0,2},{1,3},{2,0},{3,1},{4,6},{5,7},{6,4},{7,5},{8,10},{9,11},{10,... | collective-permute-start | bytes 393224 | tf_op jit(solution)/shard_map/ppermute | solution.py:35
  (2 other events, 1.6 us)

commit v3 on v2

--- a/solution.py
+++ b/solution.py
@@ -88,18 +88,8 @@
     return pl.BlockSpec(memory_space=pltpu.VMEM)
 
 
-def prepare_kernel(
-    which, gates, values_in, queries, keys, values, docs, residual, own, other, halo, *scratch
-):
-    q, k, v, r, gate, value, sems = scratch
-    cols = gate.shape[1]
+def pack_kernel(queries, keys, values, docs, residual, halo, q, k, v, r, sems):
     rows = queries.shape[0]
-    whole = [
-        pltpu.make_async_copy(src, dst, sems.at[4 + i])
-        for i, (src, dst) in enumerate(((gates, gate), (values_in, value)))
-    ]
-    for copy in whole:
-        copy.start()
     copies = [
         pltpu.make_async_copy(src.at[pl.ds(rows - TAIL, TAIL)], dst, sems.at[i])
         for i, (src, dst) in enumerate(((queries, q), (residual, r)))
@@ -118,7 +108,32 @@
         for n in range(0, src.shape[1], LANES):
             halo[at : at + src.shape[0], :] = src[:, n : n + LANES]
             at += src.shape[0]
-    for copy in whole:
+
+
+def packed(queries, keys, values, docs, residual):
+    lines = 4 * HD * WIN // LANES + TAIL + TAIL * (queries.shape[1] + residual.shape[1]) // LANES
+    scratch = [(TAIL, queries.shape[1]), (HD, 2 * WIN), (HD, 2 * WIN), (TAIL, residual.shape[1])]
+    return pl.pallas_call(
+        pack_kernel,
+        in_specs=[hbm(), hbm(), hbm(), vmem(), hbm()],
+        out_specs=vmem(),
+        out_shape=jax.ShapeDtypeStruct((lines, LANES), jnp.bfloat16),
+        scratch_shapes=[pltpu.VMEM(size, jnp.bfloat16) for size in scratch]
+        + [pltpu.SemaphoreType.DMA((4,))],
+        compiler_params=room(56),
+        name="pack",
+    )(queries, keys.T, values.T, docs, residual)
+
+
+def prepare_kernel(which, gates, values, own, other, gate, value, sems):
+    cols = gate.shape[1]
+    copies = [
+        pltpu.make_async_copy(src, dst, sems.at[i])
+        for i, (src, dst) in enumerate(((gates, gate), (values, value)))
+    ]
+    for copy in copies:
+        copy.start()
+    for copy in copies:
         copy.wait()
     half = cols // 2
     main = half // LANES * LANES
@@ -149,21 +164,17 @@
         emit(0, other)
 
 
-def prepared(which, gate, value, queries, keys, values, docs, residual):
+def prepared(which, gate, value):
     shape = jax.ShapeDtypeStruct(gate.shape, gate.dtype)
-    lines = 4 * HD * WIN // LANES + TAIL + TAIL * (queries.shape[1] + residual.shape[1]) // LANES
-    scratch = [(TAIL, queries.shape[1]), (HD, 2 * WIN), (HD, 2 * WIN)]
-    scratch += [(TAIL, residual.shape[1]), gate.shape, gate.shape]
     return pl.pallas_call(
         prepare_kernel,
-        in_specs=[pl.BlockSpec(memory_space=pltpu.SMEM)] + [hbm()] * 5 + [vmem(), hbm()],
-        out_specs=[vmem()] * 3,
-        out_shape=[shape, shape, jax.ShapeDtypeStruct((lines, LANES), jnp.bfloat16)],
-        scratch_shapes=[pltpu.VMEM(size, jnp.bfloat16) for size in scratch]
-        + [pltpu.SemaphoreType.DMA((6,))],
+        in_specs=[pl.BlockSpec(memory_space=pltpu.SMEM), hbm(), hbm()],
+        out_specs=[vmem()] * 2,
+        out_shape=[shape, shape],
+        scratch_shapes=[pltpu.VMEM(gate.shape, gate.dtype)] * 2 + [pltpu.SemaphoreType.DMA((2,))],
         compiler_params=room(56),
         name="prepare",
-    )(which, gate, value, queries, keys.T, values.T, docs, residual)
+    )(which, gate, value)
 
 
 def row_halves_kernel(which, down, own, other, sems):
@@ -514,6 +525,8 @@
 
 def down_kernel(place, near, far, *refs):
     *pieces, keep, send, ws, sems = refs
+    if len(pieces) == 3:
+        pieces.append(None)
     sp, tp = place[0], place[1]
     low, high, core = (sp // 2) % 2, sp // 4, tp % 2
     width = pieces[0].shape[1]
@@ -521,8 +534,13 @@
     for k, piece in enumerate(pieces):
         slot = 2 * (low ^ (k % 2) ^ core) + (high ^ (k // 2))
         dst = ws.at[:, pl.ds(pl.multiple_of(slot * width, width), width)]
-        copies.append(pltpu.make_async_copy(piece, dst, sems.at[k]))
-        copies[-1].start()
+        if piece is not None:
+            copies.append(pltpu.make_async_copy(piece, dst, sems.at[k]))
+            copies[-1].start()
+        else:
+            ws[:, pl.ds(pl.multiple_of(slot * width, width), width)] = jnp.zeros(
+                (ws.shape[0], width), ws.dtype
+            )
     for copy in copies:
         copy.wait()
     for out, base in ((send, 2 * width), (keep, 0)):
@@ -544,12 +562,49 @@
         out_specs=[vmem(), vmem()],
         out_shape=[shape, shape],
         scratch_shapes=[
-            pltpu.VMEM((pieces[0].shape[0], len(pieces) * pieces[0].shape[1]), jnp.bfloat16),
-            pltpu.SemaphoreType.DMA((len(pieces),)),
+            pltpu.VMEM((pieces[0].shape[0], 4 * pieces[0].shape[1]), jnp.bfloat16),
+            pltpu.SemaphoreType.DMA((4,)),
         ],
         compiler_params=room(12),
         name="down_terms",
     )(place, near, far, *pieces)
+
+
+def last_kernel(place, near, far, piece, keep_in, send_in, keep, send, made, sems):
+    sp, tp = place[0], place[1]
+    low, high, core = (sp // 2) % 2, sp // 4, tp % 2
+    for m, hidden in enumerate((near, far)):
+        term = jnp.dot(hidden[...], piece[...], preferred_element_type=jnp.float32)
+        made[m] = term.astype(made.dtype)
+    leaves = low ^ core ^ 1
+
+    @pl.when(leaves == 0)
+    def _():
+        pltpu.make_async_copy(made, keep.at[1 - high], sems.at[0]).start()
+
+    @pl.when(leaves != 0)
+    def _():
+        pltpu.make_async_copy(made, send.at[1 - high], sems.at[0]).start()
+
+    pltpu.make_async_copy(made, keep.at[1 - high], sems.at[0]).wait()
+
+
+def last_terms(place, near, far, piece, keep, send):
+    shape = jax.ShapeDtypeStruct(keep.shape, keep.dtype)
+    anywhere = pl.BlockSpec(memory_space=pl.ANY)
+    return pl.pallas_call(
+        last_kernel,
+        in_specs=[pl.BlockSpec(memory_space=pltpu.SMEM)] + [vmem()] * 3 + [anywhere] * 2,
+        out_specs=[anywhere] * 2,
+        out_shape=[shape, shape],
+        scratch_shapes=[
+            pltpu.VMEM(keep.shape[1:], keep.dtype),
+            pltpu.SemaphoreType.DMA((1,)),
+        ],
+        input_output_aliases={4: 0, 5: 1},
+        compiler_params=room(8),
+        name="last_terms",
+    )(place, near, far, piece, keep, send)
 
 
 def reduced(keep, send, x):
@@ -626,10 +681,9 @@
     low_at, x_at, core_at = one(low), one(x), one(core)
 
     docs_rows = doc_ids.reshape(rows // LANES, LANES)
-    own, other, halo = prepared(
-        low_at, gate_proj, value_proj, query_rows, key_rows, value_rows, docs_rows, residual
-    )
+    halo = packed(query_rows, key_rows, value_rows, docs_rows, residual)
     came_halo = passed_along(halo, "sp", 1)
+    own, other = prepared(low_at, gate_proj, value_proj)
     from_z = [own, swapped(other, 2), swapped(own, 4), swapped(other, 6)]
     up_weights = []
     for piece in from_z:
@@ -672,7 +726,8 @@
     near, far, own_normed = up_hidden(place, near, far, up_weights, taps, share)
     terms = down_terms(place, near, far, down_same)
     ffn_same = reduced(*terms, x_at)
-    terms = down_terms(place, near, far, down_far)
+    terms = down_terms(place, near, far, down_far[:3])
+    terms = last_terms(place, near, far, down_far[3], *terms)
     ffn_far = reduced(*terms, x_at)
     ffn_own = jnp.where(
         y == 0,

time: 258 us -> 260 us (level)
  Pallas kernels: 39.3 us -> 42.4 us
    pallas_call x0 -> x2, Pallas kernels: none -> 4.01 us  [the longest x1 2.18 us: packed(): pl.pallas_call(pack_kernel, in_specs=[hbm(), hbm(), hbm(), vmem(), hbm()]...]
    unnamed x79 -> x75, local copies, waits for them, and re-layouts: 17.6 us -> 16.7 us
  transfers between devices with their start and end apart: 34 -> 34, of which waited for: 17 -> 16; matrix products, arithmetic and copies ran while one was open for 1% -> 1% of each run, Pallas kernels for 10% -> 12%
where the time goes in v3:
time: 260 us; the launch traced here: 259 us
  waiting for transfers between devices  115 us (44%)
  starting transfers between devices  59 us (23%)
  Pallas kernels  42.4 us (16%)
  local copies, waits for them, and re-layouts  19 us (7%)
  other arithmetic  9.83 us (4%)
  matrix products  7.71 us (3%)
  blocking collectives  5.66 us (2%)
    ppermute x19, waiting for transfers between devices, swapped(): return lax.ppermute(block, 'sp', [(i, i ^ sp_mask) for i in range(n_sp)])  100 us
    ppermute x19, starting transfers between devices, swapped(): return lax.ppermute(block, 'sp', [(i, i ^ sp_mask) for i in range(n_sp)])  45.7 us
    unnamed x75, local copies, waits for them, and re-layouts  16.7 us
    pallas_call x1, Pallas kernels, up_hidden(): pl.pallas_call(functools.partial(up_kernel, pieces=len(weights), quarter=...  14.6 us
    ppermute x14, waiting for transfers between devices, swapped(): return lax.ppermute(block, 'tp', [(i, i ^ tp_mask) for i in range(n_tp)])  12.4 us
    ppermute x14, starting transfers between devices, swapped(): return lax.ppermute(block, 'tp', [(i, i ^ tp_mask) for i in range(n_tp)])  8.41 us
    pallas_call x2, Pallas kernels, down_terms(): pl.pallas_call(down_kernel, in_specs=[pl.BlockSpec(memory_space=pltpu.SME...  7.14 us
    psum x1, blocking collectives, paired(): lax.psum((jnp.sum(second_sum, axis=1), jnp.sum(second_sum * second_sum, a...  5.66 us
  transfers between devices with their start and end apart: 34, of which 16 were waited for; matrix products, arithmetic and copies ran while one was open for 1% of the time, Pallas kernels for 12%

profile of v3, /device:TPU:0, one launch (start us, length us, event | category | flops | bytes accessed | tf_op | source)
XLA Modules:
  0.0 258.8 jit_solution(13573613678700452937)
XLA Ops:
  0.0 2.2 pack.1
  2.2 4.9 %collective-permute-start = (bf16[424,128]{1,0:T(8,128)(2,1)}, bf16[424,128]{1,0:T(8,128)(2,1)S(1)}, u32[]{:S(2)}, u32[]{:S(2)}) collective-permute-start(bf16[424,128]{1,0:T(8,128)(2,1)} %pack.1), channel_id=1, source_target_pairs={{0,4},{4,8},{8,12},{12,16},{16,20},{20,24},{24,28},{1,5},{5,9},{9,... | collective-permute-start | bytes 325640 | tf_op jit(solution)/shard_map/ppermute | solution.py:27
  7.2 0.7 pad_add_fusion.2.place
  7.8 1.9 collective-permute-done
  9.9 1.1 pad_maximum_fusion
  11.4 0.8 pad_add_fusion
  12.8 3.6 %fusion.1 = (f32[8,520]{1,0:T(8,128)S(1)}, f32[648,520,8]{0,1,2:T(8,128)S(1)}) fusion(pred[520,648]{1,0:T(8,128)(4,1)S(1)} %fusion.6, bf16[520,8,64]{0,2,1:T(8,128)(2,1)S(1)} %bitcast.45, bf16[64,128]{1,0:T(8,128)(2,1)S(1)} %get-tuple-element.82, bf16[64,128]{1,0:T(8,128)(2,1)S(1)} %get-tuple-element.83, bf16[64,512]{1,0:T(8,128)(2,1)} %bitcast.48), kind=kOutput, calls=%fused_computation.4 | convolution fusion | flops 353378752 | bytes 11767104 | tf_op jit(solution)/shard_map/qkgd,skd->kgqs/dot_general | solution.py:46
  16.4 3.7 %fusion = f32[8,520]{1,0:T(8,128)S(1)} fusion(f32[648,520,8]{0,1,2:T(8,128)S(1)} %get-tuple-element.90, f32[8,520]{1,0:T(8,128)S(1)} %broadcast_maximum_fusion, pred[520,648]{1,0:T(8,128)(4,1)S(1)} %fusion.6), kind=kLoop, calls=%fused_computation.3 | loop fusion | flops 10778560 | bytes 11152960 | tf_op jit(solution)/shard_map/reduce_sum | solution.py:59
  20.2 4.1 %fusion.7 = bf16[64,8,520]{2,0,1:T(8,128)(2,1)S(1)} fusion(f32[8,520]{1,0:T(8,128)S(1)} %exponential_add_fusion, f32[8,520]{1,0:T(8,128)S(1)} %broadcast_maximum_fusion, f32[648,520,8]{0,1,2:T(8,128)S(1)} %get-tuple-element.90, pred[520,648]{1,0:T(8,128)(4,1)S(1)} %fusion.6, bf16[64,128]{1,0:T(8,128)(2,1)S(1)} %get-tuple-element.84, ...), kind=kOutput, calls=%fused_computation.12 | convolution fusion | flops 359040512 | bytes 11783744 | tf_op jit(solution)/shard_map/kgqs,skd->qkgd/dot_general | solution.py:61
  24.4 1.0 copy.20.heads
  25.5 4.7 %project.1 = (bf16[2,136,2048]{2,1,0:T(8,128)(2,1)}, bf16[2,136,2048]{2,1,0:T(8,128)(2,1)}) custom-call(s32[2]{0:T(128)} %pad_add_fusion.2.place, bf16[520,512]{1,0:T(8,128)(2,1)} %copy.20.heads, bf16[512,2048]{1,0:T(8,128)(2,1)} %weights.1), custom_call_target="tpu_custom_call" | custom-call | tf_op jit(solution)/shard_map/project/pallas_call | solution.py:400
  30.3 2.9 %collective-permute-done.1.second = bf16[2,136,2048]{2,1,0:T(8,128)(2,1)S(1)} collective-permute-done((bf16[2,136,2048]{2,1,0:T(8,128)(2,1)}, bf16[2,136,2048]{2,1,0:T(8,128)(2,1)S(1)}, u32[]{:S(2)}, u32[]{:S(2)}) %collective-permute-start.1) | collective-permute-done | bytes 1114144 | tf_op jit(solution)/shard_map/ppermute | solution.py:35
  33.3 1.0 copy-done.21
  34.2 2.7 %merge.1 = (bf16[136,2048]{1,0:T(8,128)(2,1)}, bf16[136,2048]{1,0:T(8,128)(2,1)}) custom-call(s32[1]{0:T(128)} %bitcast.2.which, bf16[2,136,2048]{2,1,0:T(8,128)(2,1)} %get-tuple-element.38.first, bf16[2,136,2048]{2,1,0:T(8,128)(2,1)} %copy-done.21), custom_call_target="tpu_custom_call" | custom-call | tf_op jit(solution)/shard_map/merge/pallas_call | solution.py:425
  37.0 1.5 collective-permute-start.2
  38.4 2.0 row_halves.1
  40.4 3.4 %collective-permute-start.17 = (bf16[704,256]{1,0:T(8,128)(2,1)}, bf16[704,256]{1,0:T(8,128)(2,1)}, u32[]{:S(2)}, u32[]{:S(2)}) collective-permute-start(bf16[704,256]{1,0:T(8,128)(2,1)} %get-tuple-element.48), channel_id=1, source_target_pairs={{0,8},{4,12},{8,0},{12,4},{16,24},{20,28},{24,16},{28,20},{1,9},{5... | collective-permute-start | bytes 1081352 | tf_op jit(solution)/shard_map/ppermute | solution.py:33
  43.8 2.6 collective-permute-start.18
  46.4 2.9 %prepare.1 = (bf16[256,1408]{1,0:T(8,128)(2,1)}, bf16[256,1408]{1,0:T(8,128)(2,1)}) custom-call(s32[1]{0:T(128)} %bitcast.17.which, bf16[256,1408]{1,0:T(8,128)(2,1)} %gates.1, bf16[256,1408]{1,0:T(8,128)(2,1)} %values.1), custom_call_target="tpu_custom_call" | custom-call | tf_op jit(solution)/shard_map/prepare/pallas_call | solution.py:169
  49.8 11.2 %collective-permute-done.17.refs_1_ = bf16[704,256]{1,0:T(8,128)(2,1)} collective-permute-done((bf16[704,256]{1,0:T(8,128)(2,1)}, bf16[704,256]{1,0:T(8,128)(2,1)}, u32[]{:S(2)}, u32[]{:S(2)}) %collective-permute-start.17) | collective-permute-done | bytes 360480 | tf_op jit(solution)/shard_map/ppermute | solution.py:33
  61.0 3.9 %collective-permute-start.15 = (bf16[256,1408]{1,0:T(8,128)(2,1)}, bf16[256,1408]{1,0:T(8,128)(2,1)S(1)}, u32[]{:S(2)}, u32[]{:S(2)}) collective-permute-start(bf16[256,1408]{1,0:T(8,128)(2,1)} %get-tuple-element.43), channel_id=1, source_target_pairs={{0,24},{4,28},{8,16},{12,20},{16,8},{20,12},{24,0},{28,4},{1,25},{... | collective-permute-start | bytes 2162696 | tf_op jit(solution)/shard_map/ppermute | solution.py:33
  65.0 1.5 collective-permute-start.19
  66.6 0.7 collective-permute-start.10
  68.0 3.6 %normed_rows.1.refs_0_ = bf16[136,2048]{1,0:T(8,128)(2,1)} custom-call(s32[2]{0:T(128)} %pad_add_fusion.2.place, bf16[136,2048]{1,0:T(8,128)(2,1)} %get-tuple-element.40.first, bf16[136,2048]{1,0:T(8,128)(2,1)} %copy-done.22, bf16[512,2048]{1,0:T(8,128)(2,1)} %residual.3, bf16[8,2048]{1,0:T(8,128)(2,1)} %copy-done.24, f32[1,2048]{1,0:T(1,128)} %bitcast.52, ...), custom_call_target="tpu_custom_call" | custom-call | tf_op jit(solution)/shard_map/normed_rows/pallas_call | solution.py:515
  71.7 45.0 %collective-permute-done.19.refs_3_ = bf16[704,256]{1,0:T(8,128)(2,1)} collective-permute-done((bf16[704,256]{1,0:T(8,128)(2,1)}, bf16[704,256]{1,0:T(8,128)(2,1)}, u32[]{:S(2)}, u32[]{:S(2)}) %collective-permute-start.19) | collective-permute-done | bytes 360480 | tf_op jit(solution)/shard_map/ppermute | solution.py:33
  116.7 23.8 %collective-permute-start.6 = (bf16[136,2048]{1,0:T(8,128)(2,1)}, bf16[136,2048]{1,0:T(8,128)(2,1)S(1)}, u32[]{:S(2)}, u32[]{:S(2)}) collective-permute-start(bf16[136,2048]{1,0:T(8,128)(2,1)} %normed_rows.1.refs_0_), channel_id=1, source_target_pairs={{0,8},{4,12},{8,0},{12,4},{16,24},{20,28},{24,16},{28,20},{1,9},{5... | collective-permute-start | bytes 1671176 | tf_op jit(solution)/shard_map/ppermute | solution.py:33
  141.2 1.4 collective-permute-start.14
  143.1 9.2 %collective-permute-done.6.refs_4_ = bf16[136,2048]{1,0:T(8,128)(2,1)S(1)} collective-permute-done((bf16[136,2048]{1,0:T(8,128)(2,1)}, bf16[136,2048]{1,0:T(8,128)(2,1)S(1)}, u32[]{:S(2)}, u32[]{:S(2)}) %collective-permute-start.6) | collective-permute-done | bytes 557088 | tf_op jit(solution)/shard_map/ppermute | solution.py:33
  153.5 6.1 %collective-permute-done.12.refs_11_ = bf16[256,1408]{1,0:T(8,128)(2,1)S(1)} collective-permute-done((bf16[256,1408]{1,0:T(8,128)(2,1)S(1)}, bf16[256,1408]{1,0:T(8,128)(2,1)S(1)}, u32[]{:S(2)}, u32[]{:S(2)}) %collective-permute-start.12) | collective-permute-done | bytes 720928 | tf_op jit(solution)/shard_map/ppermute | solution.py:33
  159.6 0.9 copy-done.2
  160.9 0.8 copy-done.8
  161.7 13.3 %collective-permute-done.14.refs_13_ = bf16[256,1408]{1,0:T(8,128)(2,1)S(1)} collective-permute-done((bf16[256,1408]{1,0:T(8,128)(2,1)S(1)}, bf16[256,1408]{1,0:T(8,128)(2,1)S(1)}, u32[]{:S(2)}, u32[]{:S(2)}) %collective-permute-start.14) | collective-permute-done | bytes 720928 | tf_op jit(solution)/shard_map/ppermute | solution.py:33
  175.0 0.9 copy-done.4
  176.4 11.6 %collective-permute-done.16.refs_15_ = bf16[256,1408]{1,0:T(8,128)(2,1)S(1)} collective-permute-done((bf16[256,1408]{1,0:T(8,128)(2,1)S(1)}, bf16[256,1408]{1,0:T(8,128)(2,1)S(1)}, u32[]{:S(2)}, u32[]{:S(2)}) %collective-permute-start.16) | collective-permute-done | bytes 720928 | tf_op jit(solution)/shard_map/ppermute | solution.py:33
  188.0 0.9 copy-done.6
  189.5 0.8 copy-done.10
  190.3 1.4 collective-permute-start.27
  191.7 0.8 copy-done.12
  193.1 0.8 copy-done.14
  193.9 1.4 collective-permute-start.25
  195.6 1.0 copy-done
  196.7 1.1 copy-done.1
  197.8 1.1 copy-done.3
  198.9 1.1 copy-done.5
  200.0 1.1 copy-done.7
  201.1 1.1 copy-done.9
  202.2 1.1 copy-done.11
  203.2 1.1 copy-done.13
  204.3 1.1 copy-done.15
  205.3 14.6 %up_hidden.1 = (bf16[512,704]{1,0:T(8,128)(2,1)S(1)}, bf16[512,704]{1,0:T(8,128)(2,1)S(1)}, bf16[512,512]{1,0:T(8,128)(2,1)S(1)}) custom-call(s32[2]{0:T(128)S(1)} %copy-done.20, bf16[136,2048]{1,0:T(8,128)(2,1)S(1)} %copy-done, bf16[136,2048]{1,0:T(8,128)(2,1)S(1)} %copy-done.9, bf16[136,2048]{1,0:T(8,128)(2,1)S(1)} %copy-done.11, ...), custom_call_target="tpu_custom_call" | custom-call | tf_op jit(solution)/shard_map/up_hidden/pallas_call | solution.py:341
  220.0 3.6 %down_terms.3 = (bf16[2,2,512,256]{3,2,1,0:T(8,128)(2,1)S(1)}, bf16[2,2,512,256]{3,2,1,0:T(8,128)(2,1)S(1)}) custom-call(s32[2]{0:T(128)S(1)} %copy-done.20, bf16[512,704]{1,0:T(8,128)(2,1)S(1)} %get-tuple-element.45.near, bf16[512,704]{1,0:T(8,128)(2,1)S(1)} %get-tuple-element.46.far, bf16[704,256]{1,0:T(8,128)(2,1)} %collective-permute-done.26.refs_0_, ...), custom_call_target="tpu_custom_call" | custom-call | tf_op jit(solution)/shard_map/down_terms/pallas_call | solution.py:559
  223.6 1.8 last_terms.1
  225.5 3.5 %down_terms.2 = (bf16[2,2,512,256]{3,2,1,0:T(8,128)(2,1)S(1)}, bf16[2,2,512,256]{3,2,1,0:T(8,128)(2,1)S(1)}) custom-call(s32[2]{0:T(128)S(1)} %copy-done.20, bf16[512,704]{1,0:T(8,128)(2,1)S(1)} %get-tuple-element.45.near, bf16[512,704]{1,0:T(8,128)(2,1)S(1)} %get-tuple-element.46.far, bf16[704,256]{1,0:T(8,128)(2,1)S(1)} %copy-done.17, ...), custom_call_target="tpu_custom_call" | custom-call | tf_op jit(solution)/shard_map/down_terms/pallas_call | solution.py:559
  230.7 1.2 collective-permute-done.20.second
  232.7 1.6 collective-permute-start.22
  234.3 4.8 %collective-permute-done.30.came_a = bf16[2,512,128]{2,1,0:T(8,128)(2,1)S(1)} collective-permute-done((bf16[2,512,128]{2,1,0:T(8,128)(2,1)S(1)}, bf16[2,512,128]{2,1,0:T(8,128)(2,1)S(1)}, u32[]{:S(2)}, u32[]{:S(2)}) %collective-permute-start.30) | collective-permute-done | bytes 262176 | tf_op jit(solution)/shard_map/ppermute | solution.py:35
  240.1 1.5 collective-permute-start.33
  241.6 3.1 %collective-permute-done.21.came_a = bf16[2,512,128]{2,1,0:T(8,128)(2,1)S(1)} collective-permute-done((bf16[2,512,128]{2,1,0:T(8,128)(2,1)S(1)}, bf16[2,512,128]{2,1,0:T(8,128)(2,1)S(1)}, u32[]{:S(2)}, u32[]{:S(2)}) %collective-permute-start.21) | collective-permute-done | bytes 262176 | tf_op jit(solution)/shard_map/ppermute | solution.py:35
  245.7 1.5 collective-permute-start.24
  247.2 0.6 collective-permute-done.32
  248.0 2.4 collective-permute-done.23
  250.7 1.4 fusion.28
  252.1 5.7 %all-reduce.2 = (f32[512]{0:T(512)S(1)}, f32[512]{0:T(512)S(1)}) all-reduce(f32[512]{0:T(512)S(1)} %get-tuple-element.72, f32[512]{0:T(512)S(1)} %get-tuple-element.71), channel_id=1, replica_groups=mesh['sp'=8,'tp'=4] {'tp'}, use_global_device_ids=true, to_apply=%region_5.6 | all-reduce | flops 1024 | bytes 8192 | tf_op jit(solution)/shard_map/psum | solution.py:738
  257.7 1.0 multiply_convert_fusion
  (135 shorter events, 12.5 us)
Async XLA Ops:
  2.2 7.5 %collective-permute-start = (bf16[424,128]{1,0:T(8,128)(2,1)}, bf16[424,128]{1,0:T(8,128)(2,1)S(1)}, u32[]{:S(2)}, u32[]{:S(2)}) collective-permute-start(bf16[424,128]{1,0:T(8,128)(2,1)} %pack.1), channel_id=1, source_target_pairs={{0,4},{4,8},{8,12},{12,16},{16,20},{20,24},{24,28},{1,5},{5,9},{9,... | collective-permute-start | bytes 325640 | tf_op jit(solution)/shard_map/ppermute | solution.py:27
  9.9 6.5 %copy-start.24 = (bf16[8,2048]{1,0:T(8,128)(2,1)}, bf16[8,2048]{1,0:T(8,128)(2,1)S(1)}, u32[]{:S(2)}) copy-start(bf16[8,2048]{1,0:T(8,128)(2,1)S(1)} %get-tuple-element.76.before) | copy-start | bytes 98308
  12.8 3.6 %copy-start.29 = (f32[8]{0:T(128)S(1)}, f32[8]{0:T(128)}, u32[]{:S(2)}) copy-start(f32[8]{0:T(128)} %param.18) | copy-start | bytes 100
  16.4 3.8 %copy-start.23 = (bf16[512,64]{0,1:T(8,128)(2,1)S(1)}, bf16[512,64]{0,1:T(8,128)(2,1)}, u32[]{:S(2)}) copy-start(bf16[512,64]{0,1:T(8,128)(2,1)} %param.16) | copy-start | bytes 196612
  24.4 42.1 %copy-start.25 = (s32[512]{0:T(512)S(1)}, s32[512]{0:T(512)}, u32[]{:S(2)}) copy-start(s32[512]{0:T(512)} %param.17) | copy-start | bytes 6148
  24.4 170.9 %copy-start.26 = (f32[3,1408]{1,0:T(4,128)S(1)}, f32[3,1408]{1,0:T(4,128)}, u32[]{:S(2)}) copy-start(f32[3,1408]{1,0:T(4,128)} %param.25) | copy-start | bytes 50692
  24.4 170.9 %copy-start.27 = (f32[3,1408]{1,0:T(4,128)S(1)}, f32[3,1408]{1,0:T(4,128)}, u32[]{:S(2)}) copy-start(f32[3,1408]{1,0:T(4,128)} %param.24) | copy-start | bytes 50692
  24.4 171.2 %copy-start.20 = (s32[2]{0:T(128)S(1)}, s32[2]{0:T(128)}, u32[]{:S(2)}) copy-start(s32[2]{0:T(128)} %pad_add_fusion.2.place) | copy-start | bytes 28
  30.2 3.0 %collective-permute-start.1 = (bf16[2,136,2048]{2,1,0:T(8,128)(2,1)}, bf16[2,136,2048]{2,1,0:T(8,128)(2,1)S(1)}, u32[]{:S(2)}, u32[]{:S(2)}) collective-permute-start(bf16[2,136,2048]{2,1,0:T(8,128)(2,1)} %get-tuple-element.39), channel_id=1, source_target_pairs={{0,1},{1,0},{2,3},{3,2},{4,5},{5,4},{6,7},{7,6},{8,9},{9,8},{10,11... | collective-permute-start | bytes 3342344 | tf_op jit(solution)/shard_map/ppermute | solution.py:35
  33.3 1.0 copy-start.21
  37.0 29.6 %collective-permute-start.2 = (bf16[136,2048]{1,0:T(8,128)(2,1)}, bf16[136,2048]{1,0:T(8,128)(2,1)S(1)}, u32[]{:S(2)}, u32[]{:S(2)}) collective-permute-start(bf16[136,2048]{1,0:T(8,128)(2,1)} %get-tuple-element.41), channel_id=1, source_target_pairs={{0,2},{1,3},{2,0},{3,1},{4,6},{5,7},{6,4},{7,5},{8,10},{9,11},{10,... | collective-permute-start | bytes 1671176 | tf_op jit(solution)/shard_map/ppermute | solution.py:35
  40.4 20.6 %collective-permute-start.17 = (bf16[704,256]{1,0:T(8,128)(2,1)}, bf16[704,256]{1,0:T(8,128)(2,1)}, u32[]{:S(2)}, u32[]{:S(2)}) collective-permute-start(bf16[704,256]{1,0:T(8,128)(2,1)} %get-tuple-element.48), channel_id=1, source_target_pairs={{0,8},{4,12},{8,0},{12,4},{16,24},{20,28},{24,16},{28,20},{1,9},{5... | collective-permute-start | bytes 1081352 | tf_op jit(solution)/shard_map/ppermute | solution.py:33
  43.8 21.2 %collective-permute-start.18 = (bf16[704,256]{1,0:T(8,128)(2,1)}, bf16[704,256]{1,0:T(8,128)(2,1)S(1)}, u32[]{:S(2)}, u32[]{:S(2)}) collective-permute-start(bf16[704,256]{1,0:T(8,128)(2,1)} %get-tuple-element.47.refs_0_), channel_id=1, source_target_pairs={{0,16},{4,20},{8,24},{12,28},{16,0},{20,4},{24,8},{28,12},{1,17},{... | collective-permute-start | bytes 1081352 | tf_op jit(solution)/shard_map/ppermute | solution.py:33
  49.3 91.2 %collective-permute-start.11 = (bf16[256,1408]{1,0:T(8,128)(2,1)}, bf16[256,1408]{1,0:T(8,128)(2,1)S(1)}, u32[]{:S(2)}, u32[]{:S(2)}) collective-permute-start(bf16[256,1408]{1,0:T(8,128)(2,1)} %get-tuple-element.43), channel_id=1, source_target_pairs={{0,8},{4,12},{8,0},{12,4},{16,24},{20,28},{24,16},{28,20},{1,9},{5... | collective-permute-start | bytes 2162696 | tf_op jit(solution)/shard_map/ppermute | solution.py:33
  49.8 91.3 %collective-permute-start.13 = (bf16[256,1408]{1,0:T(8,128)(2,1)}, bf16[256,1408]{1,0:T(8,128)(2,1)S(1)}, u32[]{:S(2)}, u32[]{:S(2)}) collective-permute-start(bf16[256,1408]{1,0:T(8,128)(2,1)} %get-tuple-element.42.refs_8_), channel_id=1, source_target_pairs={{0,16},{4,20},{8,24},{12,28},{16,0},{20,4},{24,8},{28,12},{1,17},{... | collective-permute-start | bytes 2162696 | tf_op jit(solution)/shard_map/ppermute | solution.py:33
  61.0 81.6 %collective-permute-start.15 = (bf16[256,1408]{1,0:T(8,128)(2,1)}, bf16[256,1408]{1,0:T(8,128)(2,1)S(1)}, u32[]{:S(2)}, u32[]{:S(2)}) collective-permute-start(bf16[256,1408]{1,0:T(8,128)(2,1)} %get-tuple-element.43), channel_id=1, source_target_pairs={{0,24},{4,28},{8,16},{12,20},{16,8},{20,12},{24,0},{28,4},{1,25},{... | collective-permute-start | bytes 2162696 | tf_op jit(solution)/shard_map/ppermute | solution.py:33
  65.0 1.6 copy-start.18
  65.0 51.7 %collective-permute-start.19 = (bf16[704,256]{1,0:T(8,128)(2,1)}, bf16[704,256]{1,0:T(8,128)(2,1)}, u32[]{:S(2)}, u32[]{:S(2)}) collective-permute-start(bf16[704,256]{1,0:T(8,128)(2,1)} %get-tuple-element.48), channel_id=1, source_target_pairs={{0,24},{4,28},{8,16},{12,20},{16,8},{20,12},{24,0},{28,4},{1,25},{... | collective-permute-start | bytes 1081352 | tf_op jit(solution)/shard_map/ppermute | solution.py:33
  66.6 1.4 copy-start.22
  66.6 86.2 %collective-permute-start.10 = (bf16[256,1408]{1,0:T(8,128)(2,1)}, bf16[256,1408]{1,0:T(8,128)(2,1)S(1)}, u32[]{:S(2)}, u32[]{:S(2)}) collective-permute-start(bf16[256,1408]{1,0:T(8,128)(2,1)} %get-tuple-element.42.refs_8_), channel_id=1, source_target_pairs={{0,4},{4,0},{8,12},{12,8},{16,20},{20,16},{24,28},{28,24},{1,5},{5... | collective-permute-start | bytes 2162696 | tf_op jit(solution)/shard_map/ppermute | solution.py:33
  116.7 35.6 %collective-permute-start.6 = (bf16[136,2048]{1,0:T(8,128)(2,1)}, bf16[136,2048]{1,0:T(8,128)(2,1)S(1)}, u32[]{:S(2)}, u32[]{:S(2)}) collective-permute-start(bf16[136,2048]{1,0:T(8,128)(2,1)} %normed_rows.1.refs_0_), channel_id=1, source_target_pairs={{0,8},{4,12},{8,0},{12,4},{16,24},{20,28},{24,16},{28,20},{1,9},{5... | collective-permute-start | bytes 1671176 | tf_op jit(solution)/shard_map/ppermute | solution.py:33
  140.5 19.0 %collective-permute-start.12 = (bf16[256,1408]{1,0:T(8,128)(2,1)S(1)}, bf16[256,1408]{1,0:T(8,128)(2,1)S(1)}, u32[]{:S(2)}, u32[]{:S(2)}) collective-permute-start(bf16[256,1408]{1,0:T(8,128)(2,1)S(1)} %collective-permute-done.11.refs_10_), channel_id=1, source_target_pairs={{0,4},{4,0},{8,12},{12,8},{16,20},{20,16},{24,28},{28,24},{1,5},{5... | collective-permute-start | bytes 2162696 | tf_op jit(solution)/shard_map/ppermute | solution.py:33
  141.2 33.8 %collective-permute-start.14 = (bf16[256,1408]{1,0:T(8,128)(2,1)S(1)}, bf16[256,1408]{1,0:T(8,128)(2,1)S(1)}, u32[]{:S(2)}, u32[]{:S(2)}) collective-permute-start(bf16[256,1408]{1,0:T(8,128)(2,1)S(1)} %collective-permute-done.13.refs_12_), channel_id=1, source_target_pairs={{0,4},{4,0},{8,12},{12,8},{16,20},{20,16},{24,28},{28,24},{1,5},{5... | collective-permute-start | bytes 2162696 | tf_op jit(solution)/shard_map/ppermute | solution.py:33
  142.6 17.8 %collective-permute-start.3 = (bf16[136,2048]{1,0:T(8,128)(2,1)}, bf16[136,2048]{1,0:T(8,128)(2,1)S(1)}, u32[]{:S(2)}, u32[]{:S(2)}) collective-permute-start(bf16[136,2048]{1,0:T(8,128)(2,1)} %normed_rows.1.refs_0_), channel_id=1, source_target_pairs={{0,2},{1,3},{2,0},{3,1},{4,6},{5,7},{6,4},{7,5},{8,10},{9,11},{10,... | collective-permute-start | bytes 1671176 | tf_op jit(solution)/shard_map/ppermute | solution.py:35
  152.3 23.6 %collective-permute-start.7 = (bf16[136,2048]{1,0:T(8,128)(2,1)S(1)}, bf16[136,2048]{1,0:T(8,128)(2,1)}, u32[]{:S(2)}, u32[]{:S(2)}) collective-permute-start(bf16[136,2048]{1,0:T(8,128)(2,1)S(1)} %collective-permute-done.6.refs_4_), channel_id=1, source_target_pairs={{0,2},{1,3},{2,0},{3,1},{4,6},{5,7},{6,4},{7,5},{8,10},{9,11},{10,... | collective-permute-start | bytes 1671176 | tf_op jit(solution)/shard_map/ppermute | solution.py:35
  152.8 35.1 %collective-permute-start.16 = (bf16[256,1408]{1,0:T(8,128)(2,1)S(1)}, bf16[256,1408]{1,0:T(8,128)(2,1)S(1)}, u32[]{:S(2)}, u32[]{:S(2)}) collective-permute-start(bf16[256,1408]{1,0:T(8,128)(2,1)S(1)} %collective-permute-done.15.refs_14_), channel_id=1, source_target_pairs={{0,4},{4,0},{8,12},{12,8},{16,20},{20,16},{24,28},{28,24},{1,5},{5... | collective-permute-start | bytes 2162696 | tf_op jit(solution)/shard_map/ppermute | solution.py:33
  159.6 0.9 copy-start.2
  160.4 29.0 %collective-permute-start.4 = (bf16[136,2048]{1,0:T(8,128)(2,1)}, bf16[136,2048]{1,0:T(8,128)(2,1)S(1)}, u32[]{:S(2)}, u32[]{:S(2)}) collective-permute-start(bf16[136,2048]{1,0:T(8,128)(2,1)} %normed_rows.1.refs_0_), channel_id=1, source_target_pairs={{0,1},{1,0},{2,3},{3,2},{4,5},{5,4},{6,7},{7,6},{8,9},{9,8},{10,11... | collective-permute-start | bytes 1671176 | tf_op jit(solution)/shard_map/ppermute | solution.py:35
  160.4 31.3 %collective-permute-start.5 = (bf16[136,2048]{1,0:T(8,128)(2,1)S(1)}, bf16[136,2048]{1,0:T(8,128)(2,1)S(1)}, u32[]{:S(2)}, u32[]{:S(2)}) collective-permute-start(bf16[136,2048]{1,0:T(8,128)(2,1)S(1)} %collective-permute-done.3.refs_1_), channel_id=1, source_target_pairs={{0,1},{1,0},{2,3},{3,2},{4,5},{5,4},{6,7},{7,6},{8,9},{9,8},{10,11... | collective-permute-start | bytes 1671176 | tf_op jit(solution)/shard_map/ppermute | solution.py:35
  160.9 0.8 copy-start.8
  175.0 0.9 copy-start.4
  175.9 17.2 %collective-permute-start.8 = (bf16[136,2048]{1,0:T(8,128)(2,1)S(1)}, bf16[136,2048]{1,0:T(8,128)(2,1)S(1)}, u32[]{:S(2)}, u32[]{:S(2)}) collective-permute-start(bf16[136,2048]{1,0:T(8,128)(2,1)S(1)} %collective-permute-done.6.refs_4_), channel_id=1, source_target_pairs={{0,1},{1,0},{2,3},{3,2},{4,5},{5,4},{6,7},{7,6},{8,9},{9,8},{10,11... | collective-permute-start | bytes 1671176 | tf_op jit(solution)/shard_map/ppermute | solution.py:35
  175.9 19.7 %collective-permute-start.9 = (bf16[136,2048]{1,0:T(8,128)(2,1)}, bf16[136,2048]{1,0:T(8,128)(2,1)}, u32[]{:S(2)}, u32[]{:S(2)}) collective-permute-start(bf16[136,2048]{1,0:T(8,128)(2,1)} %collective-permute-done.7.refs_5_), channel_id=1, source_target_pairs={{0,1},{1,0},{2,3},{3,2},{4,5},{5,4},{6,7},{7,6},{8,9},{9,8},{10,11... | collective-permute-start | bytes 1671176 | tf_op jit(solution)/shard_map/ppermute | solution.py:35
  188.0 0.9 copy-start.6
  188.8 31.1 %collective-permute-start.26 = (bf16[704,256]{1,0:T(8,128)(2,1)}, bf16[704,256]{1,0:T(8,128)(2,1)}, u32[]{:S(2)}, u32[]{:S(2)}) collective-permute-start(bf16[704,256]{1,0:T(8,128)(2,1)} %get-tuple-element.47.refs_0_), channel_id=1, source_target_pairs={{0,4},{4,0},{8,12},{12,8},{16,20},{20,16},{24,28},{28,24},{1,5},{5... | collective-permute-start | bytes 1081352 | tf_op jit(solution)/shard_map/ppermute | solution.py:33
  189.5 0.8 copy-start.10
  190.3 29.7 %collective-permute-start.27 = (bf16[704,256]{1,0:T(8,128)(2,1)}, bf16[704,256]{1,0:T(8,128)(2,1)}, u32[]{:S(2)}, u32[]{:S(2)}) collective-permute-start(bf16[704,256]{1,0:T(8,128)(2,1)} %collective-permute-done.17.refs_1_), channel_id=1, source_target_pairs={{0,4},{4,0},{8,12},{12,8},{16,20},{20,16},{24,28},{28,24},{1,5},{5... | collective-permute-start | bytes 1081352 | tf_op jit(solution)/shard_map/ppermute | solution.py:33
  191.7 0.8 copy-start.12
  192.5 27.5 %collective-permute-start.28 = (bf16[704,256]{1,0:T(8,128)(2,1)}, bf16[704,256]{1,0:T(8,128)(2,1)}, u32[]{:S(2)}, u32[]{:S(2)}) collective-permute-start(bf16[704,256]{1,0:T(8,128)(2,1)} %copy-done.18), channel_id=1, source_target_pairs={{0,4},{4,0},{8,12},{12,8},{16,20},{20,16},{24,28},{28,24},{1,5},{5... | collective-permute-start | bytes 1081352 | tf_op jit(solution)/shard_map/ppermute | solution.py:33
  193.1 0.8 copy-start.14
  193.9 29.7 %collective-permute-start.25 = (bf16[704,256]{1,0:T(8,128)(2,1)}, bf16[704,256]{1,0:T(8,128)(2,1)}, u32[]{:S(2)}, u32[]{:S(2)}) collective-permute-start(bf16[704,256]{1,0:T(8,128)(2,1)} %collective-permute-done.19.refs_3_), channel_id=1, source_target_pairs={{0,4},{4,0},{8,12},{12,8},{16,20},{20,16},{24,28},{28,24},{1,5},{5... | collective-permute-start | bytes 1081352 | tf_op jit(solution)/shard_map/ppermute | solution.py:33
  195.6 1.1 copy-start
  196.7 1.1 copy-start.1
  197.8 1.1 copy-start.3
  198.9 1.1 copy-start.5
  200.0 1.1 copy-start.7
  201.1 1.1 copy-start.9
  202.2 1.1 copy-start.11
  203.2 1.1 copy-start.13
  204.3 1.1 copy-start.15
  205.3 20.2 %copy-start.17 = (bf16[704,256]{1,0:T(8,128)(2,1)S(1)}, bf16[704,256]{1,0:T(8,128)(2,1)}, u32[]{:S(2)}) copy-start(bf16[704,256]{1,0:T(8,128)(2,1)} %get-tuple-element.47.refs_0_) | copy-start | bytes 1081348
  205.3 20.2 %copy-start.19 = (bf16[704,256]{1,0:T(8,128)(2,1)S(1)}, bf16[704,256]{1,0:T(8,128)(2,1)}, u32[]{:S(2)}) copy-start(bf16[704,256]{1,0:T(8,128)(2,1)} %copy-done.18) | copy-start | bytes 1081348
  219.9 12.2 %copy-start.16 = (bf16[512,512]{1,0:T(8,128)(2,1)}, bf16[512,512]{1,0:T(8,128)(2,1)S(1)}, u32[]{:S(2)}) copy-start(bf16[512,512]{1,0:T(8,128)(2,1)S(1)} %get-tuple-element.44) | copy-start | bytes 1572868
  225.4 32.3 %copy-start.28 = (f32[512]{0:T(512)S(1)}, f32[512]{0:T(512)}, u32[]{:S(2)}) copy-start(f32[512]{0:T(512)} %param.27) | copy-start | bytes 6148
  225.4 4.2 %collective-permute-start.29 = (bf16[2,2,512,256]{3,2,1,0:T(8,128)(2,1)S(1)}, bf16[2,2,512,256]{3,2,1,0:T(8,128)(2,1)S(1)}, u32[]{:S(2)}, u32[]{:S(2)}) collective-permute-start(bf16[2,2,512,256]{3,2,1,0:T(8,128)(2,1)S(1)} %get-tuple-element.62), channel_id=1, source_target_pairs={{0,1},{1,0},{2,3},{3,2},{4,5},{5,4},{6,7},{7,6},{8,9},{9,8},{10,11... | collective-permute-start | bytes 3145736 | tf_op jit(solution)/shard_map/ppermute | solution.py:35
  229.1 2.8 %collective-permute-start.20 = (bf16[2,2,512,256]{3,2,1,0:T(8,128)(2,1)S(1)}, bf16[2,2,512,256]{3,2,1,0:T(8,128)(2,1)S(1)}, u32[]{:S(2)}, u32[]{:S(2)}) collective-permute-start(bf16[2,2,512,256]{3,2,1,0:T(8,128)(2,1)S(1)} %get-tuple-element.50), channel_id=1, source_target_pairs={{0,1},{1,0},{2,3},{3,2},{4,5},{5,4},{6,7},{7,6},{8,9},{9,8},{10,11... | collective-permute-start | bytes 3145736 | tf_op jit(solution)/shard_map/ppermute | solution.py:35
  229.9 9.2 %collective-permute-start.30 = (bf16[2,512,128]{2,1,0:T(8,128)(2,1)S(1)}, bf16[2,512,128]{2,1,0:T(8,128)(2,1)S(1)}, u32[]{:S(2)}, u32[]{:S(2)}) collective-permute-start(bf16[2,512,128]{2,1,0:T(8,128)(2,1)S(1)} %get-tuple-element.64), channel_id=1, source_target_pairs={{0,2},{1,3},{2,0},{3,1},{4,6},{5,7},{6,4},{7,5},{8,10},{9,11},{10,... | collective-permute-start | bytes 786440 | tf_op jit(solution)/shard_map/ppermute | solution.py:35
  230.4 9.2 %collective-permute-start.31 = (bf16[2,512,128]{2,1,0:T(8,128)(2,1)S(1)}, bf16[2,512,128]{2,1,0:T(8,128)(2,1)S(1)}, u32[]{:S(2)}, u32[]{:S(2)}) collective-permute-start(bf16[2,512,128]{2,1,0:T(8,128)(2,1)S(1)} %get-tuple-element.66), channel_id=1, source_target_pairs={{0,8},{4,12},{8,0},{12,4},{16,24},{20,28},{24,16},{28,20},{1,9},{5... | collective-permute-start | bytes 786440 | tf_op jit(solution)/shard_map/ppermute | solution.py:33
  232.2 12.6 %collective-permute-start.21 = (bf16[2,512,128]{2,1,0:T(8,128)(2,1)S(1)}, bf16[2,512,128]{2,1,0:T(8,128)(2,1)S(1)}, u32[]{:S(2)}, u32[]{:S(2)}) collective-permute-start(bf16[2,512,128]{2,1,0:T(8,128)(2,1)S(1)} %get-tuple-element.52), channel_id=1, source_target_pairs={{0,2},{1,3},{2,0},{3,1},{4,6},{5,7},{6,4},{7,5},{8,10},{9,11},{10,... | collective-permute-start | bytes 786440 | tf_op jit(solution)/shard_map/ppermute | solution.py:35
  232.7 12.5 %collective-permute-start.22 = (bf16[2,512,128]{2,1,0:T(8,128)(2,1)S(1)}, bf16[2,512,128]{2,1,0:T(8,128)(2,1)S(1)}, u32[]{:S(2)}, u32[]{:S(2)}) collective-permute-start(bf16[2,512,128]{2,1,0:T(8,128)(2,1)S(1)} %get-tuple-element.54), channel_id=1, source_target_pairs={{0,8},{4,12},{8,0},{12,4},{16,24},{20,28},{24,16},{28,20},{1,9},{5... | collective-permute-start | bytes 786440 | tf_op jit(solution)/shard_map/ppermute | solution.py:33
  239.7 8.1 %collective-permute-start.32 = (bf16[512,128]{1,0:T(8,128)(2,1)S(1)}, bf16[512,128]{1,0:T(8,128)(2,1)S(1)}, u32[]{:S(2)}, u32[]{:S(2)}) collective-permute-start(bf16[512,128]{1,0:T(8,128)(2,1)S(1)} %get-tuple-element.68), channel_id=1, source_target_pairs={{0,8},{4,12},{8,0},{12,4},{16,24},{20,28},{24,16},{28,20},{1,9},{5... | collective-permute-start | bytes 393224 | tf_op jit(solution)/shard_map/ppermute | solution.py:33
  240.1 7.8 %collective-permute-start.33 = (bf16[512,128]{1,0:T(8,128)(2,1)S(1)}, bf16[512,128]{1,0:T(8,128)(2,1)S(1)}, u32[]{:S(2)}, u32[]{:S(2)}) collective-permute-start(bf16[512,128]{1,0:T(8,128)(2,1)S(1)} %get-tuple-element.70), channel_id=1, source_target_pairs={{0,2},{1,3},{2,0},{3,1},{4,6},{5,7},{6,4},{7,5},{8,10},{9,11},{10,... | collective-permute-start | bytes 393224 | tf_op jit(solution)/shard_map/ppermute | solution.py:35
  245.3 5.0 %collective-permute-start.23 = (bf16[512,128]{1,0:T(8,128)(2,1)S(1)}, bf16[512,128]{1,0:T(8,128)(2,1)S(1)}, u32[]{:S(2)}, u32[]{:S(2)}) collective-permute-start(bf16[512,128]{1,0:T(8,128)(2,1)S(1)} %get-tuple-element.56), channel_id=1, source_target_pairs={{0,8},{4,12},{8,0},{12,4},{16,24},{20,28},{24,16},{28,20},{1,9},{5... | collective-permute-start | bytes 393224 | tf_op jit(solution)/shard_map/ppermute | solution.py:33
  245.7 5.0 %collective-permute-start.24 = (bf16[512,128]{1,0:T(8,128)(2,1)S(1)}, bf16[512,128]{1,0:T(8,128)(2,1)S(1)}, u32[]{:S(2)}, u32[]{:S(2)}) collective-permute-start(bf16[512,128]{1,0:T(8,128)(2,1)S(1)} %get-tuple-element.58), channel_id=1, source_target_pairs={{0,2},{1,3},{2,0},{3,1},{4,6},{5,7},{6,4},{7,5},{8,10},{9,11},{10,... | collective-permute-start | bytes 393224 | tf_op jit(solution)/shard_map/ppermute | solution.py:35

commit v4 on v3

--- a/solution.py
+++ b/solution.py
@@ -125,53 +125,72 @@
     )(queries, keys.T, values.T, docs, residual)
 
 
-def prepare_kernel(which, gates, values, own, other, gate, value, sems):
-    cols = gate.shape[1]
-    copies = [
-        pltpu.make_async_copy(src, dst, sems.at[i])
-        for i, (src, dst) in enumerate(((gates, gate), (values, value)))
-    ]
-    for copy in copies:
-        copy.start()
-    for copy in copies:
-        copy.wait()
+def prepare_kernel(which, gates, values, own, other, gate, value, near, far, came, went):
+    count, lines, cols = gate.shape
     half = cols // 2
     main = half // LANES * LANES
     rest = half - main
-
-    def emit(part, out):
+    loads = []
+    for i in range(count):
+        at = pl.ds(i * lines, lines)
+        loads.append(
+            [
+                pltpu.make_async_copy(src.at[at], dst.at[i], came.at[i, f])
+                for f, (src, dst) in enumerate(((gates, gate), (values, value)))
+            ]
+        )
+        for copy in loads[-1]:
+            copy.start()
+
+    def emit(i, part, out):
         start = part * (cols - main)
         for n in range(0, main, LANES):
-            out[:, 2 * n : 2 * n + LANES] = gate[:, start + n : start + n + LANES]
-            out[:, 2 * n + LANES : 2 * n + 2 * LANES] = value[:, start + n : start + n + LANES]
-        left = gate[:, main : main + LANES].astype(jnp.float32)
-        right = value[:, main : main + LANES].astype(jnp.float32)
+            out[i, :, 2 * n : 2 * n + LANES] = gate[i, :, start + n : start + n + LANES]
+            out[i, :, 2 * n + LANES : 2 * n + 2 * LANES] = value[
+                i, :, start + n : start + n + LANES
+            ]
+        left = gate[i, :, main : main + LANES].astype(jnp.float32)
+        right = value[i, :, main : main + LANES].astype(jnp.float32)
         if part:
             left = pltpu.roll(left, rest, 1)
         else:
             right = pltpu.roll(right, rest, 1)
         lane = lax.broadcasted_iota(jnp.int32, left.shape, 1)
-        out[:, 2 * main :] = jnp.where(lane < rest, left, right).astype(out.dtype)
-
-    @pl.when(which[0] == 0)
-    def _():
-        emit(0, own)
-        emit(1, other)
-
-    @pl.when(which[0] != 0)
-    def _():
-        emit(1, own)
-        emit(0, other)
+        out[i, :, 2 * main :] = jnp.where(lane < rest, left, right).astype(out.dtype)
+
+    stores = []
+    for i in range(count):
+        for copy in loads[i]:
+            copy.wait()
+
+        @pl.when(which[0] == 0)
+        def _(i=i):
+            emit(i, 0, near)
+            emit(i, 1, far)
+
+        @pl.when(which[0] != 0)
+        def _(i=i):
+            emit(i, 1, near)
+            emit(i, 0, far)
+
+        for f, (src, dst) in enumerate(((near, own), (far, other))):
+            copy = pltpu.make_async_copy(src.at[i], dst.at[pl.ds(i * lines, lines)], went.at[i, f])
+            copy.start()
+            stores.append(copy)
+    for copy in stores:
+        copy.wait()
 
 
 def prepared(which, gate, value):
+    count = 4
     shape = jax.ShapeDtypeStruct(gate.shape, gate.dtype)
+    cut = pltpu.VMEM((count, gate.shape[0] // count, gate.shape[1]), gate.dtype)
     return pl.pallas_call(
         prepare_kernel,
         in_specs=[pl.BlockSpec(memory_space=pltpu.SMEM), hbm(), hbm()],
-        out_specs=[vmem()] * 2,
+        out_specs=[pl.BlockSpec(memory_space=pl.ANY)] * 2,
         out_shape=[shape, shape],
-        scratch_shapes=[pltpu.VMEM(gate.shape, gate.dtype)] * 2 + [pltpu.SemaphoreType.DMA((2,))],
+        scratch_shapes=[cut] * 4 + [pltpu.SemaphoreType.DMA((count, 2))] * 2,
         compiler_params=room(56),
         name="prepare",
     )(which, gate, value)

time: 260 us -> 260 us (level)
  no operation moved by 1% of the time
where the time goes in v4:
time: 260 us; the launch traced here: 259 us
  waiting for transfers between devices  115 us (44%)
  starting transfers between devices  59 us (23%)
  Pallas kernels  42 us (16%)
  local copies, waits for them, and re-layouts  19 us (7%)
  other arithmetic  9.83 us (4%)
  matrix products  7.71 us (3%)
  blocking collectives  5.66 us (2%)
    ppermute x19, waiting for transfers between devices, swapped(): return lax.ppermute(block, 'sp', [(i, i ^ sp_mask) for i in range(n_sp)])  101 us
    ppermute x19, starting transfers between devices, swapped(): return lax.ppermute(block, 'sp', [(i, i ^ sp_mask) for i in range(n_sp)])  45.7 us
    unnamed x75, local copies, waits for them, and re-layouts  16.7 us
    pallas_call x1, Pallas kernels, up_hidden(): pl.pallas_call(functools.partial(up_kernel, pieces=len(weights), quarter=...  14.6 us
    ppermute x14, waiting for transfers between devices, swapped(): return lax.ppermute(block, 'tp', [(i, i ^ tp_mask) for i in range(n_tp)])  12.4 us
    ppermute x14, starting transfers between devices, swapped(): return lax.ppermute(block, 'tp', [(i, i ^ tp_mask) for i in range(n_tp)])  8.41 us
    pallas_call x2, Pallas kernels, down_terms(): pl.pallas_call(down_kernel, in_specs=[pl.BlockSpec(memory_space=pltpu.SME...  7.14 us
    psum x1, blocking collectives, paired(): lax.psum((jnp.sum(second_sum, axis=1), jnp.sum(second_sum * second_sum, a...  5.66 us
  transfers between devices with their start and end apart: 34, of which 16 were waited for; matrix products, arithmetic and copies ran while one was open for 1% of the time, Pallas kernels for 12%

profile of v4, /device:TPU:0, one launch (start us, length us, event | category | flops | bytes accessed | tf_op | source)
XLA Modules:
  0.0 258.8 jit_solution(1117705226446794522)
XLA Ops:
  0.0 2.2 pack.1
  2.2 4.9 %collective-permute-start = (bf16[424,128]{1,0:T(8,128)(2,1)}, bf16[424,128]{1,0:T(8,128)(2,1)S(1)}, u32[]{:S(2)}, u32[]{:S(2)}) collective-permute-start(bf16[424,128]{1,0:T(8,128)(2,1)} %pack.1), channel_id=1, source_target_pairs={{0,4},{4,8},{8,12},{12,16},{16,20},{20,24},{24,28},{1,5},{5,9},{9,... | collective-permute-start | bytes 325640 | tf_op jit(solution)/shard_map/ppermute | solution.py:27
  7.2 0.7 pad_add_fusion.2.place
  7.8 1.9 collective-permute-done
  9.9 1.1 pad_maximum_fusion
  11.4 0.8 pad_add_fusion
  12.8 3.6 %fusion.1 = (f32[8,520]{1,0:T(8,128)S(1)}, f32[648,520,8]{0,1,2:T(8,128)S(1)}) fusion(pred[520,648]{1,0:T(8,128)(4,1)S(1)} %fusion.6, bf16[520,8,64]{0,2,1:T(8,128)(2,1)S(1)} %bitcast.45, bf16[64,128]{1,0:T(8,128)(2,1)S(1)} %get-tuple-element.82, bf16[64,128]{1,0:T(8,128)(2,1)S(1)} %get-tuple-element.83, bf16[64,512]{1,0:T(8,128)(2,1)} %bitcast.48), kind=kOutput, calls=%fused_computation.4 | convolution fusion | flops 353378752 | bytes 11767104 | tf_op jit(solution)/shard_map/qkgd,skd->kgqs/dot_general | solution.py:46
  16.4 3.7 %fusion = f32[8,520]{1,0:T(8,128)S(1)} fusion(f32[648,520,8]{0,1,2:T(8,128)S(1)} %get-tuple-element.90, f32[8,520]{1,0:T(8,128)S(1)} %broadcast_maximum_fusion, pred[520,648]{1,0:T(8,128)(4,1)S(1)} %fusion.6), kind=kLoop, calls=%fused_computation.3 | loop fusion | flops 10778560 | bytes 11152960 | tf_op jit(solution)/shard_map/reduce_sum | solution.py:59
  20.2 4.1 %fusion.7 = bf16[64,8,520]{2,0,1:T(8,128)(2,1)S(1)} fusion(f32[8,520]{1,0:T(8,128)S(1)} %exponential_add_fusion, f32[8,520]{1,0:T(8,128)S(1)} %broadcast_maximum_fusion, f32[648,520,8]{0,1,2:T(8,128)S(1)} %get-tuple-element.90, pred[520,648]{1,0:T(8,128)(4,1)S(1)} %fusion.6, bf16[64,128]{1,0:T(8,128)(2,1)S(1)} %get-tuple-element.84, ...), kind=kOutput, calls=%fused_computation.12 | convolution fusion | flops 359040512 | bytes 11783744 | tf_op jit(solution)/shard_map/kgqs,skd->qkgd/dot_general | solution.py:61
  24.4 1.0 copy.20.heads
  25.5 4.7 %project.1 = (bf16[2,136,2048]{2,1,0:T(8,128)(2,1)}, bf16[2,136,2048]{2,1,0:T(8,128)(2,1)}) custom-call(s32[2]{0:T(128)} %pad_add_fusion.2.place, bf16[520,512]{1,0:T(8,128)(2,1)} %copy.20.heads, bf16[512,2048]{1,0:T(8,128)(2,1)} %weights.1), custom_call_target="tpu_custom_call" | custom-call | tf_op jit(solution)/shard_map/project/pallas_call | solution.py:419
  30.3 2.9 %collective-permute-done.1.second = bf16[2,136,2048]{2,1,0:T(8,128)(2,1)S(1)} collective-permute-done((bf16[2,136,2048]{2,1,0:T(8,128)(2,1)}, bf16[2,136,2048]{2,1,0:T(8,128)(2,1)S(1)}, u32[]{:S(2)}, u32[]{:S(2)}) %collective-permute-start.1) | collective-permute-done | bytes 1114144 | tf_op jit(solution)/shard_map/ppermute | solution.py:35
  33.3 1.0 copy-done.21
  34.2 2.7 %merge.1 = (bf16[136,2048]{1,0:T(8,128)(2,1)}, bf16[136,2048]{1,0:T(8,128)(2,1)}) custom-call(s32[1]{0:T(128)} %bitcast.2.which, bf16[2,136,2048]{2,1,0:T(8,128)(2,1)} %get-tuple-element.38.first, bf16[2,136,2048]{2,1,0:T(8,128)(2,1)} %copy-done.21), custom_call_target="tpu_custom_call" | custom-call | tf_op jit(solution)/shard_map/merge/pallas_call | solution.py:444
  37.0 1.5 collective-permute-start.2
  38.4 2.0 row_halves.1
  40.4 3.4 %collective-permute-start.17 = (bf16[704,256]{1,0:T(8,128)(2,1)}, bf16[704,256]{1,0:T(8,128)(2,1)}, u32[]{:S(2)}, u32[]{:S(2)}) collective-permute-start(bf16[704,256]{1,0:T(8,128)(2,1)} %get-tuple-element.48), channel_id=1, source_target_pairs={{0,8},{4,12},{8,0},{12,4},{16,24},{20,28},{24,16},{28,20},{1,9},{5... | collective-permute-start | bytes 1081352 | tf_op jit(solution)/shard_map/ppermute | solution.py:33
  43.8 2.6 collective-permute-start.18
  46.4 2.5 prepare.1
  49.5 11.5 %collective-permute-done.17.refs_1_ = bf16[704,256]{1,0:T(8,128)(2,1)} collective-permute-done((bf16[704,256]{1,0:T(8,128)(2,1)}, bf16[704,256]{1,0:T(8,128)(2,1)}, u32[]{:S(2)}, u32[]{:S(2)}) %collective-permute-start.17) | collective-permute-done | bytes 360480 | tf_op jit(solution)/shard_map/ppermute | solution.py:33
  61.0 3.9 %collective-permute-start.15 = (bf16[256,1408]{1,0:T(8,128)(2,1)}, bf16[256,1408]{1,0:T(8,128)(2,1)S(1)}, u32[]{:S(2)}, u32[]{:S(2)}) collective-permute-start(bf16[256,1408]{1,0:T(8,128)(2,1)} %get-tuple-element.43), channel_id=1, source_target_pairs={{0,24},{4,28},{8,16},{12,20},{16,8},{20,12},{24,0},{28,4},{1,25},{... | collective-permute-start | bytes 2162696 | tf_op jit(solution)/shard_map/ppermute | solution.py:33
  65.0 1.5 collective-permute-start.19
  66.6 0.7 collective-permute-start.10
  68.0 3.6 %normed_rows.1.refs_0_ = bf16[136,2048]{1,0:T(8,128)(2,1)} custom-call(s32[2]{0:T(128)} %pad_add_fusion.2.place, bf16[136,2048]{1,0:T(8,128)(2,1)} %get-tuple-element.40.first, bf16[136,2048]{1,0:T(8,128)(2,1)} %copy-done.22, bf16[512,2048]{1,0:T(8,128)(2,1)} %residual.3, bf16[8,2048]{1,0:T(8,128)(2,1)} %copy-done.24, f32[1,2048]{1,0:T(1,128)} %bitcast.52, ...), custom_call_target="tpu_custom_call" | custom-call | tf_op jit(solution)/shard_map/normed_rows/pallas_call | solution.py:534
  71.7 45.0 %collective-permute-done.19.refs_3_ = bf16[704,256]{1,0:T(8,128)(2,1)} collective-permute-done((bf16[704,256]{1,0:T(8,128)(2,1)}, bf16[704,256]{1,0:T(8,128)(2,1)}, u32[]{:S(2)}, u32[]{:S(2)}) %collective-permute-start.19) | collective-permute-done | bytes 360480 | tf_op jit(solution)/shard_map/ppermute | solution.py:33
  116.7 23.8 %collective-permute-start.6 = (bf16[136,2048]{1,0:T(8,128)(2,1)}, bf16[136,2048]{1,0:T(8,128)(2,1)S(1)}, u32[]{:S(2)}, u32[]{:S(2)}) collective-permute-start(bf16[136,2048]{1,0:T(8,128)(2,1)} %normed_rows.1.refs_0_), channel_id=1, source_target_pairs={{0,8},{4,12},{8,0},{12,4},{16,24},{20,28},{24,16},{28,20},{1,9},{5... | collective-permute-start | bytes 1671176 | tf_op jit(solution)/shard_map/ppermute | solution.py:33
  141.2 1.4 collective-permute-start.14
  143.1 9.2 %collective-permute-done.6.refs_4_ = bf16[136,2048]{1,0:T(8,128)(2,1)S(1)} collective-permute-done((bf16[136,2048]{1,0:T(8,128)(2,1)}, bf16[136,2048]{1,0:T(8,128)(2,1)S(1)}, u32[]{:S(2)}, u32[]{:S(2)}) %collective-permute-start.6) | collective-permute-done | bytes 557088 | tf_op jit(solution)/shard_map/ppermute | solution.py:33
  153.5 6.1 %collective-permute-done.12.refs_11_ = bf16[256,1408]{1,0:T(8,128)(2,1)S(1)} collective-permute-done((bf16[256,1408]{1,0:T(8,128)(2,1)S(1)}, bf16[256,1408]{1,0:T(8,128)(2,1)S(1)}, u32[]{:S(2)}, u32[]{:S(2)}) %collective-permute-start.12) | collective-permute-done | bytes 720928 | tf_op jit(solution)/shard_map/ppermute | solution.py:33
  159.6 0.9 copy-done.2
  160.9 0.8 copy-done.8
  161.7 13.3 %collective-permute-done.14.refs_13_ = bf16[256,1408]{1,0:T(8,128)(2,1)S(1)} collective-permute-done((bf16[256,1408]{1,0:T(8,128)(2,1)S(1)}, bf16[256,1408]{1,0:T(8,128)(2,1)S(1)}, u32[]{:S(2)}, u32[]{:S(2)}) %collective-permute-start.14) | collective-permute-done | bytes 720928 | tf_op jit(solution)/shard_map/ppermute | solution.py:33
  175.0 0.9 copy-done.4
  176.4 11.6 %collective-permute-done.16.refs_15_ = bf16[256,1408]{1,0:T(8,128)(2,1)S(1)} collective-permute-done((bf16[256,1408]{1,0:T(8,128)(2,1)S(1)}, bf16[256,1408]{1,0:T(8,128)(2,1)S(1)}, u32[]{:S(2)}, u32[]{:S(2)}) %collective-permute-start.16) | collective-permute-done | bytes 720928 | tf_op jit(solution)/shard_map/ppermute | solution.py:33
  188.0 0.9 copy-done.6
  189.5 0.8 copy-done.10
  190.3 1.4 collective-permute-start.27
  191.7 0.8 copy-done.12
  193.1 0.8 copy-done.14
  193.9 1.4 collective-permute-start.25
  195.6 1.0 copy-done
  196.7 1.1 copy-done.1
  197.8 1.1 copy-done.3
  198.9 1.1 copy-done.5
  200.0 1.1 copy-done.7
  201.1 1.1 copy-done.9
  202.2 1.1 copy-done.11
  203.2 1.1 copy-done.13
  204.3 1.1 copy-done.15
  205.3 14.6 %up_hidden.1 = (bf16[512,704]{1,0:T(8,128)(2,1)S(1)}, bf16[512,704]{1,0:T(8,128)(2,1)S(1)}, bf16[512,512]{1,0:T(8,128)(2,1)S(1)}) custom-call(s32[2]{0:T(128)S(1)} %copy-done.20, bf16[136,2048]{1,0:T(8,128)(2,1)S(1)} %copy-done, bf16[136,2048]{1,0:T(8,128)(2,1)S(1)} %copy-done.9, bf16[136,2048]{1,0:T(8,128)(2,1)S(1)} %copy-done.11, ...), custom_call_target="tpu_custom_call" | custom-call | tf_op jit(solution)/shard_map/up_hidden/pallas_call | solution.py:360
  220.0 3.6 %down_terms.3 = (bf16[2,2,512,256]{3,2,1,0:T(8,128)(2,1)S(1)}, bf16[2,2,512,256]{3,2,1,0:T(8,128)(2,1)S(1)}) custom-call(s32[2]{0:T(128)S(1)} %copy-done.20, bf16[512,704]{1,0:T(8,128)(2,1)S(1)} %get-tuple-element.45.near, bf16[512,704]{1,0:T(8,128)(2,1)S(1)} %get-tuple-element.46.far, bf16[704,256]{1,0:T(8,128)(2,1)} %collective-permute-done.26.refs_0_, ...), custom_call_target="tpu_custom_call" | custom-call | tf_op jit(solution)/shard_map/down_terms/pallas_call | solution.py:578
  223.6 1.8 last_terms.1
  225.5 3.5 %down_terms.2 = (bf16[2,2,512,256]{3,2,1,0:T(8,128)(2,1)S(1)}, bf16[2,2,512,256]{3,2,1,0:T(8,128)(2,1)S(1)}) custom-call(s32[2]{0:T(128)S(1)} %copy-done.20, bf16[512,704]{1,0:T(8,128)(2,1)S(1)} %get-tuple-element.45.near, bf16[512,704]{1,0:T(8,128)(2,1)S(1)} %get-tuple-element.46.far, bf16[704,256]{1,0:T(8,128)(2,1)S(1)} %copy-done.17, ...), custom_call_target="tpu_custom_call" | custom-call | tf_op jit(solution)/shard_map/down_terms/pallas_call | solution.py:578
  230.7 1.2 collective-permute-done.20.second
  232.7 1.6 collective-permute-start.22
  234.3 4.8 %collective-permute-done.30.came_a = bf16[2,512,128]{2,1,0:T(8,128)(2,1)S(1)} collective-permute-done((bf16[2,512,128]{2,1,0:T(8,128)(2,1)S(1)}, bf16[2,512,128]{2,1,0:T(8,128)(2,1)S(1)}, u32[]{:S(2)}, u32[]{:S(2)}) %collective-permute-start.30) | collective-permute-done | bytes 262176 | tf_op jit(solution)/shard_map/ppermute | solution.py:35
  240.1 1.5 collective-permute-start.33
  241.6 3.1 %collective-permute-done.21.came_a = bf16[2,512,128]{2,1,0:T(8,128)(2,1)S(1)} collective-permute-done((bf16[2,512,128]{2,1,0:T(8,128)(2,1)S(1)}, bf16[2,512,128]{2,1,0:T(8,128)(2,1)S(1)}, u32[]{:S(2)}, u32[]{:S(2)}) %collective-permute-start.21) | collective-permute-done | bytes 262176 | tf_op jit(solution)/shard_map/ppermute | solution.py:35
  245.7 1.5 collective-permute-start.24
  247.2 0.6 collective-permute-done.32
  248.0 2.4 collective-permute-done.23
  250.7 1.4 fusion.28
  252.1 5.7 %all-reduce.2 = (f32[512]{0:T(512)S(1)}, f32[512]{0:T(512)S(1)}) all-reduce(f32[512]{0:T(512)S(1)} %get-tuple-element.72, f32[512]{0:T(512)S(1)} %get-tuple-element.71), channel_id=1, replica_groups=mesh['sp'=8,'tp'=4] {'tp'}, use_global_device_ids=true, to_apply=%region_5.6 | all-reduce | flops 1024 | bytes 8192 | tf_op jit(solution)/shard_map/psum | solution.py:757
  257.7 1.0 multiply_convert_fusion
  (135 shorter events, 12.5 us)
Async XLA Ops:
  2.2 7.5 %collective-permute-start = (bf16[424,128]{1,0:T(8,128)(2,1)}, bf16[424,128]{1,0:T(8,128)(2,1)S(1)}, u32[]{:S(2)}, u32[]{:S(2)}) collective-permute-start(bf16[424,128]{1,0:T(8,128)(2,1)} %pack.1), channel_id=1, source_target_pairs={{0,4},{4,8},{8,12},{12,16},{16,20},{20,24},{24,28},{1,5},{5,9},{9,... | collective-permute-start | bytes 325640 | tf_op jit(solution)/shard_map/ppermute | solution.py:27
  9.9 6.5 %copy-start.24 = (bf16[8,2048]{1,0:T(8,128)(2,1)}, bf16[8,2048]{1,0:T(8,128)(2,1)S(1)}, u32[]{:S(2)}) copy-start(bf16[8,2048]{1,0:T(8,128)(2,1)S(1)} %get-tuple-element.76.before) | copy-start | bytes 98308
  12.8 3.6 %copy-start.29 = (f32[8]{0:T(128)S(1)}, f32[8]{0:T(128)}, u32[]{:S(2)}) copy-start(f32[8]{0:T(128)} %param.18) | copy-start | bytes 100
  16.4 3.8 %copy-start.23 = (bf16[512,64]{0,1:T(8,128)(2,1)S(1)}, bf16[512,64]{0,1:T(8,128)(2,1)}, u32[]{:S(2)}) copy-start(bf16[512,64]{0,1:T(8,128)(2,1)} %param.16) | copy-start | bytes 196612
  24.4 42.1 %copy-start.25 = (s32[512]{0:T(512)S(1)}, s32[512]{0:T(512)}, u32[]{:S(2)}) copy-start(s32[512]{0:T(512)} %param.17) | copy-start | bytes 6148
  24.4 170.9 %copy-start.26 = (f32[3,1408]{1,0:T(4,128)S(1)}, f32[3,1408]{1,0:T(4,128)}, u32[]{:S(2)}) copy-start(f32[3,1408]{1,0:T(4,128)} %param.25) | copy-start | bytes 50692
  24.4 170.9 %copy-start.27 = (f32[3,1408]{1,0:T(4,128)S(1)}, f32[3,1408]{1,0:T(4,128)}, u32[]{:S(2)}) copy-start(f32[3,1408]{1,0:T(4,128)} %param.24) | copy-start | bytes 50692
  24.4 171.2 %copy-start.20 = (s32[2]{0:T(128)S(1)}, s32[2]{0:T(128)}, u32[]{:S(2)}) copy-start(s32[2]{0:T(128)} %pad_add_fusion.2.place) | copy-start | bytes 28
  30.2 3.0 %collective-permute-start.1 = (bf16[2,136,2048]{2,1,0:T(8,128)(2,1)}, bf16[2,136,2048]{2,1,0:T(8,128)(2,1)S(1)}, u32[]{:S(2)}, u32[]{:S(2)}) collective-permute-start(bf16[2,136,2048]{2,1,0:T(8,128)(2,1)} %get-tuple-element.39), channel_id=1, source_target_pairs={{0,1},{1,0},{2,3},{3,2},{4,5},{5,4},{6,7},{7,6},{8,9},{9,8},{10,11... | collective-permute-start | bytes 3342344 | tf_op jit(solution)/shard_map/ppermute | solution.py:35
  33.3 1.0 copy-start.21
  37.0 29.6 %collective-permute-start.2 = (bf16[136,2048]{1,0:T(8,128)(2,1)}, bf16[136,2048]{1,0:T(8,128)(2,1)S(1)}, u32[]{:S(2)}, u32[]{:S(2)}) collective-permute-start(bf16[136,2048]{1,0:T(8,128)(2,1)} %get-tuple-element.41), channel_id=1, source_target_pairs={{0,2},{1,3},{2,0},{3,1},{4,6},{5,7},{6,4},{7,5},{8,10},{9,11},{10,... | collective-permute-start | bytes 1671176 | tf_op jit(solution)/shard_map/ppermute | solution.py:35
  40.4 20.6 %collective-permute-start.17 = (bf16[704,256]{1,0:T(8,128)(2,1)}, bf16[704,256]{1,0:T(8,128)(2,1)}, u32[]{:S(2)}, u32[]{:S(2)}) collective-permute-start(bf16[704,256]{1,0:T(8,128)(2,1)} %get-tuple-element.48), channel_id=1, source_target_pairs={{0,8},{4,12},{8,0},{12,4},{16,24},{20,28},{24,16},{28,20},{1,9},{5... | collective-permute-start | bytes 1081352 | tf_op jit(solution)/shard_map/ppermute | solution.py:33
  43.8 21.2 %collective-permute-start.18 = (bf16[704,256]{1,0:T(8,128)(2,1)}, bf16[704,256]{1,0:T(8,128)(2,1)S(1)}, u32[]{:S(2)}, u32[]{:S(2)}) collective-permute-start(bf16[704,256]{1,0:T(8,128)(2,1)} %get-tuple-element.47.refs_0_), channel_id=1, source_target_pairs={{0,16},{4,20},{8,24},{12,28},{16,0},{20,4},{24,8},{28,12},{1,17},{... | collective-permute-start | bytes 1081352 | tf_op jit(solution)/shard_map/ppermute | solution.py:33
  49.0 91.6 %collective-permute-start.11 = (bf16[256,1408]{1,0:T(8,128)(2,1)}, bf16[256,1408]{1,0:T(8,128)(2,1)S(1)}, u32[]{:S(2)}, u32[]{:S(2)}) collective-permute-start(bf16[256,1408]{1,0:T(8,128)(2,1)} %get-tuple-element.43), channel_id=1, source_target_pairs={{0,8},{4,12},{8,0},{12,4},{16,24},{20,28},{24,16},{28,20},{1,9},{5... | collective-permute-start | bytes 2162696 | tf_op jit(solution)/shard_map/ppermute | solution.py:33
  49.5 91.7 %collective-permute-start.13 = (bf16[256,1408]{1,0:T(8,128)(2,1)}, bf16[256,1408]{1,0:T(8,128)(2,1)S(1)}, u32[]{:S(2)}, u32[]{:S(2)}) collective-permute-start(bf16[256,1408]{1,0:T(8,128)(2,1)} %get-tuple-element.42.refs_8_), channel_id=1, source_target_pairs={{0,16},{4,20},{8,24},{12,28},{16,0},{20,4},{24,8},{28,12},{1,17},{... | collective-permute-start | bytes 2162696 | tf_op jit(solution)/shard_map/ppermute | solution.py:33
  61.0 81.6 %collective-permute-start.15 = (bf16[256,1408]{1,0:T(8,128)(2,1)}, bf16[256,1408]{1,0:T(8,128)(2,1)S(1)}, u32[]{:S(2)}, u32[]{:S(2)}) collective-permute-start(bf16[256,1408]{1,0:T(8,128)(2,1)} %get-tuple-element.43), channel_id=1, source_target_pairs={{0,24},{4,28},{8,16},{12,20},{16,8},{20,12},{24,0},{28,4},{1,25},{... | collective-permute-start | bytes 2162696 | tf_op jit(solution)/shard_map/ppermute | solution.py:33
  65.0 1.6 copy-start.18
  65.0 51.7 %collective-permute-start.19 = (bf16[704,256]{1,0:T(8,128)(2,1)}, bf16[704,256]{1,0:T(8,128)(2,1)}, u32[]{:S(2)}, u32[]{:S(2)}) collective-permute-start(bf16[704,256]{1,0:T(8,128)(2,1)} %get-tuple-element.48), channel_id=1, source_target_pairs={{0,24},{4,28},{8,16},{12,20},{16,8},{20,12},{24,0},{28,4},{1,25},{... | collective-permute-start | bytes 1081352 | tf_op jit(solution)/shard_map/ppermute | solution.py:33
  66.6 1.4 copy-start.22
  66.6 86.2 %collective-permute-start.10 = (bf16[256,1408]{1,0:T(8,128)(2,1)}, bf16[256,1408]{1,0:T(8,128)(2,1)S(1)}, u32[]{:S(2)}, u32[]{:S(2)}) collective-permute-start(bf16[256,1408]{1,0:T(8,128)(2,1)} %get-tuple-element.42.refs_8_), channel_id=1, source_target_pairs={{0,4},{4,0},{8,12},{12,8},{16,20},{20,16},{24,28},{28,24},{1,5},{5... | collective-permute-start | bytes 2162696 | tf_op jit(solution)/shard_map/ppermute | solution.py:33
  116.7 35.6 %collective-permute-start.6 = (bf16[136,2048]{1,0:T(8,128)(2,1)}, bf16[136,2048]{1,0:T(8,128)(2,1)S(1)}, u32[]{:S(2)}, u32[]{:S(2)}) collective-permute-start(bf16[136,2048]{1,0:T(8,128)(2,1)} %normed_rows.1.refs_0_), channel_id=1, source_target_pairs={{0,8},{4,12},{8,0},{12,4},{16,24},{20,28},{24,16},{28,20},{1,9},{5... | collective-permute-start | bytes 1671176 | tf_op jit(solution)/shard_map/ppermute | solution.py:33
  140.5 19.0 %collective-permute-start.12 = (bf16[256,1408]{1,0:T(8,128)(2,1)S(1)}, bf16[256,1408]{1,0:T(8,128)(2,1)S(1)}, u32[]{:S(2)}, u32[]{:S(2)}) collective-permute-start(bf16[256,1408]{1,0:T(8,128)(2,1)S(1)} %collective-permute-done.11.refs_10_), channel_id=1, source_target_pairs={{0,4},{4,0},{8,12},{12,8},{16,20},{20,16},{24,28},{28,24},{1,5},{5... | collective-permute-start | bytes 2162696 | tf_op jit(solution)/shard_map/ppermute | solution.py:33
  141.2 33.8 %collective-permute-start.14 = (bf16[256,1408]{1,0:T(8,128)(2,1)S(1)}, bf16[256,1408]{1,0:T(8,128)(2,1)S(1)}, u32[]{:S(2)}, u32[]{:S(2)}) collective-permute-start(bf16[256,1408]{1,0:T(8,128)(2,1)S(1)} %collective-permute-done.13.refs_12_), channel_id=1, source_target_pairs={{0,4},{4,0},{8,12},{12,8},{16,20},{20,16},{24,28},{28,24},{1,5},{5... | collective-permute-start | bytes 2162696 | tf_op jit(solution)/shard_map/ppermute | solution.py:33
  142.6 17.8 %collective-permute-start.3 = (bf16[136,2048]{1,0:T(8,128)(2,1)}, bf16[136,2048]{1,0:T(8,128)(2,1)S(1)}, u32[]{:S(2)}, u32[]{:S(2)}) collective-permute-start(bf16[136,2048]{1,0:T(8,128)(2,1)} %normed_rows.1.refs_0_), channel_id=1, source_target_pairs={{0,2},{1,3},{2,0},{3,1},{4,6},{5,7},{6,4},{7,5},{8,10},{9,11},{10,... | collective-permute-start | bytes 1671176 | tf_op jit(solution)/shard_map/ppermute | solution.py:35
  152.3 23.6 %collective-permute-start.7 = (bf16[136,2048]{1,0:T(8,128)(2,1)S(1)}, bf16[136,2048]{1,0:T(8,128)(2,1)}, u32[]{:S(2)}, u32[]{:S(2)}) collective-permute-start(bf16[136,2048]{1,0:T(8,128)(2,1)S(1)} %collective-permute-done.6.refs_4_), channel_id=1, source_target_pairs={{0,2},{1,3},{2,0},{3,1},{4,6},{5,7},{6,4},{7,5},{8,10},{9,11},{10,... | collective-permute-start | bytes 1671176 | tf_op jit(solution)/shard_map/ppermute | solution.py:35
  152.8 35.1 %collective-permute-start.16 = (bf16[256,1408]{1,0:T(8,128)(2,1)S(1)}, bf16[256,1408]{1,0:T(8,128)(2,1)S(1)}, u32[]{:S(2)}, u32[]{:S(2)}) collective-permute-start(bf16[256,1408]{1,0:T(8,128)(2,1)S(1)} %collective-permute-done.15.refs_14_), channel_id=1, source_target_pairs={{0,4},{4,0},{8,12},{12,8},{16,20},{20,16},{24,28},{28,24},{1,5},{5... | collective-permute-start | bytes 2162696 | tf_op jit(solution)/shard_map/ppermute | solution.py:33
  159.6 0.9 copy-start.2
  160.4 29.0 %collective-permute-start.4 = (bf16[136,2048]{1,0:T(8,128)(2,1)}, bf16[136,2048]{1,0:T(8,128)(2,1)S(1)}, u32[]{:S(2)}, u32[]{:S(2)}) collective-permute-start(bf16[136,2048]{1,0:T(8,128)(2,1)} %normed_rows.1.refs_0_), channel_id=1, source_target_pairs={{0,1},{1,0},{2,3},{3,2},{4,5},{5,4},{6,7},{7,6},{8,9},{9,8},{10,11... | collective-permute-start | bytes 1671176 | tf_op jit(solution)/shard_map/ppermute | solution.py:35
  160.4 31.3 %collective-permute-start.5 = (bf16[136,2048]{1,0:T(8,128)(2,1)S(1)}, bf16[136,2048]{1,0:T(8,128)(2,1)S(1)}, u32[]{:S(2)}, u32[]{:S(2)}) collective-permute-start(bf16[136,2048]{1,0:T(8,128)(2,1)S(1)} %collective-permute-done.3.refs_1_), channel_id=1, source_target_pairs={{0,1},{1,0},{2,3},{3,2},{4,5},{5,4},{6,7},{7,6},{8,9},{9,8},{10,11... | collective-permute-start | bytes 1671176 | tf_op jit(solution)/shard_map/ppermute | solution.py:35
  160.9 0.8 copy-start.8
  175.0 0.9 copy-start.4
  175.9 17.2 %collective-permute-start.8 = (bf16[136,2048]{1,0:T(8,128)(2,1)S(1)}, bf16[136,2048]{1,0:T(8,128)(2,1)S(1)}, u32[]{:S(2)}, u32[]{:S(2)}) collective-permute-start(bf16[136,2048]{1,0:T(8,128)(2,1)S(1)} %collective-permute-done.6.refs_4_), channel_id=1, source_target_pairs={{0,1},{1,0},{2,3},{3,2},{4,5},{5,4},{6,7},{7,6},{8,9},{9,8},{10,11... | collective-permute-start | bytes 1671176 | tf_op jit(solution)/shard_map/ppermute | solution.py:35
  175.9 19.7 %collective-permute-start.9 = (bf16[136,2048]{1,0:T(8,128)(2,1)}, bf16[136,2048]{1,0:T(8,128)(2,1)}, u32[]{:S(2)}, u32[]{:S(2)}) collective-permute-start(bf16[136,2048]{1,0:T(8,128)(2,1)} %collective-permute-done.7.refs_5_), channel_id=1, source_target_pairs={{0,1},{1,0},{2,3},{3,2},{4,5},{5,4},{6,7},{7,6},{8,9},{9,8},{10,11... | collective-permute-start | bytes 1671176 | tf_op jit(solution)/shard_map/ppermute | solution.py:35
  188.0 0.9 copy-start.6
  188.8 31.1 %collective-permute-start.26 = (bf16[704,256]{1,0:T(8,128)(2,1)}, bf16[704,256]{1,0:T(8,128)(2,1)}, u32[]{:S(2)}, u32[]{:S(2)}) collective-permute-start(bf16[704,256]{1,0:T(8,128)(2,1)} %get-tuple-element.47.refs_0_), channel_id=1, source_target_pairs={{0,4},{4,0},{8,12},{12,8},{16,20},{20,16},{24,28},{28,24},{1,5},{5... | collective-permute-start | bytes 1081352 | tf_op jit(solution)/shard_map/ppermute | solution.py:33
  189.5 0.8 copy-start.10
  190.3 29.7 %collective-permute-start.27 = (bf16[704,256]{1,0:T(8,128)(2,1)}, bf16[704,256]{1,0:T(8,128)(2,1)}, u32[]{:S(2)}, u32[]{:S(2)}) collective-permute-start(bf16[704,256]{1,0:T(8,128)(2,1)} %collective-permute-done.17.refs_1_), channel_id=1, source_target_pairs={{0,4},{4,0},{8,12},{12,8},{16,20},{20,16},{24,28},{28,24},{1,5},{5... | collective-permute-start | bytes 1081352 | tf_op jit(solution)/shard_map/ppermute | solution.py:33
  191.7 0.8 copy-start.12
  192.5 27.5 %collective-permute-start.28 = (bf16[704,256]{1,0:T(8,128)(2,1)}, bf16[704,256]{1,0:T(8,128)(2,1)}, u32[]{:S(2)}, u32[]{:S(2)}) collective-permute-start(bf16[704,256]{1,0:T(8,128)(2,1)} %copy-done.18), channel_id=1, source_target_pairs={{0,4},{4,0},{8,12},{12,8},{16,20},{20,16},{24,28},{28,24},{1,5},{5... | collective-permute-start | bytes 1081352 | tf_op jit(solution)/shard_map/ppermute | solution.py:33
  193.1 0.8 copy-start.14
  193.9 29.7 %collective-permute-start.25 = (bf16[704,256]{1,0:T(8,128)(2,1)}, bf16[704,256]{1,0:T(8,128)(2,1)}, u32[]{:S(2)}, u32[]{:S(2)}) collective-permute-start(bf16[704,256]{1,0:T(8,128)(2,1)} %collective-permute-done.19.refs_3_), channel_id=1, source_target_pairs={{0,4},{4,0},{8,12},{12,8},{16,20},{20,16},{24,28},{28,24},{1,5},{5... | collective-permute-start | bytes 1081352 | tf_op jit(solution)/shard_map/ppermute | solution.py:33
  195.6 1.1 copy-start
  196.7 1.1 copy-start.1
  197.8 1.1 copy-start.3
  198.9 1.1 copy-start.5
  200.0 1.1 copy-start.7
  201.1 1.1 copy-start.9
  202.2 1.1 copy-start.11
  203.2 1.1 copy-start.13
  204.3 1.1 copy-start.15
  205.3 20.2 %copy-start.17 = (bf16[704,256]{1,0:T(8,128)(2,1)S(1)}, bf16[704,256]{1,0:T(8,128)(2,1)}, u32[]{:S(2)}) copy-start(bf16[704,256]{1,0:T(8,128)(2,1)} %get-tuple-element.47.refs_0_) | copy-start | bytes 1081348
  205.3 20.2 %copy-start.19 = (bf16[704,256]{1,0:T(8,128)(2,1)S(1)}, bf16[704,256]{1,0:T(8,128)(2,1)}, u32[]{:S(2)}) copy-start(bf16[704,256]{1,0:T(8,128)(2,1)} %copy-done.18) | copy-start | bytes 1081348
  219.9 12.2 %copy-start.16 = (bf16[512,512]{1,0:T(8,128)(2,1)}, bf16[512,512]{1,0:T(8,128)(2,1)S(1)}, u32[]{:S(2)}) copy-start(bf16[512,512]{1,0:T(8,128)(2,1)S(1)} %get-tuple-element.44) | copy-start | bytes 1572868
  225.4 32.3 %copy-start.28 = (f32[512]{0:T(512)S(1)}, f32[512]{0:T(512)}, u32[]{:S(2)}) copy-start(f32[512]{0:T(512)} %param.27) | copy-start | bytes 6148
  225.4 4.2 %collective-permute-start.29 = (bf16[2,2,512,256]{3,2,1,0:T(8,128)(2,1)S(1)}, bf16[2,2,512,256]{3,2,1,0:T(8,128)(2,1)S(1)}, u32[]{:S(2)}, u32[]{:S(2)}) collective-permute-start(bf16[2,2,512,256]{3,2,1,0:T(8,128)(2,1)S(1)} %get-tuple-element.62), channel_id=1, source_target_pairs={{0,1},{1,0},{2,3},{3,2},{4,5},{5,4},{6,7},{7,6},{8,9},{9,8},{10,11... | collective-permute-start | bytes 3145736 | tf_op jit(solution)/shard_map/ppermute | solution.py:35
  229.1 2.8 %collective-permute-start.20 = (bf16[2,2,512,256]{3,2,1,0:T(8,128)(2,1)S(1)}, bf16[2,2,512,256]{3,2,1,0:T(8,128)(2,1)S(1)}, u32[]{:S(2)}, u32[]{:S(2)}) collective-permute-start(bf16[2,2,512,256]{3,2,1,0:T(8,128)(2,1)S(1)} %get-tuple-element.50), channel_id=1, source_target_pairs={{0,1},{1,0},{2,3},{3,2},{4,5},{5,4},{6,7},{7,6},{8,9},{9,8},{10,11... | collective-permute-start | bytes 3145736 | tf_op jit(solution)/shard_map/ppermute | solution.py:35
  229.9 9.2 %collective-permute-start.30 = (bf16[2,512,128]{2,1,0:T(8,128)(2,1)S(1)}, bf16[2,512,128]{2,1,0:T(8,128)(2,1)S(1)}, u32[]{:S(2)}, u32[]{:S(2)}) collective-permute-start(bf16[2,512,128]{2,1,0:T(8,128)(2,1)S(1)} %get-tuple-element.64), channel_id=1, source_target_pairs={{0,2},{1,3},{2,0},{3,1},{4,6},{5,7},{6,4},{7,5},{8,10},{9,11},{10,... | collective-permute-start | bytes 786440 | tf_op jit(solution)/shard_map/ppermute | solution.py:35
  230.4 9.2 %collective-permute-start.31 = (bf16[2,512,128]{2,1,0:T(8,128)(2,1)S(1)}, bf16[2,512,128]{2,1,0:T(8,128)(2,1)S(1)}, u32[]{:S(2)}, u32[]{:S(2)}) collective-permute-start(bf16[2,512,128]{2,1,0:T(8,128)(2,1)S(1)} %get-tuple-element.66), channel_id=1, source_target_pairs={{0,8},{4,12},{8,0},{12,4},{16,24},{20,28},{24,16},{28,20},{1,9},{5... | collective-permute-start | bytes 786440 | tf_op jit(solution)/shard_map/ppermute | solution.py:33
  232.2 12.6 %collective-permute-start.21 = (bf16[2,512,128]{2,1,0:T(8,128)(2,1)S(1)}, bf16[2,512,128]{2,1,0:T(8,128)(2,1)S(1)}, u32[]{:S(2)}, u32[]{:S(2)}) collective-permute-start(bf16[2,512,128]{2,1,0:T(8,128)(2,1)S(1)} %get-tuple-element.52), channel_id=1, source_target_pairs={{0,2},{1,3},{2,0},{3,1},{4,6},{5,7},{6,4},{7,5},{8,10},{9,11},{10,... | collective-permute-start | bytes 786440 | tf_op jit(solution)/shard_map/ppermute | solution.py:35
  232.7 12.5 %collective-permute-start.22 = (bf16[2,512,128]{2,1,0:T(8,128)(2,1)S(1)}, bf16[2,512,128]{2,1,0:T(8,128)(2,1)S(1)}, u32[]{:S(2)}, u32[]{:S(2)}) collective-permute-start(bf16[2,512,128]{2,1,0:T(8,128)(2,1)S(1)} %get-tuple-element.54), channel_id=1, source_target_pairs={{0,8},{4,12},{8,0},{12,4},{16,24},{20,28},{24,16},{28,20},{1,9},{5... | collective-permute-start | bytes 786440 | tf_op jit(solution)/shard_map/ppermute | solution.py:33
  239.7 8.1 %collective-permute-start.32 = (bf16[512,128]{1,0:T(8,128)(2,1)S(1)}, bf16[512,128]{1,0:T(8,128)(2,1)S(1)}, u32[]{:S(2)}, u32[]{:S(2)}) collective-permute-start(bf16[512,128]{1,0:T(8,128)(2,1)S(1)} %get-tuple-element.68), channel_id=1, source_target_pairs={{0,8},{4,12},{8,0},{12,4},{16,24},{20,28},{24,16},{28,20},{1,9},{5... | collective-permute-start | bytes 393224 | tf_op jit(solution)/shard_map/ppermute | solution.py:33
  240.1 7.8 %collective-permute-start.33 = (bf16[512,128]{1,0:T(8,128)(2,1)S(1)}, bf16[512,128]{1,0:T(8,128)(2,1)S(1)}, u32[]{:S(2)}, u32[]{:S(2)}) collective-permute-start(bf16[512,128]{1,0:T(8,128)(2,1)S(1)} %get-tuple-element.70), channel_id=1, source_target_pairs={{0,2},{1,3},{2,0},{3,1},{4,6},{5,7},{6,4},{7,5},{8,10},{9,11},{10,... | collective-permute-start | bytes 393224 | tf_op jit(solution)/shard_map/ppermute | solution.py:35
  245.3 5.0 %collective-permute-start.23 = (bf16[512,128]{1,0:T(8,128)(2,1)S(1)}, bf16[512,128]{1,0:T(8,128)(2,1)S(1)}, u32[]{:S(2)}, u32[]{:S(2)}) collective-permute-start(bf16[512,128]{1,0:T(8,128)(2,1)S(1)} %get-tuple-element.56), channel_id=1, source_target_pairs={{0,8},{4,12},{8,0},{12,4},{16,24},{20,28},{24,16},{28,20},{1,9},{5... | collective-permute-start | bytes 393224 | tf_op jit(solution)/shard_map/ppermute | solution.py:33
  245.7 5.0 %collective-permute-start.24 = (bf16[512,128]{1,0:T(8,128)(2,1)S(1)}, bf16[512,128]{1,0:T(8,128)(2,1)S(1)}, u32[]{:S(2)}, u32[]{:S(2)}) collective-permute-start(bf16[512,128]{1,0:T(8,128)(2,1)S(1)} %get-tuple-element.58), channel_id=1, source_target_pairs={{0,2},{1,3},{2,0},{3,1},{4,6},{5,7},{6,4},{7,5},{8,10},{9,11},{10,... | collective-permute-start | bytes 393224 | tf_op jit(solution)/shard_map/ppermute | solution.py:35

commit v5 on v4

--- a/solution.py
+++ b/solution.py
@@ -523,8 +523,9 @@
         total = first[at].astype(jnp.float32) + second[at].astype(jnp.float32)
         total = mix_scale * base[at].astype(jnp.float32) + total
         mean = jnp.mean(total, axis=1, keepdims=True)
-        var = jnp.mean(total * total, axis=1, keepdims=True) - mean * mean
-        out[at] = ((total - mean) * lax.rsqrt(var + norm_eps) * gain[...]).astype(out.dtype)
+        total = total - mean
+        var = jnp.mean(total * total, axis=1, keepdims=True)
+        out[at] = (total * lax.rsqrt(var + norm_eps) * gain[...]).astype(out.dtype)
     line = lax.broadcasted_iota(jnp.int32, (TAIL, LANES), 0)
     rows_of = out[:TAIL, :LANES].astype(jnp.float32)
     out[:TAIL, :LANES] = jnp.where(line < 2, flags[...], rows_of).astype(out.dtype)
@@ -758,7 +759,7 @@
         (jnp.sum(second_sum, axis=1), jnp.sum(second_sum * second_sum, axis=1)), "tp"
     )
     mean = row_sum / width
-    var = row_squares / width - mean * mean
+    var = jnp.maximum(row_squares / width - mean * mean, 0.0)
     return (
         (second_sum - mean[:, None]) * lax.rsqrt(var + norm_eps)[:, None] * final_gain[None, :]
     ).astype(jnp.bfloat16)

time: 260 us -> 260 us (level)
  no operation moved by 1% of the time
where the time goes in v5:
time: 260 us; the launch traced here: 259 us
  waiting for transfers between devices  115 us (44%)
  starting transfers between devices  59 us (23%)
  Pallas kernels  42 us (16%)
  local copies, waits for them, and re-layouts  19 us (7%)
  other arithmetic  9.83 us (4%)
  matrix products  7.71 us (3%)
  blocking collectives  5.66 us (2%)
    ppermute x19, waiting for transfers between devices, swapped(): return lax.ppermute(block, 'sp', [(i, i ^ sp_mask) for i in range(n_sp)])  101 us
    ppermute x19, starting transfers between devices, swapped(): return lax.ppermute(block, 'sp', [(i, i ^ sp_mask) for i in range(n_sp)])  45.7 us
    unnamed x75, local copies, waits for them, and re-layouts  16.7 us
    pallas_call x1, Pallas kernels, up_hidden(): pl.pallas_call(functools.partial(up_kernel, pieces=len(weights), quarter=...  14.6 us
    ppermute x14, waiting for transfers between devices, swapped(): return lax.ppermute(block, 'tp', [(i, i ^ tp_mask) for i in range(n_tp)])  12.4 us
    ppermute x14, starting transfers between devices, swapped(): return lax.ppermute(block, 'tp', [(i, i ^ tp_mask) for i in range(n_tp)])  8.41 us
    pallas_call x2, Pallas kernels, down_terms(): pl.pallas_call(down_kernel, in_specs=[pl.BlockSpec(memory_space=pltpu.SME...  7.14 us
    psum x1, blocking collectives, paired(): lax.psum((jnp.sum(second_sum, axis=1), jnp.sum(second_sum * second_sum, a...  5.66 us
  transfers between devices with their start and end apart: 34, of which 16 were waited for; matrix products, arithmetic and copies ran while one was open for 1% of the time, Pallas kernels for 12%

profile of v5, /device:TPU:0, one launch (start us, length us, event | category | flops | bytes accessed | tf_op | source)
XLA Modules:
  0.0 258.8 jit_solution(15851113671682566823)
XLA Ops:
  0.0 2.2 pack.1
  2.2 4.9 %collective-permute-start = (bf16[424,128]{1,0:T(8,128)(2,1)}, bf16[424,128]{1,0:T(8,128)(2,1)S(1)}, u32[]{:S(2)}, u32[]{:S(2)}) collective-permute-start(bf16[424,128]{1,0:T(8,128)(2,1)} %pack.1), channel_id=1, source_target_pairs={{0,4},{4,8},{8,12},{12,16},{16,20},{20,24},{24,28},{1,5},{5,9},{9,... | collective-permute-start | bytes 325640 | tf_op jit(solution)/shard_map/ppermute | solution.py:27
  7.2 0.7 pad_add_fusion.2.place
  7.8 1.9 collective-permute-done
  9.9 1.1 pad_maximum_fusion
  11.4 0.8 pad_add_fusion
  12.8 3.6 %fusion.1 = (f32[8,520]{1,0:T(8,128)S(1)}, f32[648,520,8]{0,1,2:T(8,128)S(1)}) fusion(pred[520,648]{1,0:T(8,128)(4,1)S(1)} %fusion.6, bf16[520,8,64]{0,2,1:T(8,128)(2,1)S(1)} %bitcast.45, bf16[64,128]{1,0:T(8,128)(2,1)S(1)} %get-tuple-element.82, bf16[64,128]{1,0:T(8,128)(2,1)S(1)} %get-tuple-element.83, bf16[64,512]{1,0:T(8,128)(2,1)} %bitcast.48), kind=kOutput, calls=%fused_computation.4 | convolution fusion | flops 353378752 | bytes 11767104 | tf_op jit(solution)/shard_map/qkgd,skd->kgqs/dot_general | solution.py:46
  16.4 3.7 %fusion = f32[8,520]{1,0:T(8,128)S(1)} fusion(f32[648,520,8]{0,1,2:T(8,128)S(1)} %get-tuple-element.90, f32[8,520]{1,0:T(8,128)S(1)} %broadcast_maximum_fusion, pred[520,648]{1,0:T(8,128)(4,1)S(1)} %fusion.6), kind=kLoop, calls=%fused_computation.3 | loop fusion | flops 10778560 | bytes 11152960 | tf_op jit(solution)/shard_map/reduce_sum | solution.py:59
  20.2 4.1 %fusion.7 = bf16[64,8,520]{2,0,1:T(8,128)(2,1)S(1)} fusion(f32[8,520]{1,0:T(8,128)S(1)} %exponential_add_fusion, f32[8,520]{1,0:T(8,128)S(1)} %broadcast_maximum_fusion, f32[648,520,8]{0,1,2:T(8,128)S(1)} %get-tuple-element.90, pred[520,648]{1,0:T(8,128)(4,1)S(1)} %fusion.6, bf16[64,128]{1,0:T(8,128)(2,1)S(1)} %get-tuple-element.84, ...), kind=kOutput, calls=%fused_computation.12 | convolution fusion | flops 359040512 | bytes 11783744 | tf_op jit(solution)/shard_map/kgqs,skd->qkgd/dot_general | solution.py:61
  24.4 1.0 copy.20.heads
  25.5 4.7 %project.1 = (bf16[2,136,2048]{2,1,0:T(8,128)(2,1)}, bf16[2,136,2048]{2,1,0:T(8,128)(2,1)}) custom-call(s32[2]{0:T(128)} %pad_add_fusion.2.place, bf16[520,512]{1,0:T(8,128)(2,1)} %copy.20.heads, bf16[512,2048]{1,0:T(8,128)(2,1)} %weights.1), custom_call_target="tpu_custom_call" | custom-call | tf_op jit(solution)/shard_map/project/pallas_call | solution.py:419
  30.3 2.9 %collective-permute-done.1.second = bf16[2,136,2048]{2,1,0:T(8,128)(2,1)S(1)} collective-permute-done((bf16[2,136,2048]{2,1,0:T(8,128)(2,1)}, bf16[2,136,2048]{2,1,0:T(8,128)(2,1)S(1)}, u32[]{:S(2)}, u32[]{:S(2)}) %collective-permute-start.1) | collective-permute-done | bytes 1114144 | tf_op jit(solution)/shard_map/ppermute | solution.py:35
  33.3 1.0 copy-done.21
  34.2 2.7 %merge.1 = (bf16[136,2048]{1,0:T(8,128)(2,1)}, bf16[136,2048]{1,0:T(8,128)(2,1)}) custom-call(s32[1]{0:T(128)} %bitcast.2.which, bf16[2,136,2048]{2,1,0:T(8,128)(2,1)} %get-tuple-element.38.first, bf16[2,136,2048]{2,1,0:T(8,128)(2,1)} %copy-done.21), custom_call_target="tpu_custom_call" | custom-call | tf_op jit(solution)/shard_map/merge/pallas_call | solution.py:444
  37.0 1.5 collective-permute-start.2
  38.4 2.0 row_halves.1
  40.4 3.4 %collective-permute-start.17 = (bf16[704,256]{1,0:T(8,128)(2,1)}, bf16[704,256]{1,0:T(8,128)(2,1)}, u32[]{:S(2)}, u32[]{:S(2)}) collective-permute-start(bf16[704,256]{1,0:T(8,128)(2,1)} %get-tuple-element.48), channel_id=1, source_target_pairs={{0,8},{4,12},{8,0},{12,4},{16,24},{20,28},{24,16},{28,20},{1,9},{5... | collective-permute-start | bytes 1081352 | tf_op jit(solution)/shard_map/ppermute | solution.py:33
  43.8 2.6 collective-permute-start.18
  46.4 2.5 prepare.1
  49.5 11.5 %collective-permute-done.17.refs_1_ = bf16[704,256]{1,0:T(8,128)(2,1)} collective-permute-done((bf16[704,256]{1,0:T(8,128)(2,1)}, bf16[704,256]{1,0:T(8,128)(2,1)}, u32[]{:S(2)}, u32[]{:S(2)}) %collective-permute-start.17) | collective-permute-done | bytes 360480 | tf_op jit(solution)/shard_map/ppermute | solution.py:33
  61.0 3.9 %collective-permute-start.15 = (bf16[256,1408]{1,0:T(8,128)(2,1)}, bf16[256,1408]{1,0:T(8,128)(2,1)S(1)}, u32[]{:S(2)}, u32[]{:S(2)}) collective-permute-start(bf16[256,1408]{1,0:T(8,128)(2,1)} %get-tuple-element.43), channel_id=1, source_target_pairs={{0,24},{4,28},{8,16},{12,20},{16,8},{20,12},{24,0},{28,4},{1,25},{... | collective-permute-start | bytes 2162696 | tf_op jit(solution)/shard_map/ppermute | solution.py:33
  65.0 1.5 collective-permute-start.19
  66.6 0.7 collective-permute-start.10
  68.0 3.6 %normed_rows.1.refs_0_ = bf16[136,2048]{1,0:T(8,128)(2,1)} custom-call(s32[2]{0:T(128)} %pad_add_fusion.2.place, bf16[136,2048]{1,0:T(8,128)(2,1)} %get-tuple-element.40.first, bf16[136,2048]{1,0:T(8,128)(2,1)} %copy-done.22, bf16[512,2048]{1,0:T(8,128)(2,1)} %residual.3, bf16[8,2048]{1,0:T(8,128)(2,1)} %copy-done.24, f32[1,2048]{1,0:T(1,128)} %bitcast.52, ...), custom_call_target="tpu_custom_call" | custom-call | tf_op jit(solution)/shard_map/normed_rows/pallas_call | solution.py:535
  71.7 45.0 %collective-permute-done.19.refs_3_ = bf16[704,256]{1,0:T(8,128)(2,1)} collective-permute-done((bf16[704,256]{1,0:T(8,128)(2,1)}, bf16[704,256]{1,0:T(8,128)(2,1)}, u32[]{:S(2)}, u32[]{:S(2)}) %collective-permute-start.19) | collective-permute-done | bytes 360480 | tf_op jit(solution)/shard_map/ppermute | solution.py:33
  116.7 23.8 %collective-permute-start.6 = (bf16[136,2048]{1,0:T(8,128)(2,1)}, bf16[136,2048]{1,0:T(8,128)(2,1)S(1)}, u32[]{:S(2)}, u32[]{:S(2)}) collective-permute-start(bf16[136,2048]{1,0:T(8,128)(2,1)} %normed_rows.1.refs_0_), channel_id=1, source_target_pairs={{0,8},{4,12},{8,0},{12,4},{16,24},{20,28},{24,16},{28,20},{1,9},{5... | collective-permute-start | bytes 1671176 | tf_op jit(solution)/shard_map/ppermute | solution.py:33
  141.2 1.4 collective-permute-start.14
  143.1 9.2 %collective-permute-done.6.refs_4_ = bf16[136,2048]{1,0:T(8,128)(2,1)S(1)} collective-permute-done((bf16[136,2048]{1,0:T(8,128)(2,1)}, bf16[136,2048]{1,0:T(8,128)(2,1)S(1)}, u32[]{:S(2)}, u32[]{:S(2)}) %collective-permute-start.6) | collective-permute-done | bytes 557088 | tf_op jit(solution)/shard_map/ppermute | solution.py:33
  153.5 6.1 %collective-permute-done.12.refs_11_ = bf16[256,1408]{1,0:T(8,128)(2,1)S(1)} collective-permute-done((bf16[256,1408]{1,0:T(8,128)(2,1)S(1)}, bf16[256,1408]{1,0:T(8,128)(2,1)S(1)}, u32[]{:S(2)}, u32[]{:S(2)}) %collective-permute-start.12) | collective-permute-done | bytes 720928 | tf_op jit(solution)/shard_map/ppermute | solution.py:33
  159.6 0.9 copy-done.2
  160.9 0.8 copy-done.8
  161.7 13.3 %collective-permute-done.14.refs_13_ = bf16[256,1408]{1,0:T(8,128)(2,1)S(1)} collective-permute-done((bf16[256,1408]{1,0:T(8,128)(2,1)S(1)}, bf16[256,1408]{1,0:T(8,128)(2,1)S(1)}, u32[]{:S(2)}, u32[]{:S(2)}) %collective-permute-start.14) | collective-permute-done | bytes 720928 | tf_op jit(solution)/shard_map/ppermute | solution.py:33
  175.0 0.9 copy-done.4
  176.4 11.6 %collective-permute-done.16.refs_15_ = bf16[256,1408]{1,0:T(8,128)(2,1)S(1)} collective-permute-done((bf16[256,1408]{1,0:T(8,128)(2,1)S(1)}, bf16[256,1408]{1,0:T(8,128)(2,1)S(1)}, u32[]{:S(2)}, u32[]{:S(2)}) %collective-permute-start.16) | collective-permute-done | bytes 720928 | tf_op jit(solution)/shard_map/ppermute | solution.py:33
  188.0 0.9 copy-done.6
  189.5 0.8 copy-done.10
  190.3 1.4 collective-permute-start.27
  191.7 0.8 copy-done.12
  193.1 0.8 copy-done.14
  193.9 1.4 collective-permute-start.25
  195.6 1.0 copy-done
  196.7 1.1 copy-done.1
  197.8 1.1 copy-done.3
  198.9 1.1 copy-done.5
  200.0 1.1 copy-done.7
  201.1 1.1 copy-done.9
  202.2 1.1 copy-done.11
  203.2 1.1 copy-done.13
  204.3 1.1 copy-done.15
  205.3 14.6 %up_hidden.1 = (bf16[512,704]{1,0:T(8,128)(2,1)S(1)}, bf16[512,704]{1,0:T(8,128)(2,1)S(1)}, bf16[512,512]{1,0:T(8,128)(2,1)S(1)}) custom-call(s32[2]{0:T(128)S(1)} %copy-done.20, bf16[136,2048]{1,0:T(8,128)(2,1)S(1)} %copy-done, bf16[136,2048]{1,0:T(8,128)(2,1)S(1)} %copy-done.9, bf16[136,2048]{1,0:T(8,128)(2,1)S(1)} %copy-done.11, ...), custom_call_target="tpu_custom_call" | custom-call | tf_op jit(solution)/shard_map/up_hidden/pallas_call | solution.py:360
  220.0 3.6 %down_terms.3 = (bf16[2,2,512,256]{3,2,1,0:T(8,128)(2,1)S(1)}, bf16[2,2,512,256]{3,2,1,0:T(8,128)(2,1)S(1)}) custom-call(s32[2]{0:T(128)S(1)} %copy-done.20, bf16[512,704]{1,0:T(8,128)(2,1)S(1)} %get-tuple-element.45.near, bf16[512,704]{1,0:T(8,128)(2,1)S(1)} %get-tuple-element.46.far, bf16[704,256]{1,0:T(8,128)(2,1)} %collective-permute-done.26.refs_0_, ...), custom_call_target="tpu_custom_call" | custom-call | tf_op jit(solution)/shard_map/down_terms/pallas_call | solution.py:579
  223.6 1.8 last_terms.1
  225.5 3.5 %down_terms.2 = (bf16[2,2,512,256]{3,2,1,0:T(8,128)(2,1)S(1)}, bf16[2,2,512,256]{3,2,1,0:T(8,128)(2,1)S(1)}) custom-call(s32[2]{0:T(128)S(1)} %copy-done.20, bf16[512,704]{1,0:T(8,128)(2,1)S(1)} %get-tuple-element.45.near, bf16[512,704]{1,0:T(8,128)(2,1)S(1)} %get-tuple-element.46.far, bf16[704,256]{1,0:T(8,128)(2,1)S(1)} %copy-done.17, ...), custom_call_target="tpu_custom_call" | custom-call | tf_op jit(solution)/shard_map/down_terms/pallas_call | solution.py:579
  230.7 1.2 collective-permute-done.20.second
  232.7 1.6 collective-permute-start.22
  234.3 4.8 %collective-permute-done.30.came_a = bf16[2,512,128]{2,1,0:T(8,128)(2,1)S(1)} collective-permute-done((bf16[2,512,128]{2,1,0:T(8,128)(2,1)S(1)}, bf16[2,512,128]{2,1,0:T(8,128)(2,1)S(1)}, u32[]{:S(2)}, u32[]{:S(2)}) %collective-permute-start.30) | collective-permute-done | bytes 262176 | tf_op jit(solution)/shard_map/ppermute | solution.py:35
  240.1 1.5 collective-permute-start.33
  241.6 3.1 %collective-permute-done.21.came_a = bf16[2,512,128]{2,1,0:T(8,128)(2,1)S(1)} collective-permute-done((bf16[2,512,128]{2,1,0:T(8,128)(2,1)S(1)}, bf16[2,512,128]{2,1,0:T(8,128)(2,1)S(1)}, u32[]{:S(2)}, u32[]{:S(2)}) %collective-permute-start.21) | collective-permute-done | bytes 262176 | tf_op jit(solution)/shard_map/ppermute | solution.py:35
  245.7 1.5 collective-permute-start.24
  247.2 0.6 collective-permute-done.32
  248.0 2.4 collective-permute-done.23
  250.7 1.4 fusion.28
  252.1 5.7 %all-reduce.2 = (f32[512]{0:T(512)S(1)}, f32[512]{0:T(512)S(1)}) all-reduce(f32[512]{0:T(512)S(1)} %get-tuple-element.72, f32[512]{0:T(512)S(1)} %get-tuple-element.71), channel_id=1, replica_groups=mesh['sp'=8,'tp'=4] {'tp'}, use_global_device_ids=true, to_apply=%region_5.6 | all-reduce | flops 1024 | bytes 8192 | tf_op jit(solution)/shard_map/psum | solution.py:758
  257.7 1.0 multiply_convert_fusion
  (135 shorter events, 12.5 us)
Async XLA Ops:
  2.2 7.5 %collective-permute-start = (bf16[424,128]{1,0:T(8,128)(2,1)}, bf16[424,128]{1,0:T(8,128)(2,1)S(1)}, u32[]{:S(2)}, u32[]{:S(2)}) collective-permute-start(bf16[424,128]{1,0:T(8,128)(2,1)} %pack.1), channel_id=1, source_target_pairs={{0,4},{4,8},{8,12},{12,16},{16,20},{20,24},{24,28},{1,5},{5,9},{9,... | collective-permute-start | bytes 325640 | tf_op jit(solution)/shard_map/ppermute | solution.py:27
  9.9 6.5 %copy-start.24 = (bf16[8,2048]{1,0:T(8,128)(2,1)}, bf16[8,2048]{1,0:T(8,128)(2,1)S(1)}, u32[]{:S(2)}) copy-start(bf16[8,2048]{1,0:T(8,128)(2,1)S(1)} %get-tuple-element.76.before) | copy-start | bytes 98308
  12.8 3.6 %copy-start.29 = (f32[8]{0:T(128)S(1)}, f32[8]{0:T(128)}, u32[]{:S(2)}) copy-start(f32[8]{0:T(128)} %param.18) | copy-start | bytes 100
  16.4 3.8 %copy-start.23 = (bf16[512,64]{0,1:T(8,128)(2,1)S(1)}, bf16[512,64]{0,1:T(8,128)(2,1)}, u32[]{:S(2)}) copy-start(bf16[512,64]{0,1:T(8,128)(2,1)} %param.16) | copy-start | bytes 196612
  24.4 42.1 %copy-start.25 = (s32[512]{0:T(512)S(1)}, s32[512]{0:T(512)}, u32[]{:S(2)}) copy-start(s32[512]{0:T(512)} %param.17) | copy-start | bytes 6148
  24.4 170.9 %copy-start.26 = (f32[3,1408]{1,0:T(4,128)S(1)}, f32[3,1408]{1,0:T(4,128)}, u32[]{:S(2)}) copy-start(f32[3,1408]{1,0:T(4,128)} %param.25) | copy-start | bytes 50692
  24.4 170.9 %copy-start.27 = (f32[3,1408]{1,0:T(4,128)S(1)}, f32[3,1408]{1,0:T(4,128)}, u32[]{:S(2)}) copy-start(f32[3,1408]{1,0:T(4,128)} %param.24) | copy-start | bytes 50692
  24.4 171.2 %copy-start.20 = (s32[2]{0:T(128)S(1)}, s32[2]{0:T(128)}, u32[]{:S(2)}) copy-start(s32[2]{0:T(128)} %pad_add_fusion.2.place) | copy-start | bytes 28
  30.2 3.0 %collective-permute-start.1 = (bf16[2,136,2048]{2,1,0:T(8,128)(2,1)}, bf16[2,136,2048]{2,1,0:T(8,128)(2,1)S(1)}, u32[]{:S(2)}, u32[]{:S(2)}) collective-permute-start(bf16[2,136,2048]{2,1,0:T(8,128)(2,1)} %get-tuple-element.39), channel_id=1, source_target_pairs={{0,1},{1,0},{2,3},{3,2},{4,5},{5,4},{6,7},{7,6},{8,9},{9,8},{10,11... | collective-permute-start | bytes 3342344 | tf_op jit(solution)/shard_map/ppermute | solution.py:35
  33.3 1.0 copy-start.21
  37.0 29.6 %collective-permute-start.2 = (bf16[136,2048]{1,0:T(8,128)(2,1)}, bf16[136,2048]{1,0:T(8,128)(2,1)S(1)}, u32[]{:S(2)}, u32[]{:S(2)}) collective-permute-start(bf16[136,2048]{1,0:T(8,128)(2,1)} %get-tuple-element.41), channel_id=1, source_target_pairs={{0,2},{1,3},{2,0},{3,1},{4,6},{5,7},{6,4},{7,5},{8,10},{9,11},{10,... | collective-permute-start | bytes 1671176 | tf_op jit(solution)/shard_map/ppermute | solution.py:35
  40.4 20.6 %collective-permute-start.17 = (bf16[704,256]{1,0:T(8,128)(2,1)}, bf16[704,256]{1,0:T(8,128)(2,1)}, u32[]{:S(2)}, u32[]{:S(2)}) collective-permute-start(bf16[704,256]{1,0:T(8,128)(2,1)} %get-tuple-element.48), channel_id=1, source_target_pairs={{0,8},{4,12},{8,0},{12,4},{16,24},{20,28},{24,16},{28,20},{1,9},{5... | collective-permute-start | bytes 1081352 | tf_op jit(solution)/shard_map/ppermute | solution.py:33
  43.8 21.2 %collective-permute-start.18 = (bf16[704,256]{1,0:T(8,128)(2,1)}, bf16[704,256]{1,0:T(8,128)(2,1)S(1)}, u32[]{:S(2)}, u32[]{:S(2)}) collective-permute-start(bf16[704,256]{1,0:T(8,128)(2,1)} %get-tuple-element.47.refs_0_), channel_id=1, source_target_pairs={{0,16},{4,20},{8,24},{12,28},{16,0},{20,4},{24,8},{28,12},{1,17},{... | collective-permute-start | bytes 1081352 | tf_op jit(solution)/shard_map/ppermute | solution.py:33
  49.0 91.6 %collective-permute-start.11 = (bf16[256,1408]{1,0:T(8,128)(2,1)}, bf16[256,1408]{1,0:T(8,128)(2,1)S(1)}, u32[]{:S(2)}, u32[]{:S(2)}) collective-permute-start(bf16[256,1408]{1,0:T(8,128)(2,1)} %get-tuple-element.43), channel_id=1, source_target_pairs={{0,8},{4,12},{8,0},{12,4},{16,24},{20,28},{24,16},{28,20},{1,9},{5... | collective-permute-start | bytes 2162696 | tf_op jit(solution)/shard_map/ppermute | solution.py:33
  49.5 91.7 %collective-permute-start.13 = (bf16[256,1408]{1,0:T(8,128)(2,1)}, bf16[256,1408]{1,0:T(8,128)(2,1)S(1)}, u32[]{:S(2)}, u32[]{:S(2)}) collective-permute-start(bf16[256,1408]{1,0:T(8,128)(2,1)} %get-tuple-element.42.refs_8_), channel_id=1, source_target_pairs={{0,16},{4,20},{8,24},{12,28},{16,0},{20,4},{24,8},{28,12},{1,17},{... | collective-permute-start | bytes 2162696 | tf_op jit(solution)/shard_map/ppermute | solution.py:33
  61.0 81.6 %collective-permute-start.15 = (bf16[256,1408]{1,0:T(8,128)(2,1)}, bf16[256,1408]{1,0:T(8,128)(2,1)S(1)}, u32[]{:S(2)}, u32[]{:S(2)}) collective-permute-start(bf16[256,1408]{1,0:T(8,128)(2,1)} %get-tuple-element.43), channel_id=1, source_target_pairs={{0,24},{4,28},{8,16},{12,20},{16,8},{20,12},{24,0},{28,4},{1,25},{... | collective-permute-start | bytes 2162696 | tf_op jit(solution)/shard_map/ppermute | solution.py:33
  65.0 1.6 copy-start.18
  65.0 51.7 %collective-permute-start.19 = (bf16[704,256]{1,0:T(8,128)(2,1)}, bf16[704,256]{1,0:T(8,128)(2,1)}, u32[]{:S(2)}, u32[]{:S(2)}) collective-permute-start(bf16[704,256]{1,0:T(8,128)(2,1)} %get-tuple-element.48), channel_id=1, source_target_pairs={{0,24},{4,28},{8,16},{12,20},{16,8},{20,12},{24,0},{28,4},{1,25},{... | collective-permute-start | bytes 1081352 | tf_op jit(solution)/shard_map/ppermute | solution.py:33
  66.6 1.4 copy-start.22
  66.6 86.2 %collective-permute-start.10 = (bf16[256,1408]{1,0:T(8,128)(2,1)}, bf16[256,1408]{1,0:T(8,128)(2,1)S(1)}, u32[]{:S(2)}, u32[]{:S(2)}) collective-permute-start(bf16[256,1408]{1,0:T(8,128)(2,1)} %get-tuple-element.42.refs_8_), channel_id=1, source_target_pairs={{0,4},{4,0},{8,12},{12,8},{16,20},{20,16},{24,28},{28,24},{1,5},{5... | collective-permute-start | bytes 2162696 | tf_op jit(solution)/shard_map/ppermute | solution.py:33
  116.7 35.6 %collective-permute-start.6 = (bf16[136,2048]{1,0:T(8,128)(2,1)}, bf16[136,2048]{1,0:T(8,128)(2,1)S(1)}, u32[]{:S(2)}, u32[]{:S(2)}) collective-permute-start(bf16[136,2048]{1,0:T(8,128)(2,1)} %normed_rows.1.refs_0_), channel_id=1, source_target_pairs={{0,8},{4,12},{8,0},{12,4},{16,24},{20,28},{24,16},{28,20},{1,9},{5... | collective-permute-start | bytes 1671176 | tf_op jit(solution)/shard_map/ppermute | solution.py:33
  140.5 19.0 %collective-permute-start.12 = (bf16[256,1408]{1,0:T(8,128)(2,1)S(1)}, bf16[256,1408]{1,0:T(8,128)(2,1)S(1)}, u32[]{:S(2)}, u32[]{:S(2)}) collective-permute-start(bf16[256,1408]{1,0:T(8,128)(2,1)S(1)} %collective-permute-done.11.refs_10_), channel_id=1, source_target_pairs={{0,4},{4,0},{8,12},{12,8},{16,20},{20,16},{24,28},{28,24},{1,5},{5... | collective-permute-start | bytes 2162696 | tf_op jit(solution)/shard_map/ppermute | solution.py:33
  141.2 33.8 %collective-permute-start.14 = (bf16[256,1408]{1,0:T(8,128)(2,1)S(1)}, bf16[256,1408]{1,0:T(8,128)(2,1)S(1)}, u32[]{:S(2)}, u32[]{:S(2)}) collective-permute-start(bf16[256,1408]{1,0:T(8,128)(2,1)S(1)} %collective-permute-done.13.refs_12_), channel_id=1, source_target_pairs={{0,4},{4,0},{8,12},{12,8},{16,20},{20,16},{24,28},{28,24},{1,5},{5... | collective-permute-start | bytes 2162696 | tf_op jit(solution)/shard_map/ppermute | solution.py:33
  142.6 17.8 %collective-permute-start.3 = (bf16[136,2048]{1,0:T(8,128)(2,1)}, bf16[136,2048]{1,0:T(8,128)(2,1)S(1)}, u32[]{:S(2)}, u32[]{:S(2)}) collective-permute-start(bf16[136,2048]{1,0:T(8,128)(2,1)} %normed_rows.1.refs_0_), channel_id=1, source_target_pairs={{0,2},{1,3},{2,0},{3,1},{4,6},{5,7},{6,4},{7,5},{8,10},{9,11},{10,... | collective-permute-start | bytes 1671176 | tf_op jit(solution)/shard_map/ppermute | solution.py:35
  152.3 23.6 %collective-permute-start.7 = (bf16[136,2048]{1,0:T(8,128)(2,1)S(1)}, bf16[136,2048]{1,0:T(8,128)(2,1)}, u32[]{:S(2)}, u32[]{:S(2)}) collective-permute-start(bf16[136,2048]{1,0:T(8,128)(2,1)S(1)} %collective-permute-done.6.refs_4_), channel_id=1, source_target_pairs={{0,2},{1,3},{2,0},{3,1},{4,6},{5,7},{6,4},{7,5},{8,10},{9,11},{10,... | collective-permute-start | bytes 1671176 | tf_op jit(solution)/shard_map/ppermute | solution.py:35
  152.8 35.1 %collective-permute-start.16 = (bf16[256,1408]{1,0:T(8,128)(2,1)S(1)}, bf16[256,1408]{1,0:T(8,128)(2,1)S(1)}, u32[]{:S(2)}, u32[]{:S(2)}) collective-permute-start(bf16[256,1408]{1,0:T(8,128)(2,1)S(1)} %collective-permute-done.15.refs_14_), channel_id=1, source_target_pairs={{0,4},{4,0},{8,12},{12,8},{16,20},{20,16},{24,28},{28,24},{1,5},{5... | collective-permute-start | bytes 2162696 | tf_op jit(solution)/shard_map/ppermute | solution.py:33
  159.6 0.9 copy-start.2
  160.4 29.0 %collective-permute-start.4 = (bf16[136,2048]{1,0:T(8,128)(2,1)}, bf16[136,2048]{1,0:T(8,128)(2,1)S(1)}, u32[]{:S(2)}, u32[]{:S(2)}) collective-permute-start(bf16[136,2048]{1,0:T(8,128)(2,1)} %normed_rows.1.refs_0_), channel_id=1, source_target_pairs={{0,1},{1,0},{2,3},{3,2},{4,5},{5,4},{6,7},{7,6},{8,9},{9,8},{10,11... | collective-permute-start | bytes 1671176 | tf_op jit(solution)/shard_map/ppermute | solution.py:35
  160.4 31.3 %collective-permute-start.5 = (bf16[136,2048]{1,0:T(8,128)(2,1)S(1)}, bf16[136,2048]{1,0:T(8,128)(2,1)S(1)}, u32[]{:S(2)}, u32[]{:S(2)}) collective-permute-start(bf16[136,2048]{1,0:T(8,128)(2,1)S(1)} %collective-permute-done.3.refs_1_), channel_id=1, source_target_pairs={{0,1},{1,0},{2,3},{3,2},{4,5},{5,4},{6,7},{7,6},{8,9},{9,8},{10,11... | collective-permute-start | bytes 1671176 | tf_op jit(solution)/shard_map/ppermute | solution.py:35
  160.9 0.8 copy-start.8
  175.0 0.9 copy-start.4
  175.9 17.2 %collective-permute-start.8 = (bf16[136,2048]{1,0:T(8,128)(2,1)S(1)}, bf16[136,2048]{1,0:T(8,128)(2,1)S(1)}, u32[]{:S(2)}, u32[]{:S(2)}) collective-permute-start(bf16[136,2048]{1,0:T(8,128)(2,1)S(1)} %collective-permute-done.6.refs_4_), channel_id=1, source_target_pairs={{0,1},{1,0},{2,3},{3,2},{4,5},{5,4},{6,7},{7,6},{8,9},{9,8},{10,11... | collective-permute-start | bytes 1671176 | tf_op jit(solution)/shard_map/ppermute | solution.py:35
  175.9 19.7 %collective-permute-start.9 = (bf16[136,2048]{1,0:T(8,128)(2,1)}, bf16[136,2048]{1,0:T(8,128)(2,1)}, u32[]{:S(2)}, u32[]{:S(2)}) collective-permute-start(bf16[136,2048]{1,0:T(8,128)(2,1)} %collective-permute-done.7.refs_5_), channel_id=1, source_target_pairs={{0,1},{1,0},{2,3},{3,2},{4,5},{5,4},{6,7},{7,6},{8,9},{9,8},{10,11... | collective-permute-start | bytes 1671176 | tf_op jit(solution)/shard_map/ppermute | solution.py:35
  188.0 0.9 copy-start.6
  188.8 31.1 %collective-permute-start.26 = (bf16[704,256]{1,0:T(8,128)(2,1)}, bf16[704,256]{1,0:T(8,128)(2,1)}, u32[]{:S(2)}, u32[]{:S(2)}) collective-permute-start(bf16[704,256]{1,0:T(8,128)(2,1)} %get-tuple-element.47.refs_0_), channel_id=1, source_target_pairs={{0,4},{4,0},{8,12},{12,8},{16,20},{20,16},{24,28},{28,24},{1,5},{5... | collective-permute-start | bytes 1081352 | tf_op jit(solution)/shard_map/ppermute | solution.py:33
  189.5 0.8 copy-start.10
  190.3 29.7 %collective-permute-start.27 = (bf16[704,256]{1,0:T(8,128)(2,1)}, bf16[704,256]{1,0:T(8,128)(2,1)}, u32[]{:S(2)}, u32[]{:S(2)}) collective-permute-start(bf16[704,256]{1,0:T(8,128)(2,1)} %collective-permute-done.17.refs_1_), channel_id=1, source_target_pairs={{0,4},{4,0},{8,12},{12,8},{16,20},{20,16},{24,28},{28,24},{1,5},{5... | collective-permute-start | bytes 1081352 | tf_op jit(solution)/shard_map/ppermute | solution.py:33
  191.7 0.8 copy-start.12
  192.5 27.5 %collective-permute-start.28 = (bf16[704,256]{1,0:T(8,128)(2,1)}, bf16[704,256]{1,0:T(8,128)(2,1)}, u32[]{:S(2)}, u32[]{:S(2)}) collective-permute-start(bf16[704,256]{1,0:T(8,128)(2,1)} %copy-done.18), channel_id=1, source_target_pairs={{0,4},{4,0},{8,12},{12,8},{16,20},{20,16},{24,28},{28,24},{1,5},{5... | collective-permute-start | bytes 1081352 | tf_op jit(solution)/shard_map/ppermute | solution.py:33
  193.1 0.8 copy-start.14
  193.9 29.7 %collective-permute-start.25 = (bf16[704,256]{1,0:T(8,128)(2,1)}, bf16[704,256]{1,0:T(8,128)(2,1)}, u32[]{:S(2)}, u32[]{:S(2)}) collective-permute-start(bf16[704,256]{1,0:T(8,128)(2,1)} %collective-permute-done.19.refs_3_), channel_id=1, source_target_pairs={{0,4},{4,0},{8,12},{12,8},{16,20},{20,16},{24,28},{28,24},{1,5},{5... | collective-permute-start | bytes 1081352 | tf_op jit(solution)/shard_map/ppermute | solution.py:33
  195.6 1.1 copy-start
  196.7 1.1 copy-start.1
  197.8 1.1 copy-start.3
  198.9 1.1 copy-start.5
  200.0 1.1 copy-start.7
  201.1 1.1 copy-start.9
  202.2 1.1 copy-start.11
  203.2 1.1 copy-start.13
  204.3 1.1 copy-start.15
  205.3 20.2 %copy-start.17 = (bf16[704,256]{1,0:T(8,128)(2,1)S(1)}, bf16[704,256]{1,0:T(8,128)(2,1)}, u32[]{:S(2)}) copy-start(bf16[704,256]{1,0:T(8,128)(2,1)} %get-tuple-element.47.refs_0_) | copy-start | bytes 1081348
  205.3 20.2 %copy-start.19 = (bf16[704,256]{1,0:T(8,128)(2,1)S(1)}, bf16[704,256]{1,0:T(8,128)(2,1)}, u32[]{:S(2)}) copy-start(bf16[704,256]{1,0:T(8,128)(2,1)} %copy-done.18) | copy-start | bytes 1081348
  219.9 12.2 %copy-start.16 = (bf16[512,512]{1,0:T(8,128)(2,1)}, bf16[512,512]{1,0:T(8,128)(2,1)S(1)}, u32[]{:S(2)}) copy-start(bf16[512,512]{1,0:T(8,128)(2,1)S(1)} %get-tuple-element.44) | copy-start | bytes 1572868
  225.4 32.3 %copy-start.28 = (f32[512]{0:T(512)S(1)}, f32[512]{0:T(512)}, u32[]{:S(2)}) copy-start(f32[512]{0:T(512)} %param.27) | copy-start | bytes 6148
  225.4 4.2 %collective-permute-start.29 = (bf16[2,2,512,256]{3,2,1,0:T(8,128)(2,1)S(1)}, bf16[2,2,512,256]{3,2,1,0:T(8,128)(2,1)S(1)}, u32[]{:S(2)}, u32[]{:S(2)}) collective-permute-start(bf16[2,2,512,256]{3,2,1,0:T(8,128)(2,1)S(1)} %get-tuple-element.62), channel_id=1, source_target_pairs={{0,1},{1,0},{2,3},{3,2},{4,5},{5,4},{6,7},{7,6},{8,9},{9,8},{10,11... | collective-permute-start | bytes 3145736 | tf_op jit(solution)/shard_map/ppermute | solution.py:35
  229.1 2.8 %collective-permute-start.20 = (bf16[2,2,512,256]{3,2,1,0:T(8,128)(2,1)S(1)}, bf16[2,2,512,256]{3,2,1,0:T(8,128)(2,1)S(1)}, u32[]{:S(2)}, u32[]{:S(2)}) collective-permute-start(bf16[2,2,512,256]{3,2,1,0:T(8,128)(2,1)S(1)} %get-tuple-element.50), channel_id=1, source_target_pairs={{0,1},{1,0},{2,3},{3,2},{4,5},{5,4},{6,7},{7,6},{8,9},{9,8},{10,11... | collective-permute-start | bytes 3145736 | tf_op jit(solution)/shard_map/ppermute | solution.py:35
  229.9 9.2 %collective-permute-start.30 = (bf16[2,512,128]{2,1,0:T(8,128)(2,1)S(1)}, bf16[2,512,128]{2,1,0:T(8,128)(2,1)S(1)}, u32[]{:S(2)}, u32[]{:S(2)}) collective-permute-start(bf16[2,512,128]{2,1,0:T(8,128)(2,1)S(1)} %get-tuple-element.64), channel_id=1, source_target_pairs={{0,2},{1,3},{2,0},{3,1},{4,6},{5,7},{6,4},{7,5},{8,10},{9,11},{10,... | collective-permute-start | bytes 786440 | tf_op jit(solution)/shard_map/ppermute | solution.py:35
  230.4 9.2 %collective-permute-start.31 = (bf16[2,512,128]{2,1,0:T(8,128)(2,1)S(1)}, bf16[2,512,128]{2,1,0:T(8,128)(2,1)S(1)}, u32[]{:S(2)}, u32[]{:S(2)}) collective-permute-start(bf16[2,512,128]{2,1,0:T(8,128)(2,1)S(1)} %get-tuple-element.66), channel_id=1, source_target_pairs={{0,8},{4,12},{8,0},{12,4},{16,24},{20,28},{24,16},{28,20},{1,9},{5... | collective-permute-start | bytes 786440 | tf_op jit(solution)/shard_map/ppermute | solution.py:33
  232.2 12.6 %collective-permute-start.21 = (bf16[2,512,128]{2,1,0:T(8,128)(2,1)S(1)}, bf16[2,512,128]{2,1,0:T(8,128)(2,1)S(1)}, u32[]{:S(2)}, u32[]{:S(2)}) collective-permute-start(bf16[2,512,128]{2,1,0:T(8,128)(2,1)S(1)} %get-tuple-element.52), channel_id=1, source_target_pairs={{0,2},{1,3},{2,0},{3,1},{4,6},{5,7},{6,4},{7,5},{8,10},{9,11},{10,... | collective-permute-start | bytes 786440 | tf_op jit(solution)/shard_map/ppermute | solution.py:35
  232.7 12.5 %collective-permute-start.22 = (bf16[2,512,128]{2,1,0:T(8,128)(2,1)S(1)}, bf16[2,512,128]{2,1,0:T(8,128)(2,1)S(1)}, u32[]{:S(2)}, u32[]{:S(2)}) collective-permute-start(bf16[2,512,128]{2,1,0:T(8,128)(2,1)S(1)} %get-tuple-element.54), channel_id=1, source_target_pairs={{0,8},{4,12},{8,0},{12,4},{16,24},{20,28},{24,16},{28,20},{1,9},{5... | collective-permute-start | bytes 786440 | tf_op jit(solution)/shard_map/ppermute | solution.py:33
  239.7 8.1 %collective-permute-start.32 = (bf16[512,128]{1,0:T(8,128)(2,1)S(1)}, bf16[512,128]{1,0:T(8,128)(2,1)S(1)}, u32[]{:S(2)}, u32[]{:S(2)}) collective-permute-start(bf16[512,128]{1,0:T(8,128)(2,1)S(1)} %get-tuple-element.68), channel_id=1, source_target_pairs={{0,8},{4,12},{8,0},{12,4},{16,24},{20,28},{24,16},{28,20},{1,9},{5... | collective-permute-start | bytes 393224 | tf_op jit(solution)/shard_map/ppermute | solution.py:33
  240.1 7.8 %collective-permute-start.33 = (bf16[512,128]{1,0:T(8,128)(2,1)S(1)}, bf16[512,128]{1,0:T(8,128)(2,1)S(1)}, u32[]{:S(2)}, u32[]{:S(2)}) collective-permute-start(bf16[512,128]{1,0:T(8,128)(2,1)S(1)} %get-tuple-element.70), channel_id=1, source_target_pairs={{0,2},{1,3},{2,0},{3,1},{4,6},{5,7},{6,4},{7,5},{8,10},{9,11},{10,... | collective-permute-start | bytes 393224 | tf_op jit(solution)/shard_map/ppermute | solution.py:35
  245.3 5.0 %collective-permute-start.23 = (bf16[512,128]{1,0:T(8,128)(2,1)S(1)}, bf16[512,128]{1,0:T(8,128)(2,1)S(1)}, u32[]{:S(2)}, u32[]{:S(2)}) collective-permute-start(bf16[512,128]{1,0:T(8,128)(2,1)S(1)} %get-tuple-element.56), channel_id=1, source_target_pairs={{0,8},{4,12},{8,0},{12,4},{16,24},{20,28},{24,16},{28,20},{1,9},{5... | collective-permute-start | bytes 393224 | tf_op jit(solution)/shard_map/ppermute | solution.py:33
  245.7 5.0 %collective-permute-start.24 = (bf16[512,128]{1,0:T(8,128)(2,1)S(1)}, bf16[512,128]{1,0:T(8,128)(2,1)S(1)}, u32[]{:S(2)}, u32[]{:S(2)}) collective-permute-start(bf16[512,128]{1,0:T(8,128)(2,1)S(1)} %get-tuple-element.58), channel_id=1, source_target_pairs={{0,2},{1,3},{2,0},{3,1},{4,6},{5,7},{6,4},{7,5},{8,10},{9,11},{10,... | collective-permute-start | bytes 393224 | tf_op jit(solution)/shard_map/ppermute | solution.py:35
